TPU v7x, 128 devices: a whole 4x4x4 slice. The times are simulated.
128 devices in a mesh: dp: 4 (over x), kv: 16 (over z, y), tp: 2 (over core).
Axes of the slice: x: 4, y: 4, z: 4, core: 2. Of those that a mesh axis runs over, the one named last changes fastest.
Arguments:
- tokens: bfloat16 [1024, 2048], P(('dp', 'kv', 'tp')), may hold values from -6 to 6
- norm_gain: float32 [2048], replicated, may hold values from 0.1 to 1.9
- gate_proj: bfloat16 [2048, 4096], P(None, ('kv', 'tp')), may hold values from -0.125 to 0.125
- inner_proj: bfloat16 [2048, 4096], P(None, ('kv', 'tp')), may hold values from -0.125 to 0.125
- write_proj: bfloat16 [2048, 1024], P(None, ('kv', 'tp')), may hold values from -0.125 to 0.125
- read_proj: bfloat16 [2048, 1024], P(None, ('kv', 'tp')), may hold values from -0.125 to 0.125
- step_proj: bfloat16 [2048, 64], replicated, may hold values from -0.125 to 0.125
- step_bias: float32 [64], replicated, may hold values from -3 to 0
- decay_log: float32 [64], replicated, may hold values from -5 to 0.7
- skip_gain: float32 [64], replicated, may hold values from 0.25 to 4
- conv_inner: bfloat16 [4, 4096], replicated, may hold values from -3 to 3
- conv_write: bfloat16 [4, 1024], replicated, may hold values from -3 to 3
- conv_read: bfloat16 [4, 1024], replicated, may hold values from -3 to 3
- out_gain: float32 [4096], replicated, may hold values from 0.1 to 1.9
- out_proj: bfloat16 [4096, 2048], P(('kv', 'tp')), may hold values from -0.09375 to 0.09375
- saved_state: float32 [256, 64, 64, 128], P('dp', ('kv', 'tp')), may hold values from -1.75 to 1.75
- inner_history: bfloat16 [256, 7, 4096], P('dp', None, ('kv', 'tp')), may hold values from -6 to 6
- write_history: bfloat16 [256, 7, 1024], P('dp', None, ('kv', 'tp')), may hold values from -6 to 6
- read_history: bfloat16 [256, 7, 1024], P('dp', None, ('kv', 'tp')), may hold values from -6 to 6
- last_steps: float32 [256, 4, 64], P('dp', None, ('kv', 'tp')), may hold values from 0.02 to 1
- accepted: int32 [256], P('dp'), may hold values from 0 to 4
Outputs:
- mixed: bfloat16 [1024, 2048], P(('dp', 'kv', 'tp'))
- base_state: float32 [256, 64, 64, 128], P('dp', ('kv', 'tp'))
All inputs are finite; a program needn't handle non-finite values.
Results may differ from a plain program's by a relative error of at most 0.014.
Values may be sent and summed in bfloat16 or wider, within the bound.
No kernel may reach another device: no remote copies, remote signals or barrier semaphores. Data moves between devices by JAX's collectives and lax.ppermute only.
A program may use at most 64 MiB of HBM per device.

v0:
```python
import math

import jax
import jax.numpy as jnp
from jax import lax
from jax.sharding import PartitionSpec as P

INNER = 4096


EPSILON = 0.1
highest = lax.Precision.HIGHEST


def sent_to_all(shard, axis):
    count = lax.axis_size(axis)
    return lax.all_to_all(
        jnp.broadcast_to(shard[None], (count, *shard.shape)), axis, 0, 0, tiled=True
    )


def in_order(tiles, dim):
    tiles = jnp.moveaxis(tiles, 0, dim)
    lengths = tiles.shape
    return tiles.reshape(*lengths[:dim], lengths[dim] * lengths[dim + 1], *lengths[dim + 2 :])


def gather_directly(shard, axis, dim):
    tiles = sent_to_all(shard, axis)
    return in_order(tiles, dim)


def turned_gather(arrays, axis, dims):
    turned = [jnp.moveaxis(a, dim, 0) for a, dim in zip(arrays, dims)]
    both = jnp.concatenate([t.reshape(len(t), -1) for t in turned], axis=1)
    result, at, done = (lax.all_gather(both, axis, axis=0, tiled=True), 0, [])
    for t, dim in zip(turned, dims):
        share = result[:, at : at + t[0].size].reshape(-1, *t.shape[1:])
        done.append(jnp.moveaxis(share, 0, dim))
        at += t[0].size
    return tuple(done)


def swapped(value, axis, stride):
    mask = 2**stride
    pairs = [(source, source ^ mask) for source in range(lax.axis_size(axis))]
    return lax.ppermute(value, axis, pairs)


def in_blocks(shard, dim, count):
    lengths = shard.shape
    tiles = shard.reshape(*lengths[:dim], count, lengths[dim] // count, *lengths[dim + 1 :])
    return jnp.moveaxis(tiles, dim, 0)


def summed_on_arrival(shard, axis, dim):
    tiles = in_blocks(shard, dim, lax.axis_size(axis))
    arrived = lax.all_to_all(tiles, axis, split_axis=0, concat_axis=0, tiled=True)
    return arrived.astype(jnp.float32).sum(axis=0)


def sent_together(arrays, axis, dim, along):
    widths = [math.prod(a.shape[along:]) for a in arrays]
    both = jnp.concatenate(
        [a.reshape(*a.shape[:along], w) for a, w in zip(arrays, widths)], axis=along
    )
    result = summed_on_arrival(both, axis, dim)
    tiles = jnp.split(result, [sum(widths[:k]) for k in range(1, len(widths))], axis=along)
    return tuple(
        (b.reshape(*result.shape[:along], *a.shape[along:]) for a, b in zip(arrays, tiles))
    )


def conv_rows(row_block, weight):
    out_len = row_block.shape[1] - weight.shape[0] + 1
    result = weight[0] * row_block[:, 0:out_len]
    for offset in range(1, weight.shape[0]):
        result = result + weight[offset] * row_block[:, offset : offset + out_len]
    return result


def body(
    tokens,
    norm_gain,
    gate_proj,
    inner_proj,
    write_proj,
    read_proj,
    step_proj,
    step_bias,
    decay_log,
    skip_gain,
    conv_inner,
    conv_write,
    conv_read,
    out_gain,
    out_proj,
    saved_state,
    inner_history,
    write_history,
    read_history,
    last_steps,
    accepted,
):
    device_rank = lax.axis_index(("kv", "tp"))
    seq_count = saved_state.shape[0]
    local_heads = saved_state.shape[1]
    head_dim = saved_state.shape[2]
    proposals = last_steps.shape[1]
    inner_cols = inner_proj.shape[1]
    state_cols = write_proj.shape[1]
    token_count = tokens.shape[0]
    own_rows = tokens.astype(jnp.float32)
    normed_own = (
        own_rows
        * lax.rsqrt(jnp.mean(own_rows * own_rows, axis=-1, keepdims=True) + EPSILON)
        * norm_gain
    ).astype(jnp.bfloat16)
    normed = gather_directly(normed_own, ("kv", "tp"), 0)
    gate_rows = jnp.dot(normed, gate_proj, preferred_element_type=jnp.float32).astype(jnp.bfloat16)
    inner_rows = jnp.dot(normed, inner_proj, preferred_element_type=jnp.float32).astype(
        jnp.bfloat16
    )
    write_rows = jnp.dot(normed, write_proj, preferred_element_type=jnp.float32).astype(
        jnp.bfloat16
    )
    read_rows = jnp.dot(normed, read_proj, preferred_element_type=jnp.float32).astype(jnp.bfloat16)
    first_head = device_rank * local_heads
    step_weight = lax.dynamic_slice_in_dim(step_proj, first_head, local_heads, 1)
    step_rows = jnp.dot(normed, step_weight, preferred_element_type=jnp.float32)
    taps_inner = lax.dynamic_slice_in_dim(
        conv_inner, device_rank * inner_cols, inner_cols, 1
    ).astype(jnp.float32)
    taps_write = lax.dynamic_slice_in_dim(
        conv_write, device_rank * state_cols, state_cols, 1
    ).astype(jnp.float32)
    taps_read = lax.dynamic_slice_in_dim(conv_read, device_rank * state_cols, state_cols, 1).astype(
        jnp.float32
    )
    conv_width = conv_inner.shape[0]
    window_rows = accepted[:, None] + jnp.arange(conv_width - 1, dtype=jnp.int32)[None, :]

    def current(history, new_rows, weight):
        window = jnp.take_along_axis(history, window_rows[:, :, None], axis=1)
        joined = jnp.concatenate([window, new_rows.reshape(seq_count, proposals, -1)], axis=1)
        return jax.nn.silu(conv_rows(joined.astype(jnp.float32), weight))

    inner_old = jax.nn.silu(conv_rows(inner_history.astype(jnp.float32), taps_inner))
    write_old = jax.nn.silu(conv_rows(write_history.astype(jnp.float32), taps_write)).astype(
        jnp.bfloat16
    )
    inner_new = current(inner_history, inner_rows, taps_inner)
    write_new = current(write_history, write_rows, taps_write).astype(jnp.bfloat16)
    read_new = current(read_history, read_rows, taps_read).astype(jnp.bfloat16)
    write_both = jnp.concatenate([write_old, write_new], axis=1)
    pieces = (write_both, read_new)
    pieces = turned_gather((pieces[0], pieces[1]), "tp", (2, 2))
    kv_rank = lax.axis_index("kv")
    partner = swapped((pieces[0], pieces[1]), "kv", 0)
    lower = jnp.bitwise_and(jnp.right_shift(kv_rank, 0), 1) == 0
    pieces = tuple(
        (
            jnp.where(
                lower,
                jnp.concatenate([mine, theirs], axis=2),
                jnp.concatenate([theirs, mine], axis=2),
            )
            for mine, theirs in zip(pieces, partner)
        )
    )
    write_group = pieces[0].astype(jnp.float32)
    read_group = pieces[1].astype(jnp.float32)
    write_past = write_group[:, :proposals]
    write_next = write_group[:, proposals:]
    decay_rate = -jnp.exp(lax.dynamic_slice_in_dim(decay_log, first_head, local_heads, 0))
    skip_local = lax.dynamic_slice_in_dim(skip_gain, first_head, local_heads, 0)
    bias_local = lax.dynamic_slice_in_dim(step_bias, first_head, local_heads, 0)
    step_size = jax.nn.softplus(step_rows + bias_local[None, :]).reshape(
        seq_count, proposals, local_heads
    )
    accepted_mask = (jnp.arange(proposals, dtype=jnp.int32)[None, :] < accepted[:, None]).astype(
        jnp.float32
    )
    step_logs = decay_rate[None, None, :] * last_steps * accepted_mask[:, :, None]
    total_log = jnp.sum(step_logs, axis=1)
    tail_log = total_log[:, None, :] - jnp.cumsum(step_logs, axis=1)
    old_weights = accepted_mask[:, :, None] * jnp.exp(tail_log) * last_steps
    inner_old_heads = inner_old.reshape(seq_count, proposals, local_heads, head_dim)
    base_state = jnp.exp(total_log)[:, :, None, None] * saved_state + jnp.einsum(
        "sth,sthp,stn->shpn", old_weights, inner_old_heads, write_past, precision=highest
    )
    cumulative = jnp.cumsum(decay_rate[None, None, :] * step_size, axis=1)
    log_gap = cumulative[:, :, None, :] - cumulative[:, None, :, :]
    causal = (jnp.arange(proposals)[:, None] >= jnp.arange(proposals)[None, :])[None, :, :, None]
    kernel = jnp.where(causal, jnp.exp(jnp.where(causal, log_gap, 0.0)), 0.0)
    scores = jnp.einsum("sin,sjn->sij", read_group, write_next, precision=highest)
    inner_heads = inner_new.reshape(seq_count, proposals, local_heads, head_dim)
    within = jnp.einsum(
        "sijh,sjh,sjhp->sihp", kernel * scores[..., None], step_size, inner_heads, precision=highest
    )
    carried = jnp.exp(cumulative)[..., None] * jnp.einsum(
        "sin,shpn->sihp", read_group, base_state, precision=highest
    )
    mixed_heads = within + carried + skip_local[None, None, :, None] * inner_heads
    gated_rows = mixed_heads.reshape(seq_count * proposals, inner_cols) * jax.nn.silu(
        gate_rows.astype(jnp.float32)
    )
    gain_local = lax.dynamic_slice_in_dim(out_gain, device_rank * inner_cols, inner_cols, 0)
    squares = jnp.sum(gated_rows * gated_rows, axis=-1)
    unscaled = (gated_rows * gain_local).astype(jnp.bfloat16)
    partial_value = jnp.dot(unscaled, out_proj, preferred_element_type=jnp.float32)
    kv_count = lax.axis_size("kv")
    tp_count = lax.axis_size("tp")
    blocks = partial_value.reshape(kv_count, tp_count, token_count, partial_value.shape[1])
    square_blocks = squares.reshape(kv_count, tp_count, token_count)
    half_terms, half_squares = sent_together(
        (blocks.astype(jnp.bfloat16), square_blocks.astype(jnp.bfloat16)), "tp", 1, 3
    )
    wide_terms, wide_squares = sent_together(
        (half_terms.astype(jnp.bfloat16), half_squares.astype(jnp.bfloat16)), "kv", 0, 3
    )
    summed = wide_terms.reshape(token_count, partial_value.shape[1])
    square_own = wide_squares.reshape(token_count)
    mixed = (summed * lax.rsqrt(square_own / INNER + EPSILON)[:, None]).astype(jnp.bfloat16)
    return (mixed, base_state)


def solution(mesh):
    placed = (
        P(("dp", "kv", "tp"), None),
        P(),
        P(None, ("kv", "tp")),
        P(None, ("kv", "tp")),
        P(None, ("kv", "tp")),
        P(None, ("kv", "tp")),
        P(),
        P(),
        P(),
        P(),
        P(),
        P(),
        P(),
        P(),
        P(("kv", "tp"), None),
        P("dp", ("kv", "tp"), None, None),
        P("dp", None, ("kv", "tp")),
        P("dp", None, ("kv", "tp")),
        P("dp", None, ("kv", "tp")),
        P("dp", None, ("kv", "tp")),
        P("dp"),
    )
    return jax.shard_map(
        body,
        mesh=mesh,
        in_specs=placed,
        out_specs=(P(("dp", "kv", "tp"), None), P("dp", ("kv", "tp"), None, None)),
        check_vma=False,
    )
```

profile of v0, /device:TPU:0, one launch (start us, length us, event | category | flops | bytes accessed | tf_op | source)
XLA Modules:
  0.0 78.3 jit_solution(1773336176928143234)
XLA Ops:
  0.7 1.0 %fusion.28 = f32[8]{0:T(128)S(1)} fusion(bf16[8,2048]{1,0:T(8,128)(2,1)} %param.23), kind=kLoop, calls=%fused_computation.61 | loop fusion | flops 49144 | bytes 32800 | tf_op jit(solution)/shard_map/reduce_sum | solution.py:116
  1.7 0.8 %fusion.30 = bf16[8,2048]{1,0:T(8,128)(2,1)S(1)} fusion(bf16[8,2048]{1,0:T(8,128)(2,1)} %param.23, f32[2048]{0:T(1024)} %param.24, f32[8]{0:T(128)S(1)} %add_rsqrt_fusion), kind=kLoop, calls=%fused_computation.63 | loop fusion | flops 65536 | bytes 73760 | tf_op jit(solution)/shard_map/convert_element_type | solution.py:118
  2.6 1.1 %broadcast_in_dim.30 = bf16[32,8,2048]{2,1,0:T(8,128)(2,1)} broadcast(bf16[8,2048]{1,0:T(8,128)(2,1)S(1)} %fusion.30), dimensions={1,2} | broadcast | bytes 1081344 | tf_op jit(solution)/shard_map/broadcast_in_dim | solution.py:18
  3.7 8.4 %all-to-all-start = ((bf16[32,8,2048]{2,1,0:T(8,128)(2,1)}), bf16[32,8,2048]{2,1,0:T(8,128)(2,1)S(1)}, u32[]{:S(2)}, u32[]{:S(2)}) async-start(bf16[32,8,2048]{2,1,0:T(8,128)(2,1)} %broadcast_in_dim.30), calls=%async_computation | async-start | bytes 2097152 | tf_op jit(solution)/shard_map/all_to_all | solution.py:17
  12.1 0.8 shift-left_or_fusion
  12.9 0.7 fusion.49
  13.7 0.7 fusion.62
  14.3 0.7 fusion.50
  15.2 0.9 %copy.134 = bf16[64,7,32]{2,0,1:T(8,128)(2,1)S(1)} copy(bf16[64,7,32]{0,2,1:T(8,128)(2,1)} %param.40) | data formatting | bytes 57344 | tf_op args[17]
  16.1 2.4 %gather_fusion.1 = bf16[192,32]{1,0:T(8,128)(2,1)S(1)} fusion(bf16[64,7,32]{2,0,1:T(8,128)(2,1)S(1)} %copy.134, s32[192]{0:T(256)S(1)} %reshape.264), kind=kCustom, calls=%fused_computation.clone | custom fusion | bytes 26112 | tf_op jit(solution)/shard_map/jit(take_along_axis)/gather | solution.py:144
  18.7 2.4 %gather_fusion.2 = bf16[192,32]{1,0:T(8,128)(2,1)S(1)} fusion(bf16[64,7,32]{2,0,1:T(8,128)(2,1)S(1)} %copy.139, s32[192]{0:T(256)S(1)} %reshape.264), kind=kCustom, calls=%fused_computation.1.clone | custom fusion | bytes 26112 | tf_op jit(solution)/shard_map/jit(take_along_axis)/gather | solution.py:144
  21.2 2.4 %gather_fusion = bf16[192,128]{1,0:T(8,128)(2,1)S(1)} fusion(bf16[64,7,128]{2,0,1:T(8,128)(2,1)S(1)} %copy-done.2, s32[192]{0:T(256)S(1)} %reshape.264), kind=kCustom, calls=%fused_computation.2 | custom fusion | bytes 99840 | tf_op jit(solution)/shard_map/jit(take_along_axis)/gather | solution.py:144
  25.7 0.8 dynamic_slice.31
  26.5 0.7 dynamic-slice_convert_fusion.2
  27.2 0.8 dynamic-slice_convert_fusion
  28.0 1.4 %all-to-all-done = bf16[32,8,2048]{2,1,0:T(8,128)(2,1)S(1)} async-done(((bf16[32,8,2048]{2,1,0:T(8,128)(2,1)}), bf16[32,8,2048]{2,1,0:T(8,128)(2,1)S(1)}, u32[]{:S(2)}, u32[]{:S(2)}) %all-to-all-start) | async-done | bytes 1048608 | tf_op jit(solution)/shard_map/all_to_all | solution.py:17
  30.4 0.4 convolution_convert_fusion.3
  31.5 1.9 %all_gather.3 = bf16[64,768]{1,0:T(8,128)(2,1)S(1)} all-gather(bf16[32,768]{1,0:T(8,128)(2,1)S(1)} %pad_maximum_fusion), channel_id=1, replica_groups=mesh['dp'=4,'kv'=16,'tp'=2] {'tp'}, dimensions={0}, use_global_device_ids=true | all-gather | bytes 147456 | tf_op jit(solution)/shard_map/all_gather | solution.py:36
  33.5 0.7 collective-permute-start.1
  34.1 0.4 convolution_convert_fusion.2
  34.6 1.2 %compare_select_fusion.1 = f32[256,2]{0,1:T(2,128)S(1)} fusion(bf16[2048,64]{0,1:T(8,128)(2,1)} %param.29, s32[]{:T(128)S(6)} %select_n.67, bf16[32,8,2048]{2,1,0:T(8,128)(2,1)S(1)} %all-to-all-done, f32[2]{0:T(128)S(1)} %dynamic_slice.25), kind=kOutput, calls=%fused_computation.116 | convolution fusion | flops 2100736 | bytes 1058828 | tf_op jit(solution)/shard_map/dot_general | solution.py:130
  36.2 0.6 copy.128
  37.8 1.7 %collective-permute-start = (bf16[64,4,64]{2,1,0:T(4,128)(2,1)S(1)}, bf16[64,4,64]{2,1,0:T(4,128)(2,1)S(1)}, u32[]{:S(2)}, u32[]{:S(2)}) collective-permute-start(bf16[64,4,64]{2,1,0:T(4,128)(2,1)S(1)} %bitcast.109), channel_id=1, source_target_pairs={{0,2},{2,0},{4,6},{6,4},{8,10},{10,8},{12,14},{14,12},{16,18},{18,... | collective-permute-start | bytes 98312 | tf_op jit(solution)/shard_map/ppermute | solution.py:47
  39.9 5.9 %multiply_add_fusion = f32[64,2,64,128]{3,2,1,0:T(8,128)S(1)} fusion(f32[64,2,64,128]{3,2,1,0:T(8,128)} %param.38, f32[64,2]{1,0:T(8,128)S(1)} %copy.153, f32[64,4,2,64]{3,2,0,1:T(2,128)S(1)} %reshape.245, f32[64,4,2]{1,2,0:T(2,128)S(1)} %copy.155, bf16[64,8,128]{2,1,0:T(8,128)(2,1)S(1)} %maximum_select_fusion), kind=kOutput, calls=%fused_computation.3 | convolution fusion | flops 52461568 | bytes 8814592 | tf_op jit(solution)/shard_map/sth,sthp,stn->shpn/dot_general | solution.py:189
  46.2 5.0 %convolution_multiply_fusion = f32[64,4,2,64]{3,1,2,0:T(4,128)S(1)} fusion(f32[64,2,64,128]{3,2,1,0:T(8,128)S(1)} %multiply_add_fusion, f32[64,4,2]{1,2,0:T(2,128)S(1)} %copy.149, bf16[64,4,64]{2,1,0:T(4,128)(2,1)S(1)} %collective-permute-done, bf16[64,4,64]{2,1,0:T(4,128)(2,1)S(1)} %bitcast.111, pred[]{:T(512)S(6)} %eq.3), kind=kOutput, calls=%fused_computation.8 | convolution fusion | flops 50659328 | bytes 4392961 | tf_op jit(solution)/shard_map/sin,shpn->sihp/dot_general | solution.py:201
  51.2 1.3 %fusion.1 = f32[64,4,2,64]{3,1,2,0:T(4,128)S(1)} fusion(f32[64,4,2,64]{3,1,2,0:T(4,128)S(1)} %convolution_multiply_fusion, f32[64,4,2,64]{3,2,0,1:T(2,128)S(1)} %reshape.238, f32[64,4,2,64]{3,2,0,1:T(2,128)S(1)} %broadcast_multiply_fusion, f32[2]{0:T(128)S(1)} %dynamic_slice.30, f32[64,4,4]{2,1,0:T(4,128)S(1)} %fusion.33, f32[64,4,2]{1,2,0:T(2,128)S(1)} %copy.132, ...), kind=kOutput, calls=%fused_computation.7 | convolution fusion | flops 1679360 | bytes 530456 | tf_op jit(solution)/shard_map/sijh,sjh,sjhp->sihp/dot_general | solution.py:198
  52.9 0.5 multiply_reduce_fusion
  53.9 0.5 convolution_convert_fusion
  54.5 4.6 %all_to_all.15 = bf16[2,16,1,8,2049]{4,3,1,2,0:T(8,128)(2,1)S(1)} all-to-all(bf16[2,16,1,8,2049]{4,3,1,2,0:T(8,128)(2,1)S(1)} %maximum_bitcast_fusion), channel_id=1, replica_groups=mesh['dp'=4,'kv'=16,'tp'=2] {'tp'}, dimensions={0} | all-to-all | bytes 2098176 | tf_op jit(solution)/shard_map/all_to_all | solution.py:58
  59.1 0.4 reduce.2
  59.6 17.9 %all_to_all.16 = bf16[16,1,1,8,2049]{4,3,2,1,0:T(8,128)(2,1)S(1)} all-to-all(bf16[16,1,1,8,2049]{4,3,2,1,0:T(8,128)(2,1)S(1)} %bitcast.103), channel_id=1, replica_groups=mesh['dp'=4,'kv'=16,'tp'=2] {'kv'}, dimensions={0} | all-to-all | bytes 1049088 | tf_op jit(solution)/shard_map/all_to_all | solution.py:58
  77.6 0.7 fusion.32
  (100 shorter events, 7.3 us)
Async XLA Ops:
  0.6 53.2 %copy-start = (bf16[128,2048]{1,0:T(8,128)(2,1)S(1)}, bf16[128,2048]{1,0:T(8,128)(2,1)}, u32[]{:S(2)}) copy-start(bf16[128,2048]{1,0:T(8,128)(2,1)} %param.37) | copy-start | bytes 1572868
  0.6 24.3 %copy-start.4 = (bf16[64,7,32]{0,2,1:T(8,128)(2,1)S(1)}, bf16[64,7,32]{0,2,1:T(8,128)(2,1)}, u32[]{:S(2)}) copy-start(bf16[64,7,32]{0,2,1:T(8,128)(2,1)} %param.40) | copy-start | bytes 86020
  0.7 18.0 %copy-start.7 = (bf16[64,7,32]{0,2,1:T(8,128)(2,1)S(1)}, bf16[64,7,32]{0,2,1:T(8,128)(2,1)}, u32[]{:S(2)}) copy-start(bf16[64,7,32]{0,2,1:T(8,128)(2,1)} %param.41) | copy-start | bytes 86020
  0.7 20.6 %copy-start.2 = (bf16[64,7,128]{2,0,1:T(8,128)(2,1)S(1)}, bf16[64,7,128]{2,0,1:T(8,128)(2,1)}, u32[]{:S(2)}) copy-start(bf16[64,7,128]{2,0,1:T(8,128)(2,1)} %param.39) | copy-start | bytes 344068
  0.7 23.1 %copy-start.10 = (f32[64]{0:T(128)S(1)}, f32[64]{0:T(128)}, u32[]{:S(2)}) copy-start(f32[64]{0:T(128)} %param.31) | copy-start | bytes 772
  0.7 23.2 %copy-start.8 = (f32[64,4,2]{0,2,1:T(2,128)S(1)}, f32[64,4,2]{0,2,1:T(2,128)}, u32[]{:S(2)}) copy-start(f32[64,4,2]{0,2,1:T(2,128)} %param.42) | copy-start | bytes 6148
  0.7 24.9 %copy-start.11 = (f32[64]{0:T(128)S(1)}, f32[64]{0:T(128)}, u32[]{:S(2)}) copy-start(f32[64]{0:T(128)} %param.30) | copy-start | bytes 772
  0.7 24.9 %copy-start.12 = (f32[64]{0:T(128)S(1)}, f32[64]{0:T(128)}, u32[]{:S(2)}) copy-start(f32[64]{0:T(128)} %param.32) | copy-start | bytes 772
  0.7 28.6 %copy-start.5 = (bf16[2048,32]{0,1:T(8,128)(2,1)S(1)}, bf16[2048,32]{0,1:T(8,128)(2,1)}, u32[]{:S(2)}) copy-start(bf16[2048,32]{0,1:T(8,128)(2,1)} %param.27) | copy-start | bytes 393220
  3.7 25.7 %all-to-all-start = ((bf16[32,8,2048]{2,1,0:T(8,128)(2,1)}), bf16[32,8,2048]{2,1,0:T(8,128)(2,1)S(1)}, u32[]{:S(2)}, u32[]{:S(2)}) async-start(bf16[32,8,2048]{2,1,0:T(8,128)(2,1)} %broadcast_in_dim.30), calls=%async_computation | async-start | bytes 2097152 | tf_op jit(solution)/shard_map/all_to_all | solution.py:17
  12.1 18.3 %copy-start.6 = (bf16[2048,32]{0,1:T(8,128)(2,1)S(1)}, bf16[2048,32]{0,1:T(8,128)(2,1)}, u32[]{:S(2)}) copy-start(bf16[2048,32]{0,1:T(8,128)(2,1)} %param.28) | copy-start | bytes 393220
  21.2 13.0 %copy-start.3 = (bf16[2048,128]{1,0:T(8,128)(2,1)S(1)}, bf16[2048,128]{1,0:T(8,128)(2,1)}, u32[]{:S(2)}) copy-start(bf16[2048,128]{1,0:T(8,128)(2,1)} %param.26) | copy-start | bytes 1572868
  33.5 6.3 %collective-permute-start.1 = (bf16[64,8,64]{2,1,0:T(8,128)(2,1)S(1)}, bf16[64,8,64]{2,1,0:T(8,128)(2,1)S(1)}, u32[]{:S(2)}, u32[]{:S(2)}) collective-permute-start(bf16[64,8,64]{2,1,0:T(8,128)(2,1)S(1)} %bitcast.105), channel_id=1, source_target_pairs={{0,2},{2,0},{4,6},{6,4},{8,10},{10,8},{12,14},{14,12},{16,18},{18,... | collective-permute-start | bytes 196616 | tf_op jit(solution)/shard_map/ppermute | solution.py:47
  37.8 8.1 %collective-permute-start = (bf16[64,4,64]{2,1,0:T(4,128)(2,1)S(1)}, bf16[64,4,64]{2,1,0:T(4,128)(2,1)S(1)}, u32[]{:S(2)}, u32[]{:S(2)}) collective-permute-start(bf16[64,4,64]{2,1,0:T(4,128)(2,1)S(1)} %bitcast.109), channel_id=1, source_target_pairs={{0,2},{2,0},{4,6},{6,4},{8,10},{10,8},{12,14},{14,12},{16,18},{18,... | collective-permute-start | bytes 98312 | tf_op jit(solution)/shard_map/ppermute | solution.py:47
  45.8 6.7 %copy-start.1 = (f32[64,2,64,128]{3,2,1,0:T(8,128)}, f32[64,2,64,128]{3,2,1,0:T(8,128)S(1)}, u32[]{:S(2)}) copy-start(f32[64,2,64,128]{3,2,1,0:T(8,128)S(1)} %multiply_add_fusion) | copy-start | bytes 12582916
  46.1 6.8 %copy-start.9 = (bf16[2048,128]{1,0:T(8,128)(2,1)S(1)}, bf16[2048,128]{1,0:T(8,128)(2,1)}, u32[]{:S(2)}) copy-start(bf16[2048,128]{1,0:T(8,128)(2,1)} %param.25) | copy-start | bytes 1572868
where the time goes:
time: 78.9 us; the launch traced here: 78.3 us
  blocking collectives  24.4 us (31%)
  matrix products  16 us (20%)
  local copies, waits for them, and re-layouts  14.4 us (18%)
  starting transfers between devices  10.8 us (14%)
  other arithmetic  10 us (13%)
  waiting for transfers between devices  1.39 us (2%)
  between operations  1.25 us (2%)
    all_to_all x2, blocking collectives, summed_on_arrival(): lax.all_to_all(tiles, axis, split_axis=0, concat_axis=0, tiled=True)  22.5 us
    all_to_all x1, starting transfers between devices, sent_to_all(): lax.all_to_all(jnp.broadcast_to(shard[None], (count, *shard.shape)), axis...  8.45 us
    gather x7, local copies, waits for them, and re-layouts, current(): window = jnp.take_along_axis(history, window_rows[:, :, None], axis=1)  7.49 us
    dot_general x1, matrix products, body(): jnp.einsum('sth,sthp,stn->shpn', old_weights, inner_old_heads, write_past...  5.91 us
    dot_general x1, matrix products, body(): jnp.einsum('sin,shpn->sihp', read_group, base_state, precision=highest)  5 us
    ppermute x2, starting transfers between devices, swapped(): return lax.ppermute(value, axis, pairs)  2.37 us
    all_gather x1, blocking collectives, turned_gather(): result, at, done = (lax.all_gather(both, axis, axis=0, tiled=True), 0, [])  1.88 us
  transfers between devices with their start and end apart: 3, of which 1 were waited for; matrix products, arithmetic and copies ran while one was open for 33% of the time, Pallas kernels for 0%

commit v1 on v0

v1 whole, which is shorter than its diff:
```python
import jax
import jax.numpy as jnp
from jax import lax
from jax.experimental import pallas as pl
from jax.experimental.pallas import tpu as pltpu
from jax.sharding import PartitionSpec as P


EPSILON = 0.1
INNER = 4096
f32 = jnp.float32
bf16 = jnp.bfloat16
NT = (((1,), (1,)), ((), ()))
NN = (((1,), (0,)), ((), ()))


def dot(a, b, dims=NN):
    return lax.dot_general(a, b, dims, preferred_element_type=f32)


def silu(x):
    return x * (1.0 / (1.0 + jnp.exp(-x)))


def fetch(pairs, sems):
    copies = [pltpu.make_async_copy(src, dst, sems.at[k]) for k, (src, dst) in enumerate(pairs)]
    for copy in copies:
        copy.start()
    return copies


def device_rank():
    return lax.axis_index("kv") * 2 + lax.axis_index("tp")


def begin_kernel(
    tok_hbm, w_hbm, r_hbm, wh_hbm, rh_hbm, all_ref, out_ref, tok_s, wh_s, rh_s, sems
):
    copies = fetch(
        (
            (tok_hbm, tok_s),
            (wh_hbm, wh_s),
            (rh_hbm, rh_s),
            (w_hbm, out_ref.at[0:32]),
            (r_hbm, out_ref.at[32:64]),
        ),
        sems,
    )
    copies[0].wait()
    for k in range(16):
        all_ref[k] = tok_s[...]
    copies[1].wait()
    copies[2].wait()
    for t in range(7):
        both = jnp.concatenate([wh_s[t].astype(f32), rh_s[t].astype(f32)], axis=1).astype(bf16)
        out_ref[64:80, t * 128 : (t + 1) * 128] = both[0:16]
        out_ref[64:80, (7 + t) * 128 : (8 + t) * 128] = both[16:32]
    out_ref[64:80, 1792:2048] = jnp.zeros((16, 256), bf16)
    copies[3].wait()
    copies[4].wait()


def windows(rows, acc):
    out = []
    for j in range(3):
        w = rows[j]
        for a in range(1, 5):
            w = jnp.where(acc == a, rows[a + j], w)
        out.append(w)
    return out


def old_parts(taps, w):
    return (
        taps[0] * w[0] + taps[1] * w[1] + taps[2] * w[2],
        taps[0] * w[1] + taps[1] * w[2],
        taps[0] * w[2],
    )


def prep_kernel(
    saved_hbm,
    ihist_hbm,
    tin_hbm,
    tw_hbm,
    tr_hbm,
    gain_hbm,
    ls_hbm,
    acc_hbm,
    decay_hbm,
    skip_hbm,
    bias_hbm,
    step_hbm,
    low_hbm,
    hin_ref,
    a_ref,
    tot_ref,
    acc_ref,
    wide_hbm,
    vec_ref,
    low_s,
    wide_s,
    saved_s,
    ihist_s,
    tin_s,
    tw_s,
    tr_s,
    gain_s,
    ls_s,
    acc_s,
    heads_s,
    step_s,
    sems,
    sent,
):
    rank = device_rank()
    head = rank * 2
    col = pl.multiple_of(rank * 128, 128)
    group = pl.multiple_of((rank >> 2) * 128, 128)
    small = (
        (acc_hbm, acc_s),
        (ls_hbm, ls_s),
        (decay_hbm, heads_s.at[0:1]),
        (skip_hbm, heads_s.at[1:2]),
        (bias_hbm, heads_s.at[2:3]),
        (tin_hbm.at[:, pl.ds(col, 128)], tin_s),
        (tw_hbm.at[:, pl.ds(group, 128)], tw_s),
        (tr_hbm.at[:, pl.ds(group, 128)], tr_s),
        (gain_hbm.at[:, pl.ds(col, 128)], gain_s),
        (ihist_hbm, ihist_s),
        (step_hbm, step_s),
    )
    big = tuple(
        (saved_hbm.at[k * 8 : (k + 1) * 8], saved_s.at[k * 8 : (k + 1) * 8]) for k in range(8)
    )
    copies = fetch(small + big, sems)
    for copy in copies[: len(small)]:
        copy.wait()

    tin = tin_s[...].astype(f32)
    vec_ref[0:4, :] = tin
    vec_ref[4:8, :] = tw_s[...].astype(f32)
    vec_ref[8:12, :] = tr_s[...].astype(f32)
    place = lax.broadcasted_iota(jnp.int32, (1, 64), 1)
    first = lax.broadcasted_iota(jnp.int32, (1, 128), 1) < 64

    def of_head(k, h):
        return jnp.sum(jnp.where(place == head + h, heads_s[k : k + 1], 0.0), axis=-1, keepdims=True)

    def spread(k):
        return jnp.where(first, of_head(k, 0), of_head(k, 1))

    vec_ref[12:13, :] = -jnp.exp(spread(0))
    vec_ref[13:14, :] = spread(1)
    vec_ref[14:15, :] = spread(2)
    vec_ref[15:16, :] = gain_s[...]

    acc_row = acc_s[...]
    acc = jnp.broadcast_to(acc_row.astype(f32), (128, 64)).T
    acc_ref[...] = acc
    rows = [ihist_s[t].astype(f32) for t in range(7)]
    taps = [tin[k : k + 1] for k in range(4)]
    for i, part in enumerate(old_parts(taps, windows(rows, acc))):
        hin_ref[i] = part

    def wide(pair):
        return jnp.concatenate([jnp.broadcast_to(v, (64, 64)) for v in pair], axis=0).T

    weights = [[], [], [], []]
    totals = []
    for h in range(2):
        rate = -jnp.exp(of_head(0, h))
        steps = [ls_s[t, h : h + 1, :] for t in range(4)]
        keep = [(acc_row > t).astype(f32) for t in range(4)]
        logs = [rate * steps[t] * keep[t] for t in range(4)]
        tail = jnp.zeros((1, 64), f32)
        for t in (3, 2, 1, 0):
            weights[t].append(keep[t] * jnp.exp(tail) * steps[t])
            tail = tail + logs[t]
        totals.append(jnp.exp(tail))
    tot_ref[...] = wide(totals)
    for t in range(4):
        a_ref[t] = silu(sum(taps[k] * rows[t + k] for k in range(4))) * wide(weights[t])

    pick = lax.broadcasted_iota(jnp.int32, (128, 64), 1) == (
        head + (lax.broadcasted_iota(jnp.int32, (128, 64), 0) >> 6)
    )
    wide_s[...] = dot(pick.astype(f32).astype(bf16), step_s[...]).astype(bf16)
    out = [pltpu.make_async_copy(wide_s, wide_hbm, sent.at[8])]
    out[0].start()
    for k in range(8):
        block = slice(k * 8, (k + 1) * 8)
        copies[len(small) + k].wait()
        low_s[block] = saved_s[block].astype(bf16)
        out.append(pltpu.make_async_copy(low_s.at[block], low_hbm.at[block], sent.at[k]))
        out[-1].start()
    for copy in out:
        copy.wait()


def group_kernel(p0_ref, p1_ref, p2_ref, p3_ref, acc_ref, vec_ref, wall_hbm, hwr_ref, b_ref, wall_s, hist_s, sems):
    member = device_rank() & 3
    for x, p in enumerate((p0_ref, p1_ref, p2_ref, p3_ref)):
        at = pl.multiple_of((member ^ x) * 32, 32)
        wall_s[pl.ds(at, 32), :] = p[0:32, :]
        wall_s[pl.ds(128 + at, 32), :] = p[32:64, :]
        for t in range(7):
            hist_s[t, pl.ds(at, 16), :] = p[64:80, t * 128 : (t + 1) * 128].astype(f32)
            hist_s[t, pl.ds(at + 16, 16), :] = p[64:80, (7 + t) * 128 : (8 + t) * 128].astype(f32)
    copy = pltpu.make_async_copy(wall_s, wall_hbm, sems.at[0])
    copy.start()
    both = [hist_s[t].T for t in range(7)]
    acc = acc_ref[...]
    acc2 = jnp.concatenate([acc, acc], axis=0)
    taps = [
        jnp.concatenate(
            [
                jnp.broadcast_to(vec_ref[4 + k : 5 + k, :], (64, 128)),
                jnp.broadcast_to(vec_ref[8 + k : 9 + k, :], (64, 128)),
            ],
            axis=0,
        )
        for k in range(4)
    ]
    for i, part in enumerate(old_parts(taps, windows(both, acc2))):
        hwr_ref[i] = part
    for t in range(4):
        w_old = silu(sum(vec_ref[4 + k : 5 + k, :] * both[t + k][0:64] for k in range(4)))
        b_ref[t] = w_old.astype(bf16).astype(f32)
    copy.wait()


def state_kernel(saved_hbm, a_ref, b_ref, tot_ref, after_ref, base_hbm, saved_s, base_s, sems, sent):
    blocks = [slice(k * 8, (k + 1) * 8) for k in range(8)]
    copies = fetch([(saved_hbm.at[k], saved_s.at[k]) for k in blocks], sems)
    tot = tot_ref[...]
    tot = jnp.concatenate([tot, tot], axis=0).T
    at = jnp.concatenate(
        [jnp.concatenate([a_ref[2 * p], a_ref[2 * p + 1]], axis=0).T for p in range(2)], axis=1
    ).astype(bf16)
    b = b_ref[...].reshape(256, 128).astype(bf16)
    lane = lax.broadcasted_iota(jnp.int32, (1, 256), 1) & 63
    out = []
    for k in range(8):
        copies[k].wait()
        for s in range(k * 8, (k + 1) * 8):
            mask = (lane == s).astype(f32).astype(bf16)
            base_s[s] = saved_s[s] * tot[:, s : s + 1] + dot(at * mask, b)
        copy = pltpu.make_async_copy(base_s.at[blocks[k]], base_hbm.at[blocks[k]], sent.at[k])
        copy.start()
        out.append(copy)
    for copy in out:
        copy.wait()


def main_kernel(
    mine_ref,
    other_ref,
    norm_hbm,
    gate_hbm,
    inner_hbm,
    step_hbm,
    wall_hbm,
    low_hbm,
    own_hbm,
    hin_ref,
    hwr_ref,
    vec_ref,
    a_ref,
    b_ref,
    tot_ref,
    keep_ref,
    give_ref,
    own_ref,
    norm_ref,
    gate_ref,
    inner_ref,
    step_ref,
    wall_ref,
    low_ref,
    nrm_s,
    rows_s,
    read_s,
    car_s,
    sems,
):
    copies = fetch(
        (
            (norm_hbm, norm_ref),
            (step_hbm, step_ref),
            (wall_hbm, wall_ref),
            (inner_hbm, inner_ref),
            (gate_hbm, gate_ref),
            (low_hbm, low_ref),
            (own_hbm, own_ref),
        ),
        sems,
    )
    copies[0].wait()
    core = lax.axis_index("tp")
    even = core == 0
    gain = norm_ref[...]
    for kv in range(16):
        a = mine_ref[kv].astype(f32)
        b = other_ref[kv].astype(f32)
        x = jnp.concatenate([jnp.where(even, a, b), jnp.where(even, b, a)], axis=0)
        scale = lax.rsqrt(jnp.mean(x * x, axis=-1, keepdims=True) + EPSILON)
        nrm_s[kv * 16 : (kv + 1) * 16, :] = (x * scale * gain).astype(bf16)
    normed = nrm_s[...]

    def rounded(v):
        return v.astype(bf16).astype(f32)

    for copy in copies[1:5]:
        copy.wait()
    rows_s[0] = dot(normed, step_ref[...], NT)
    fixed = rounded(dot(normed, wall_ref[...], NT))
    rows_s[1] = fixed[:, 0:128]
    rows_s[2] = fixed[:, 128:256]
    rows_s[3] = rounded(dot(normed, inner_ref[...]))
    rows_s[4] = rounded(dot(normed, gate_ref[...]))

    def at_time(t, k):
        return rows_s[k, pl.ds(t, 64, stride=4), :]

    def conv_new(new, parts, taps):
        out = []
        for i in range(4):
            v = taps[3] * new[i]
            for d in range(1, i + 1):
                v = v + taps[3 - d] * new[i - d]
            out.append(silu(v if i == 3 else v + parts[i]))
        return out

    def taps_of(first):
        return [vec_ref[first + k : first + k + 1, :] for k in range(4)]

    write = [at_time(t, 1) for t in range(4)]
    read = [at_time(t, 2) for t in range(4)]
    write = [rounded(v) for v in conv_new(write, [hwr_ref[i, 0:64] for i in range(3)], taps_of(4))]
    read = [
        rounded(v) for v in conv_new(read, [hwr_ref[i, 64:128] for i in range(3)], taps_of(8))
    ]
    for t in range(4):
        read_s[pl.ds(t, 64, stride=4), :] = read[t]
    copies[5].wait()
    quarter = lax.broadcasted_iota(jnp.int32, (16, 128), 0) >> 2
    for g in range(16):
        r = read_s[g * 16 : (g + 1) * 16, :].astype(bf16)
        st = low_ref[g * 4 : (g + 1) * 4].reshape(512, 128)
        full = dot(r, st, NT)
        v = full[:, 0:128]
        for q in range(1, 4):
            v = jnp.where(quarter == q, full[:, q * 128 : (q + 1) * 128], v)
        car_s[g * 16 : (g + 1) * 16, :] = v

    inner = conv_new([at_time(t, 3) for t in range(4)], [hin_ref[i] for i in range(3)], taps_of(0))
    rate = vec_ref[12:13, :]
    skip = vec_ref[13:14, :]
    bias = vec_ref[14:15, :]
    out_gain = vec_ref[15:16, :]
    steps = []
    for t in range(4):
        z = at_time(t, 0) + bias
        steps.append(jnp.maximum(z, 0.0) + jnp.log1p(jnp.exp(-jnp.abs(z))))
    sums = [rate * steps[0]]
    for t in range(1, 4):
        sums.append(sums[-1] + rate * steps[t])
    tot = tot_ref[...]
    moved = [steps[t] * inner[t] for t in range(4)]
    for i in range(4):
        state = tot * car_s[pl.ds(i, 64, stride=4), :]
        for t in range(4):
            state = state + a_ref[t] * jnp.sum(read[i] * b_ref[t], axis=-1, keepdims=True)
        y = jnp.exp(sums[i]) * state + skip * inner[i]
        for j in range(i + 1):
            score = jnp.sum(read[i] * write[j], axis=-1, keepdims=True)
            weight = score * jnp.exp(sums[i] - sums[j]) if j < i else score
            y = y + weight * moved[j]
        read_s[pl.ds(i, 64, stride=4), :] = y * silu(at_time(i, 4))

    def piece(kv, c):
        at = pl.multiple_of(kv * 16 + c * 8, 8)
        return read_s[pl.ds(at, 8), :]

    lane = lax.broadcasted_iota(jnp.int32, (16, 128), 1)
    for c, ref in ((core, keep_ref), (1 - core, give_ref)):
        for k in range(8):
            g = jnp.concatenate([piece(2 * k, c), piece(2 * k + 1, c)], axis=0)
            sq = jnp.sum(g * g, axis=-1, keepdims=True)
            hi = rounded(sq)
            ref[k * 16 : (k + 1) * 16, 0:128] = (g * out_gain).astype(bf16)
            ref[k * 16 : (k + 1) * 16, 128:256] = jnp.where(
                lane == 0, hi, jnp.where(lane == 1, sq - hi, 0.0)
            ).astype(bf16)
    copies[6].wait()


def out_kernel(keep_ref, got_ref, own_ref, other_ref, out_ref):
    value = dot(keep_ref[:, 0:128], own_ref[...]) + dot(got_ref[:, 0:128], other_ref[...])
    out_ref[:, 0:2048] = value.astype(bf16)
    both = keep_ref[:, 128:256].astype(f32) + got_ref[:, 128:256].astype(f32)
    sq = jnp.sum(both, axis=-1, keepdims=True)
    hi = sq.astype(bf16).astype(f32)
    lane = lax.broadcasted_iota(jnp.int32, (128, 128), 1)
    out_ref[:, 2048:2176] = jnp.where(lane == 0, hi, jnp.where(lane == 1, sq - hi, 0.0)).astype(bf16)


def sum_kernel(in_ref, out_ref):
    total = in_ref[0].astype(f32)
    for k in range(1, 16):
        total = total + in_ref[k].astype(f32)
    squares = jnp.sum(total[:, 2048:2176], axis=-1, keepdims=True)
    out_ref[...] = (total[:, 0:2048] * lax.rsqrt(squares / INNER + EPSILON)).astype(bf16)


def whole(memory_space=pltpu.VMEM):
    return pl.BlockSpec(memory_space=memory_space)


def swapped(value, axis):
    return lax.ppermute(value, axis, [(k, k ^ 1) for k in range(lax.axis_size(axis))])


def params(mib, **kw):
    return pltpu.CompilerParams(vmem_limit_bytes=mib << 20, **kw)


def body(
    tokens,
    norm_gain,
    gate_proj,
    inner_proj,
    write_proj,
    read_proj,
    step_proj,
    step_bias,
    decay_log,
    skip_gain,
    conv_inner,
    conv_write,
    conv_read,
    out_gain,
    out_proj,
    saved_state,
    inner_history,
    write_history,
    read_history,
    last_steps,
    accepted,
):
    def hbm(value):
        return pltpu.with_memory_space_constraint(value, pltpu.HBM)

    anywhere = whole(pl.ANY)
    dma = pltpu.SemaphoreType.DMA

    def shape(*dims, kind=f32):
        return jax.ShapeDtypeStruct(dims, kind)

    saved = saved_state.reshape(64, 128, 128)
    sent, pack = pl.pallas_call(
        begin_kernel,
        out_shape=[shape(16, 8, 2048, kind=bf16), shape(80, 2048, kind=bf16)],
        in_specs=[anywhere] * 5,
        out_specs=[whole()] * 2,
        scratch_shapes=[
            pltpu.VMEM((8, 2048), bf16),
            pltpu.VMEM((7, 32, 64), bf16),
            pltpu.VMEM((7, 32, 64), bf16),
            dma((5,)),
        ],
        compiler_params=params(4),
        name="begin",
    )(
        hbm(tokens),
        hbm(write_proj.T),
        hbm(read_proj.T),
        hbm(write_history.transpose(1, 2, 0)),
        hbm(read_history.transpose(1, 2, 0)),
    )
    mine = lax.all_to_all(sent, "kv", 0, 0, tiled=True)
    pack_kv = swapped(pack, "kv")
    pack_tp = swapped(pack, "tp")
    pack_both = swapped(pack_kv, "tp")
    out_other = swapped(out_proj, "tp")

    low, hin, a, tot, acc, step, vec = pl.pallas_call(
        prep_kernel,
        in_specs=[anywhere] * 12,
        out_specs=[anywhere] + [whole()] * 4 + [anywhere, whole()],
        out_shape=[
            pltpu.HBM((64, 128, 128), bf16),
            shape(3, 64, 128),
            shape(4, 64, 128),
            shape(64, 128),
            shape(64, 128),
            pltpu.HBM((128, 2048), bf16),
            shape(16, 128),
        ],
        scratch_shapes=[
            pltpu.VMEM((64, 128, 128), bf16),
            pltpu.VMEM((128, 2048), bf16),
            pltpu.VMEM((64, 128, 128), f32),
            pltpu.VMEM((7, 64, 128), bf16),
            pltpu.VMEM((4, 128), bf16),
            pltpu.VMEM((4, 128), bf16),
            pltpu.VMEM((4, 128), bf16),
            pltpu.VMEM((1, 128), f32),
            pltpu.VMEM((4, 2, 64), f32),
            pltpu.VMEM((1, 64), jnp.int32),
            pltpu.VMEM((3, 64), f32),
            pltpu.VMEM((64, 2048), bf16),
            dma((19,)),
            dma((9,)),
        ],
        compiler_params=params(12),
        name="prep",
    )(
        *[
            hbm(v)
            for v in (
                saved,
                inner_history.transpose(1, 0, 2),
                conv_inner,
                conv_write,
                conv_read,
                out_gain[None, :],
                last_steps.transpose(1, 2, 0),
                accepted[None, :],
                decay_log[None, :],
                skip_gain[None, :],
                step_bias[None, :],
                step_proj.T,
            )
        ]
    )
    wall, hwr, b = pl.pallas_call(
        group_kernel,
        in_specs=[whole()] * 6,
        out_specs=[anywhere] + [whole()] * 2,
        out_shape=[pltpu.HBM((256, 2048), bf16), shape(3, 128, 128), shape(4, 64, 128)],
        scratch_shapes=[pltpu.VMEM((256, 2048), bf16), pltpu.VMEM((7, 128, 128), f32), dma((1,))],
        compiler_params=params(6),
        name="group",
    )(pack, pack_tp, pack_kv, pack_both, acc, vec)

    other = swapped(mine, "tp")
    keep, give, own_proj = pl.pallas_call(
        main_kernel,
        in_specs=[whole()] * 2 + [anywhere] * 7 + [whole()] * 6,
        out_specs=[whole()] * 3,
        out_shape=[shape(128, 256, kind=bf16)] * 2 + [shape(128, 2048, kind=bf16)],
        scratch_shapes=[
            pltpu.VMEM((1, 2048), f32),
            pltpu.VMEM((2048, 128), bf16),
            pltpu.VMEM((2048, 128), bf16),
            pltpu.VMEM((128, 2048), bf16),
            pltpu.VMEM((256, 2048), bf16),
            pltpu.VMEM((64, 128, 128), bf16),
            pltpu.VMEM((256, 2048), bf16),
            pltpu.VMEM((5, 256, 128), f32),
            pltpu.VMEM((256, 128), f32),
            pltpu.VMEM((256, 128), f32),
            dma((7,)),
        ],
        compiler_params=params(20),
        name="main",
    )(
        mine,
        other,
        *[
            hbm(v)
            for v in (
                norm_gain[None, :],
                gate_proj,
                inner_proj,
                step,
                wall,
                low,
                out_proj,
            )
        ],
        hin,
        hwr,
        vec,
        a,
        b,
        tot,
    )
    got = swapped(give, "tp")
    partial = pl.pallas_call(
        out_kernel,
        in_specs=[whole()] * 4,
        out_specs=whole(),
        out_shape=shape(128, 2176, kind=bf16),
        compiler_params=params(6),
        name="project",
    )(keep, got, own_proj, out_other)
    arrived = lax.all_to_all(partial.reshape(16, 8, 2176), "kv", 0, 0, tiled=True)
    base = pl.pallas_call(
        state_kernel,
        in_specs=[anywhere] + [whole()] * 3 + [anywhere],
        out_specs=anywhere,
        out_shape=shape(64, 128, 128),
        scratch_shapes=[
            pltpu.VMEM((64, 128, 128), f32),
            pltpu.VMEM((64, 128, 128), f32),
            dma((8,)),
            dma((8,)),
        ],
        compiler_params=params(12),
        name="state",
    )(hbm(saved), a, b, tot, partial)
    mixed = pl.pallas_call(
        sum_kernel,
        in_specs=[whole()],
        out_specs=whole(),
        out_shape=shape(8, 2048, kind=bf16),
        compiler_params=params(4),
        name="total",
    )(arrived)
    return mixed, base.reshape(64, 2, 64, 128)


def solution(mesh):
    both = ("kv", "tp")
    placed = (
        P(("dp", "kv", "tp"), None),
        P(),
        P(None, both),
        P(None, both),
        P(None, both),
        P(None, both),
        P(),
        P(),
        P(),
        P(),
        P(),
        P(),
        P(),
        P(),
        P(both, None),
        P("dp", both, None, None),
        P("dp", None, both),
        P("dp", None, both),
        P("dp", None, both),
        P("dp", None, both),
        P("dp"),
    )
    return jax.shard_map(
        body,
        mesh=mesh,
        in_specs=placed,
        out_specs=(P(("dp", "kv", "tp"), None), P("dp", both, None, None)),
        check_vma=False,
    )
```

time: 78.9 us -> 57.2 us (0.72)
  blocking collectives: 24.4 us -> 0 us
  waiting for transfers between devices: 1.39 us -> 21.5 us
  Pallas kernels: 0 us -> 17 us
  matrix products: 16 us -> 0 us
  local copies, waits for them, and re-layouts: 14.4 us -> 0 us
  other arithmetic: 10 us -> 0 us
  starting transfers between devices: 10.8 us -> 17.7 us
    all_to_all x2 -> x0, blocking collectives: 22.5 us -> none  [summed_on_arrival(): lax.all_to_all(tiles, axis, split_axis=0, concat_axis=0, tiled=True)]
    all_to_all x1 -> x2, waiting for transfers between devices: 1.38 us -> 19 us  [the longest x1 11 us: body(): mine = lax.all_to_all(sent, 'kv', 0, 0, tiled=True)]
    pallas_call x0 -> x7, Pallas kernels: none -> 17 us  [the longest x1 4.34 us: body(): pl.pallas_call(state_kernel, in_specs=[anywhere] + [whole()] * 3 + [anywh...]
    dot_general x10 -> x0, matrix products: 16 us -> none  [the longest x1 5.91 us: body(): jnp.einsum('sth,sthp,stn->shpn', old_weights, inner_old_heads, write_past...]
    gather x7 -> x0, local copies, waits for them, and re-layouts: 7.49 us -> none  [current(): window = jnp.take_along_axis(history, window_rows[:, :, None], axis=1)]
    all_to_all x1 -> x2, starting transfers between devices: 8.45 us -> 14.6 us  [the longest x1 8.17 us: body(): mine = lax.all_to_all(sent, 'kv', 0, 0, tiled=True)]
    convert_element_type x11 -> x0, other arithmetic: 3.94 us -> none  [the longest x1 0.84 us: body(): normed_own = (own_rows * lax.rsqrt(jnp.mean(own_rows * own_rows, axis=-1,...]
    ppermute x2 -> x6, waiting for transfers between devices: 0.01 us -> 2.43 us  [swapped(): lax.ppermute(value, axis, [(k, k ^ 1) for k in range(lax.axis_size(axis))])]
  transfers between devices with their start and end apart: 3 -> 8, of which waited for: 1 -> 4; matrix products, arithmetic and copies ran while one was open for 33% -> 0% of each run, Pallas kernels for 0% -> 23%
where the time goes in v1:
time: 57.2 us; the launch traced here: 56.8 us
  waiting for transfers between devices  21.5 us (38%)
  starting transfers between devices  17.7 us (31%)
  Pallas kernels  17 us (30%)
  between operations  0.72 us (1%)
    all_to_all x1, waiting for transfers between devices, body(): mine = lax.all_to_all(sent, 'kv', 0, 0, tiled=True)  11 us
    all_to_all x1, starting transfers between devices, body(): mine = lax.all_to_all(sent, 'kv', 0, 0, tiled=True)  8.17 us
    all_to_all x1, waiting for transfers between devices, body(): lax.all_to_all(partial.reshape(16, 8, 2176), 'kv', 0, 0, tiled=True)  8.06 us
    all_to_all x1, starting transfers between devices, body(): lax.all_to_all(partial.reshape(16, 8, 2176), 'kv', 0, 0, tiled=True)  6.46 us
    pallas_call x1, Pallas kernels, body(): pl.pallas_call(state_kernel, in_specs=[anywhere] + [whole()] * 3 + [anywh...  4.34 us
    pallas_call x1, Pallas kernels, body(): pl.pallas_call(main_kernel, in_specs=[whole()] * 2 + [anywhere] * 7 + [wh...  3.92 us
    pallas_call x1, Pallas kernels, body(): pl.pallas_call(prep_kernel, in_specs=[anywhere] * 12, out_specs=[anywhere...  3.62 us
    ppermute x6, starting transfers between devices, swapped(): lax.ppermute(value, axis, [(k, k ^ 1) for k in range(lax.axis_size(axis))])  3.03 us
  transfers between devices with their start and end apart: 8, of which 4 were waited for; matrix products, arithmetic and copies ran while one was open for 0% of the time, Pallas kernels for 23%

profile of v1, /device:TPU:0, one launch (start us, length us, event | category | flops | bytes accessed | tf_op | source)
XLA Modules:
  0.0 56.8 jit_solution(3262260900159365218)
XLA Ops:
  0.6 1.9 %begin.1 = (bf16[16,8,2048]{2,1,0:T(8,128)(2,1)}, bf16[80,2048]{1,0:T(8,128)(2,1)S(1)}) custom-call(bf16[8,2048]{1,0:T(8,128)(2,1)} %tok_hbm.1, bf16[32,2048]{1,0:T(8,128)(2,1)} %bitcast.20, bf16[32,2048]{1,0:T(8,128)(2,1)} %bitcast.21, bf16[7,32,64]{2,1,0:T(8,128)(2,1)} %bitcast.23, bf16[7,32,64]{2,1,0:T(8,128)(2,1)} %bitcast.24), custom_call_target="tpu_custom_call" | custom-call | tf_op jit(solution)/shard_map/begin/pallas_call | solution.py:462
  2.5 8.2 %all-to-all-start = ((bf16[16,8,2048]{2,1,0:T(8,128)(2,1)}), bf16[16,8,2048]{2,1,0:T(8,128)(2,1)S(1)}, u32[]{:S(2)}, u32[]{:S(2)}) async-start(bf16[16,8,2048]{2,1,0:T(8,128)(2,1)} %get-tuple-element.17), calls=%async_computation | async-start | bytes 1048576 | tf_op jit(solution)/shard_map/all_to_all | solution.py:482
  10.7 1.9 %collective-permute-start.2 = (bf16[80,2048]{1,0:T(8,128)(2,1)S(1)}, bf16[80,2048]{1,0:T(8,128)(2,1)S(1)}, u32[]{:S(2)}, u32[]{:S(2)}) collective-permute-start(bf16[80,2048]{1,0:T(8,128)(2,1)S(1)} %get-tuple-element.19.p0_ref), channel_id=1, source_target_pairs={{0,2},{2,0},{4,6},{6,4},{8,10},{10,8},{12,14},{14,12},{16,18},{18,... | collective-permute-start | bytes 983048 | tf_op jit(solution)/shard_map/ppermute | solution.py:422
  12.6 11.0 %all-to-all-done.mine_ref = bf16[16,8,2048]{2,1,0:T(8,128)(2,1)S(1)} async-done(((bf16[16,8,2048]{2,1,0:T(8,128)(2,1)}), bf16[16,8,2048]{2,1,0:T(8,128)(2,1)S(1)}, u32[]{:S(2)}, u32[]{:S(2)}) %all-to-all-start) | async-done | bytes 524320 | tf_op jit(solution)/shard_map/all_to_all | solution.py:482
  23.6 0.0 collective-permute-start
  23.6 0.5 collective-permute-start.5
  24.1 0.0 collective-permute-start.1
  24.1 1.5 %collective-permute-done.2.p2_ref = bf16[80,2048]{1,0:T(8,128)(2,1)S(1)} collective-permute-done((bf16[80,2048]{1,0:T(8,128)(2,1)S(1)}, bf16[80,2048]{1,0:T(8,128)(2,1)S(1)}, u32[]{:S(2)}, u32[]{:S(2)}) %collective-permute-start.2) | collective-permute-done | bytes 327712 | tf_op jit(solution)/shard_map/ppermute | solution.py:422
  25.6 0.0 collective-permute-start.3
  25.6 3.6 %prep.1 = (bf16[64,128,128]{2,1,0:T(8,128)(2,1)}, f32[3,64,128]{2,1,0:T(8,128)S(1)}, f32[4,64,128]{2,1,0:T(8,128)S(1)}, f32[64,128]{1,0:T(8,128)S(1)}, f32[64,12...) custom-call(f32[64,128,128]{2,1,0:T(8,128)} %bitcast.16, bf16[7,64,128]{2,1,0:T(8,128)(2,1)} %bitcast.22, ...), custom_call_target="tpu_custom_call" | custom-call | tf_op jit(solution)/shard_map/prep/pallas_call | solution.py:488
  29.3 0.0 collective-permute-done.1.p1_ref
  29.3 0.0 collective-permute-done.3.p3_ref
  29.3 1.3 %group.1 = (bf16[256,2048]{1,0:T(8,128)(2,1)}, f32[3,128,128]{2,1,0:T(8,128)S(1)}, f32[4,64,128]{2,1,0:T(8,128)S(1)}) custom-call(bf16[80,2048]{1,0:T(8,128)(2,1)S(1)} %get-tuple-element.19.p0_ref, bf16[80,2048]{1,0:T(8,128)(2,1)S(1)} %collective-permute-done.1.p1_ref, bf16[80,2048]{1,0:T(8,128)(2,1)S(1)} %collective-permute-done.2.p2_ref, ...), custom_call_target="tpu_custom_call" | custom-call | tf_op jit(solution)/shard_map/group/pallas_call | solution.py:538
  30.6 0.0 collective-permute-done.other_ref
  30.6 3.9 %main.1 = (bf16[128,256]{1,0:T(8,128)(2,1)S(1)}, bf16[128,256]{1,0:T(8,128)(2,1)S(1)}, bf16[128,2048]{1,0:T(8,128)(2,1)S(1)}) custom-call(bf16[16,8,2048]{2,1,0:T(8,128)(2,1)S(1)} %all-to-all-done.mine_ref, bf16[16,8,2048]{2,1,0:T(8,128)(2,1)S(1)} %collective-permute-done.other_ref, f32[1,2048]{1,0:T(1,128)} %bitcast.26, bf16[2048,128]{1,0:T(8,128)(2,1)} %gate_hbm.1, ...), custom_call_target="tpu_custom_call" | custom-call | tf_op jit(solution)/shard_map/main/pallas_call | solution.py:549
  34.5 0.6 %collective-permute-start.4 = (bf16[128,256]{1,0:T(8,128)(2,1)S(1)}, bf16[128,256]{1,0:T(8,128)(2,1)S(1)}, u32[]{:S(2)}, u32[]{:S(2)}) collective-permute-start(bf16[128,256]{1,0:T(8,128)(2,1)S(1)} %get-tuple-element.30), channel_id=1, source_target_pairs={{0,1},{1,0},{2,3},{3,2},{4,5},{5,4},{6,7},{7,6},{8,9},{9,8},{10,11... | collective-permute-start | bytes 196616 | tf_op jit(solution)/shard_map/ppermute | solution.py:422
  35.1 0.0 collective-permute-done.5.other_ref
  35.1 0.9 %collective-permute-done.4.got_ref = bf16[128,256]{1,0:T(8,128)(2,1)S(1)} collective-permute-done((bf16[128,256]{1,0:T(8,128)(2,1)S(1)}, bf16[128,256]{1,0:T(8,128)(2,1)S(1)}, u32[]{:S(2)}, u32[]{:S(2)}) %collective-permute-start.4) | collective-permute-done | bytes 65568 | tf_op jit(solution)/shard_map/ppermute | solution.py:422
  36.0 1.2 %project.1.after_ref = bf16[128,2176]{1,0:T(8,128)(2,1)} custom-call(bf16[128,256]{1,0:T(8,128)(2,1)S(1)} %get-tuple-element.29.keep_ref, bf16[128,256]{1,0:T(8,128)(2,1)S(1)} %collective-permute-done.4.got_ref, bf16[128,2048]{1,0:T(8,128)(2,1)S(1)} %get-tuple-element.31.own_ref, bf16[128,2048]{1,0:T(8,128)(2,1)S(1)} %collective-permute-done.5.other_ref), custom_call_target="tpu_custom_call" | custom-call | tf_op jit(solution)/shard_map/project/pallas_call | solution.py:592
  37.2 6.5 %all-to-all-start.1 = ((bf16[16,8,2176]{2,1,0:T(8,128)(2,1)}), bf16[16,8,2176]{2,1,0:T(8,128)(2,1)S(1)}, u32[]{:S(2)}, u32[]{:S(2)}) async-start(bf16[16,8,2176]{2,1,0:T(8,128)(2,1)} %bitcast.14), calls=%async_computation.1 | async-start | bytes 1114112 | tf_op jit(solution)/shard_map/all_to_all | solution.py:600
  43.7 4.3 %state.1 = f32[64,128,128]{2,1,0:T(8,128)} custom-call(f32[64,128,128]{2,1,0:T(8,128)} %bitcast.17, f32[4,64,128]{2,1,0:T(8,128)S(1)} %get-tuple-element.26.a_ref, f32[4,64,128]{2,1,0:T(8,128)S(1)} %get-tuple-element.27.b_ref, f32[64,128]{1,0:T(8,128)S(1)} %get-tuple-element.28.tot_ref, bf16[128,2176]{1,0:T(8,128)(2,1)} %project.1.after_ref), custom_call_target="tpu_custom_call" | custom-call | tf_op jit(solution)/shard_map/state/pallas_call | solution.py:601
  48.0 8.1 %all-to-all-done.1.in_ref = bf16[16,8,2176]{2,1,0:T(8,128)(2,1)S(1)} async-done(((bf16[16,8,2176]{2,1,0:T(8,128)(2,1)}), bf16[16,8,2176]{2,1,0:T(8,128)(2,1)S(1)}, u32[]{:S(2)}, u32[]{:S(2)}) %all-to-all-start.1) | async-done | bytes 557088 | tf_op jit(solution)/shard_map/all_to_all | solution.py:600
  56.1 0.7 %total.1 = bf16[8,2048]{1,0:T(8,128)(2,1)} custom-call(bf16[16,8,2176]{2,1,0:T(8,128)(2,1)S(1)} %all-to-all-done.1.in_ref), custom_call_target="tpu_custom_call" | custom-call | tf_op jit(solution)/shard_map/total/pallas_call | solution.py:615
Async XLA Ops:
  2.5 21.1 %all-to-all-start = ((bf16[16,8,2048]{2,1,0:T(8,128)(2,1)}), bf16[16,8,2048]{2,1,0:T(8,128)(2,1)S(1)}, u32[]{:S(2)}, u32[]{:S(2)}) async-start(bf16[16,8,2048]{2,1,0:T(8,128)(2,1)} %get-tuple-element.17), calls=%async_computation | async-start | bytes 1048576 | tf_op jit(solution)/shard_map/all_to_all | solution.py:482
  10.7 14.9 %collective-permute-start.2 = (bf16[80,2048]{1,0:T(8,128)(2,1)S(1)}, bf16[80,2048]{1,0:T(8,128)(2,1)S(1)}, u32[]{:S(2)}, u32[]{:S(2)}) collective-permute-start(bf16[80,2048]{1,0:T(8,128)(2,1)S(1)} %get-tuple-element.19.p0_ref), channel_id=1, source_target_pairs={{0,2},{2,0},{4,6},{6,4},{8,10},{10,8},{12,14},{14,12},{16,18},{18,... | collective-permute-start | bytes 983048 | tf_op jit(solution)/shard_map/ppermute | solution.py:422
  23.6 7.0 %collective-permute-start = (bf16[16,8,2048]{2,1,0:T(8,128)(2,1)S(1)}, bf16[16,8,2048]{2,1,0:T(8,128)(2,1)S(1)}, u32[]{:S(2)}, u32[]{:S(2)}) collective-permute-start(bf16[16,8,2048]{2,1,0:T(8,128)(2,1)S(1)} %all-to-all-done.mine_ref), channel_id=1, source_target_pairs={{0,1},{1,0},{2,3},{3,2},{4,5},{5,4},{6,7},{7,6},{8,9},{9,8},{10,11... | collective-permute-start | bytes 1572872 | tf_op jit(solution)/shard_map/ppermute | solution.py:422
  23.6 11.5 %collective-permute-start.5 = (bf16[128,2048]{1,0:T(8,128)(2,1)}, bf16[128,2048]{1,0:T(8,128)(2,1)S(1)}, u32[]{:S(2)}, u32[]{:S(2)}) collective-permute-start(bf16[128,2048]{1,0:T(8,128)(2,1)} %own_hbm.1), channel_id=1, source_target_pairs={{0,1},{1,0},{2,3},{3,2},{4,5},{5,4},{6,7},{7,6},{8,9},{9,8},{10,11... | collective-permute-start | bytes 1572872 | tf_op jit(solution)/shard_map/ppermute | solution.py:422
  24.1 5.2 %collective-permute-start.1 = (bf16[80,2048]{1,0:T(8,128)(2,1)S(1)}, bf16[80,2048]{1,0:T(8,128)(2,1)S(1)}, u32[]{:S(2)}, u32[]{:S(2)}) collective-permute-start(bf16[80,2048]{1,0:T(8,128)(2,1)S(1)} %get-tuple-element.19.p0_ref), channel_id=1, source_target_pairs={{0,1},{1,0},{2,3},{3,2},{4,5},{5,4},{6,7},{7,6},{8,9},{9,8},{10,11... | collective-permute-start | bytes 983048 | tf_op jit(solution)/shard_map/ppermute | solution.py:422
  25.6 3.6 %collective-permute-start.3 = (bf16[80,2048]{1,0:T(8,128)(2,1)S(1)}, bf16[80,2048]{1,0:T(8,128)(2,1)S(1)}, u32[]{:S(2)}, u32[]{:S(2)}) collective-permute-start(bf16[80,2048]{1,0:T(8,128)(2,1)S(1)} %collective-permute-done.2.p2_ref), channel_id=1, source_target_pairs={{0,1},{1,0},{2,3},{3,2},{4,5},{5,4},{6,7},{7,6},{8,9},{9,8},{10,11... | collective-permute-start | bytes 983048 | tf_op jit(solution)/shard_map/ppermute | solution.py:422
  34.5 1.5 %collective-permute-start.4 = (bf16[128,256]{1,0:T(8,128)(2,1)S(1)}, bf16[128,256]{1,0:T(8,128)(2,1)S(1)}, u32[]{:S(2)}, u32[]{:S(2)}) collective-permute-start(bf16[128,256]{1,0:T(8,128)(2,1)S(1)} %get-tuple-element.30), channel_id=1, source_target_pairs={{0,1},{1,0},{2,3},{3,2},{4,5},{5,4},{6,7},{7,6},{8,9},{9,8},{10,11... | collective-permute-start | bytes 196616 | tf_op jit(solution)/shard_map/ppermute | solution.py:422
  37.2 18.9 %all-to-all-start.1 = ((bf16[16,8,2176]{2,1,0:T(8,128)(2,1)}), bf16[16,8,2176]{2,1,0:T(8,128)(2,1)S(1)}, u32[]{:S(2)}, u32[]{:S(2)}) async-start(bf16[16,8,2176]{2,1,0:T(8,128)(2,1)} %bitcast.14), calls=%async_computation.1 | async-start | bytes 1114112 | tf_op jit(solution)/shard_map/all_to_all | solution.py:600

commit v2 on v1

v2 whole, which is shorter than its diff:
```python
import jax
import jax.numpy as jnp
from jax import lax
from jax.experimental import pallas as pl
from jax.experimental.pallas import tpu as pltpu
from jax.sharding import PartitionSpec as P


EPSILON = 0.1
INNER = 4096
f32 = jnp.float32
bf16 = jnp.bfloat16
NT = (((1,), (1,)), ((), ()))
NN = (((1,), (0,)), ((), ()))


def dot(a, b, dims=NN):
    return lax.dot_general(a, b, dims, preferred_element_type=f32)


def silu(x):
    return x * (1.0 / (1.0 + jnp.exp(-x)))


def fetch(pairs, sems):
    copies = [pltpu.make_async_copy(src, dst, sems.at[k]) for k, (src, dst) in enumerate(pairs)]
    for copy in copies:
        copy.start()
    return copies


def device_rank():
    return lax.axis_index("kv") * 2 + lax.axis_index("tp")


def begin_kernel(
    tok_hbm, w_hbm, r_hbm, wh_hbm, rh_hbm, all_hbm, out_ref, tok_s, wh_s, rh_s, sems, sent
):
    copies = fetch(
        (
            (tok_hbm, tok_s),
            (wh_hbm, wh_s),
            (rh_hbm, rh_s),
            (w_hbm, out_ref.at[0:32]),
            (r_hbm, out_ref.at[32:64]),
        ),
        sems,
    )
    copies[0].wait()
    out = fetch([(tok_s, all_hbm.at[k]) for k in range(16)], sent)
    copies[1].wait()
    copies[2].wait()
    for t in range(7):
        both = jnp.concatenate([wh_s[t].astype(f32), rh_s[t].astype(f32)], axis=1).astype(bf16)
        out_ref[64:80, t * 128 : (t + 1) * 128] = both[0:16]
        out_ref[64:80, (7 + t) * 128 : (8 + t) * 128] = both[16:32]
    out_ref[64:80, 1792:2048] = jnp.zeros((16, 256), bf16)
    for copy in copies[3:] + out:
        copy.wait()


def windows(rows, acc):
    out = []
    for j in range(3):
        w = rows[j]
        for a in range(1, 5):
            w = jnp.where(acc == a, rows[a + j], w)
        out.append(w)
    return out


def old_parts(taps, w):
    return (
        taps[0] * w[0] + taps[1] * w[1] + taps[2] * w[2],
        taps[0] * w[1] + taps[1] * w[2],
        taps[0] * w[2],
    )


def prep_kernel(
    saved_hbm,
    ihist_hbm,
    tin_hbm,
    tw_hbm,
    tr_hbm,
    gain_hbm,
    ls_hbm,
    acc_hbm,
    decay_hbm,
    skip_hbm,
    bias_hbm,
    step_hbm,
    keep_hbm,
    give_hbm,
    held_hbm,
    wide_hbm,
    acc_ref,
    vec_ref,
    sent_ref,
    held_s,
    low_s,
    wide_s,
    saved_s,
    ihist_s,
    tin_s,
    twin_s,
    tw_s,
    tr_s,
    gain_s,
    twin_gain_s,
    ls_s,
    acc_s,
    heads_s,
    step_s,
    sems,
    sent,
):
    rank = device_rank()
    core = rank & 1
    head = rank * 2
    col = pl.multiple_of(rank * 128, 128)
    twin_col = pl.multiple_of((rank ^ 1) * 128, 128)
    group = pl.multiple_of((rank >> 2) * 128, 128)
    small = (
        (acc_hbm, acc_s),
        (ls_hbm, ls_s),
        (decay_hbm, heads_s.at[0:1]),
        (skip_hbm, heads_s.at[1:2]),
        (bias_hbm, heads_s.at[2:3]),
        (tin_hbm.at[:, pl.ds(col, 128)], tin_s),
        (tin_hbm.at[:, pl.ds(twin_col, 128)], twin_s),
        (tw_hbm.at[:, pl.ds(group, 128)], tw_s),
        (tr_hbm.at[:, pl.ds(group, 128)], tr_s),
        (gain_hbm.at[:, pl.ds(col, 128)], gain_s),
        (gain_hbm.at[:, pl.ds(twin_col, 128)], twin_gain_s),
        (ihist_hbm, ihist_s),
        (step_hbm, step_s),
    )
    big = tuple(
        (saved_hbm.at[pl.ds(kv * 4 + c * 2, 2)], saved_s.at[p * 32 + kv * 2 : p * 32 + kv * 2 + 2])
        for p, c in enumerate((1 - core, core))
        for kv in range(16)
    )
    copies = fetch(small + big, sems)
    for copy in copies[: len(small)]:
        copy.wait()

    tin = tin_s[...].astype(f32)
    vec_ref[0:4, :] = tin
    vec_ref[4:8, :] = tw_s[...].astype(f32)
    vec_ref[8:12, :] = tr_s[...].astype(f32)
    place = lax.broadcasted_iota(jnp.int32, (1, 64), 1)
    first = lax.broadcasted_iota(jnp.int32, (1, 128), 1) < 64

    twin_head = (rank ^ 1) * 2

    def of_head(k, h):
        return jnp.sum(jnp.where(place == h, heads_s[k : k + 1], 0.0), axis=-1, keepdims=True)

    def spread(k, h):
        return jnp.where(first, of_head(k, h), of_head(k, h + 1))

    vec_ref[12:13, :] = -jnp.exp(spread(0, head))
    vec_ref[13:14, :] = spread(1, head)
    vec_ref[14:15, :] = spread(2, head)
    vec_ref[15:16, :] = gain_s[...]
    vec_ref[16:20, :] = twin_s[...].astype(f32)
    vec_ref[20:21, :] = -jnp.exp(spread(0, twin_head))
    vec_ref[21:22, :] = spread(1, twin_head)
    vec_ref[22:23, :] = spread(2, twin_head)
    vec_ref[23:24, :] = twin_gain_s[...]

    acc_row = acc_s[...]
    acc = jnp.broadcast_to(acc_row.astype(f32), (128, 64)).T
    acc_ref[...] = acc
    rows = [ihist_s[t].astype(f32) for t in range(7)]
    taps = [tin[k : k + 1] for k in range(4)]
    for i, part in enumerate(old_parts(taps, windows(rows, acc))):
        held_s[4 + i] = part

    def wide(pair):
        return jnp.concatenate([jnp.broadcast_to(v, (64, 64)) for v in pair], axis=0).T

    weights = [[], [], [], []]
    totals = []
    for h in range(2):
        rate = -jnp.exp(of_head(0, head + h))
        steps = [ls_s[t, h : h + 1, :] for t in range(4)]
        keep = [(acc_row > t).astype(f32) for t in range(4)]
        logs = [rate * steps[t] * keep[t] for t in range(4)]
        tail = jnp.zeros((1, 64), f32)
        for t in (3, 2, 1, 0):
            weights[t].append(keep[t] * jnp.exp(tail) * steps[t])
            tail = tail + logs[t]
        totals.append(jnp.exp(tail))
    held_s[7] = wide(totals)
    for t in range(4):
        held_s[t] = silu(sum(taps[k] * rows[t + k] for k in range(4))) * wide(weights[t])

    for q in range(2):
        start = (1 - core) * 2 + q
        block = slice(q * 16, (q + 1) * 16)
        for t in range(8):
            sent_ref[t, block] = held_s[t, pl.ds(start, 16, stride=4), :]
    held = pltpu.make_async_copy(held_s, held_hbm, sent.at[9])
    held.start()

    row = lax.broadcasted_iota(jnp.int32, (256, 64), 0)
    base = jnp.where(row < 128, head, twin_head)
    pick = lax.broadcasted_iota(jnp.int32, (256, 64), 1) == base + ((row >> 6) & 1)
    wide_s[...] = dot(pick.astype(f32).astype(bf16), step_s[...]).astype(bf16)
    out = [pltpu.make_async_copy(wide_s, wide_hbm, sent.at[8])]
    out[0].start()
    out.append(held)
    for k in range(8):
        block = slice(k * 8, (k + 1) * 8)
        for copy in copies[len(small) + k * 4 : len(small) + k * 4 + 4]:
            copy.wait()
        low_s[block] = saved_s[block].astype(bf16)
        dest = (give_hbm if k < 4 else keep_hbm).at[slice((k % 4) * 8, (k % 4 + 1) * 8)]
        out.append(pltpu.make_async_copy(low_s.at[block], dest, sent.at[k]))
        out[-1].start()
    for copy in out:
        copy.wait()


def group_kernel(p0_ref, p1_ref, p2_ref, p3_ref, acc_ref, vec_ref, wall_hbm, mix_hbm, wall_s, mix_s, hist_s, sems):
    member = device_rank() & 3
    for x, p in enumerate((p0_ref, p1_ref, p2_ref, p3_ref)):
        at = pl.multiple_of((member ^ x) * 32, 32)
        wall_s[pl.ds(at, 32), :] = p[0:32, :]
        wall_s[pl.ds(128 + at, 32), :] = p[32:64, :]
        for t in range(7):
            hist_s[t, pl.ds(at, 16), :] = p[64:80, t * 128 : (t + 1) * 128].astype(f32)
            hist_s[t, pl.ds(at + 16, 16), :] = p[64:80, (7 + t) * 128 : (8 + t) * 128].astype(f32)
    copy = pltpu.make_async_copy(wall_s, wall_hbm, sems.at[0])
    copy.start()
    both = [hist_s[t].T for t in range(7)]
    acc = acc_ref[...]
    acc2 = jnp.concatenate([acc, acc], axis=0)
    taps = [
        jnp.concatenate(
            [
                jnp.broadcast_to(vec_ref[4 + k : 5 + k, :], (64, 128)),
                jnp.broadcast_to(vec_ref[8 + k : 9 + k, :], (64, 128)),
            ],
            axis=0,
        )
        for k in range(4)
    ]
    for i, part in enumerate(old_parts(taps, windows(both, acc2))):
        mix_s[i] = part[0:64]
        mix_s[3 + i] = part[64:128]
    for t in range(4):
        w_old = silu(sum(vec_ref[4 + k : 5 + k, :] * both[t + k][0:64] for k in range(4)))
        mix_s[6 + t] = w_old.astype(bf16).astype(f32)
    last = pltpu.make_async_copy(mix_s, mix_hbm, sems.at[1])
    last.start()
    copy.wait()
    last.wait()


def state_kernel(
    saved_hbm, held_hbm, mix_hbm, after_hbm, base_hbm, saved_s, base_s, held_s, mix_s, sems, sent
):
    blocks = [slice(k * 8, (k + 1) * 8) for k in range(8)]
    copies = fetch(
        [(saved_hbm.at[k], saved_s.at[k]) for k in blocks]
        + [(held_hbm, held_s), (mix_hbm.at[6:10], mix_s)],
        sems,
    )
    copies[8].wait()
    copies[9].wait()
    tot = jnp.concatenate([held_s[7], held_s[7]], axis=0).T
    at = jnp.concatenate(
        [jnp.concatenate([held_s[2 * p], held_s[2 * p + 1]], axis=0).T for p in range(2)], axis=1
    ).astype(bf16)
    b = mix_s[...].reshape(256, 128).astype(bf16)
    lane = lax.broadcasted_iota(jnp.int32, (1, 256), 1) & 63
    out = []
    for k in range(8):
        copies[k].wait()
        for s in range(k * 8, (k + 1) * 8):
            mask = (lane == s).astype(f32).astype(bf16)
            base_s[s] = saved_s[s] * tot[:, s : s + 1] + dot(at * mask, b)
        copy = pltpu.make_async_copy(base_s.at[blocks[k]], base_hbm.at[blocks[k]], sent.at[k])
        copy.start()
        out.append(copy)
    for copy in out:
        copy.wait()


def rounded(v):
    return v.astype(bf16).astype(f32)


def main_kernel(
    mine_ref,
    norm_hbm,
    wall_hbm,
    step_hbm,
    inner_hbm,
    gate_hbm,
    held_hbm,
    mix_hbm,
    low_hbm,
    twin_low_hbm,
    own_hbm,
    twin_own_ref,
    twin_inner_ref,
    twin_gate_ref,
    got_ref,
    vec_ref,
    out_hbm,
    norm_s,
    wall_s,
    step_s,
    inner_s,
    gate_s,
    mix_s,
    held_s,
    low_s,
    proj_s,
    nrm_s,
    rows_s,
    read_s,
    car_s,
    out_s,
    sems,
    sent,
):
    copies = fetch(
        (
            (norm_hbm, norm_s),
            (wall_hbm, wall_s),
            (step_hbm, step_s),
            (inner_hbm, inner_s),
            (gate_hbm, gate_s),
            (mix_hbm, mix_s),
            (held_hbm, held_s),
            (low_hbm, low_s.at[0]),
            (twin_low_hbm, low_s.at[1]),
            (own_hbm, proj_s),
        ),
        sems,
    )
    core = lax.axis_index("tp")
    copies[0].wait()
    gain = norm_s[...]
    for k in range(8):
        x = mine_ref[2 * k : 2 * k + 2].astype(f32).reshape(16, 2048)
        scale = lax.rsqrt(jnp.mean(x * x, axis=-1, keepdims=True) + EPSILON)
        nrm_s[k * 16 : (k + 1) * 16, :] = (x * scale * gain).astype(bf16)
    normed = nrm_s[...]
    copies[1].wait()
    both = rounded(dot(normed, wall_s[...], NT))
    rows_s[2] = both[:, 0:128]
    rows_s[3] = both[:, 128:256]
    copies[2].wait()
    both = dot(normed, step_s[...], NT)
    rows_s[0] = both[:, 0:128]
    rows_s[1] = both[:, 128:256]
    rows_s[5] = rounded(dot(normed, twin_inner_ref[...]))
    rows_s[7] = rounded(dot(normed, twin_gate_ref[...]))
    copies[3].wait()
    rows_s[4] = rounded(dot(normed, inner_s[...]))
    copies[4].wait()
    rows_s[6] = rounded(dot(normed, gate_s[...]))

    def at_time(ref, t, k):
        return jnp.concatenate([ref[k, pl.ds(q * 4 + t, 16, stride=8), :] for q in range(2)], axis=0)

    def put(ref, t, k, value):
        for q in range(2):
            ref[k, pl.ds(q * 4 + t, 16, stride=8), :] = value[q * 16 : (q + 1) * 16]

    def chosen(ref, k):
        return jnp.concatenate(
            [ref[k, pl.ds(core * 2 + q, 16, stride=4), :] for q in range(2)], axis=0
        )

    def conv_new(new, parts, taps):
        out = []
        for i in range(4):
            v = taps[3] * new[i]
            for d in range(1, i + 1):
                v = v + taps[3 - d] * new[i - d]
            out.append(silu(v if i == 3 else v + parts[i]))
        return out

    def taps_of(first):
        return [vec_ref[first + k : first + k + 1, :] for k in range(4)]

    def mixing(k, base, taps):
        new = [at_time(rows_s, t, k) for t in range(4)]
        return [rounded(v) for v in conv_new(new, [chosen(mix_s, base + i) for i in range(3)], taps)]

    copies[5].wait()
    write = mixing(2, 0, taps_of(4))
    read = mixing(3, 3, taps_of(8))
    for t in range(4):
        put(read_s, t, 0, read[t])
    quarter = lax.broadcasted_iota(jnp.int32, (16, 128), 0) >> 2
    copies[7].wait()
    copies[8].wait()
    for g in range(8):
        r = read_s[0, g * 16 : (g + 1) * 16, :].astype(bf16)
        for p in range(2):
            full = dot(r, low_s[p, g * 4 : (g + 1) * 4].reshape(512, 128), NT)
            v = full[:, 0:128]
            for q in range(1, 4):
                v = jnp.where(quarter == q, full[:, q * 128 : (q + 1) * 128], v)
            car_s[p, g * 16 : (g + 1) * 16, :] = v

    def score(x, y):
        return jnp.sum(x * y, axis=-1, keepdims=True)

    scores = [[score(read[i], write[j]) for j in range(i + 1)] for i in range(4)]
    past = [chosen(mix_s, 6 + t) for t in range(4)]
    copies[6].wait()
    olds = [[score(read[i], past[t]) for t in range(4)] for i in range(4)]
    for p in range(2):
        if p == 0:
            held = [chosen(held_s, t) for t in range(4)]
            parts = [chosen(held_s, 4 + t) for t in range(3)]
            tot = chosen(held_s, 7)
        else:
            held = [got_ref[t] for t in range(4)]
            parts = [got_ref[4 + t] for t in range(3)]
            tot = got_ref[7]
        inner = conv_new(
            [at_time(rows_s, t, 4 + p) for t in range(4)], parts, taps_of(16 if p else 0)
        )
        first = 20 if p else 12
        rate, skip, bias = (vec_ref[first + k : first + k + 1, :] for k in range(3))
        steps = []
        for t in range(4):
            z = at_time(rows_s, t, p) + bias
            steps.append(jnp.maximum(z, 0.0) + jnp.log1p(jnp.exp(-jnp.abs(z))))
        sums = [rate * steps[0]]
        for t in range(1, 4):
            sums.append(sums[-1] + rate * steps[t])
        moved = [steps[t] * inner[t] for t in range(4)]
        for i in range(4):
            state = tot * at_time(car_s, i, p)
            for t in range(4):
                state = state + held[t] * olds[i][t]
            y = jnp.exp(sums[i]) * state + skip * inner[i] + scores[i][i] * moved[i]
            for j in range(i):
                y = y + scores[i][j] * jnp.exp(sums[i] - sums[j]) * moved[j]
            put(read_s, i, p, y * silu(at_time(rows_s, i, 6 + p)))

    lane = lax.broadcasted_iota(jnp.int32, (128, 128), 1)
    gated = [read_s[p] for p in range(2)]
    sq = jnp.sum(gated[0] * gated[0] + gated[1] * gated[1], axis=-1, keepdims=True)
    hi = rounded(sq)
    out_s[:, 2048:2176] = jnp.where(lane == 0, hi, jnp.where(lane == 1, sq - hi, 0.0)).astype(bf16)
    unscaled = [
        (gated[p] * vec_ref[15 + 8 * p : 16 + 8 * p, :]).astype(bf16) for p in range(2)
    ]
    copies[9].wait()
    out = []
    for k in range(4):
        cols = slice(k * 512, (k + 1) * 512)
        value = dot(unscaled[0], proj_s[:, cols]) + dot(unscaled[1], twin_own_ref[:, cols])
        out_s[:, cols] = value.astype(bf16)
        cols = slice(k * 512, 2176 if k == 3 else (k + 1) * 512)
        out.append(pltpu.make_async_copy(out_s.at[:, cols], out_hbm.at[:, cols], sent.at[k]))
        out[-1].start()
    for copy in out:
        copy.wait()


def sum_kernel(in_ref, out_ref):
    total = in_ref[0].astype(f32)
    for k in range(1, 16):
        total = total + in_ref[k].astype(f32)
    squares = jnp.sum(total[:, 2048:2176], axis=-1, keepdims=True)
    out_ref[...] = (total[:, 0:2048] * lax.rsqrt(squares / INNER + EPSILON)).astype(bf16)


def whole(memory_space=pltpu.VMEM):
    return pl.BlockSpec(memory_space=memory_space)


def swapped(value, axis):
    return lax.ppermute(value, axis, [(k, k ^ 1) for k in range(lax.axis_size(axis))])


def params(mib, **kw):
    return pltpu.CompilerParams(vmem_limit_bytes=mib << 20, **kw)


def body(
    tokens,
    norm_gain,
    gate_proj,
    inner_proj,
    write_proj,
    read_proj,
    step_proj,
    step_bias,
    decay_log,
    skip_gain,
    conv_inner,
    conv_write,
    conv_read,
    out_gain,
    out_proj,
    saved_state,
    inner_history,
    write_history,
    read_history,
    last_steps,
    accepted,
):
    def hbm(value):
        return pltpu.with_memory_space_constraint(value, pltpu.HBM)

    anywhere = whole(pl.ANY)
    dma = pltpu.SemaphoreType.DMA

    def shape(*dims, kind=f32):
        return jax.ShapeDtypeStruct(dims, kind)

    saved = saved_state.reshape(64, 128, 128)
    sent, pack = pl.pallas_call(
        begin_kernel,
        out_shape=[pltpu.HBM((16, 8, 2048), bf16), shape(80, 2048, kind=bf16)],
        in_specs=[anywhere] * 5,
        out_specs=[anywhere, whole()],
        scratch_shapes=[
            pltpu.VMEM((8, 2048), bf16),
            pltpu.VMEM((7, 32, 64), bf16),
            pltpu.VMEM((7, 32, 64), bf16),
            dma((5,)),
            dma((16,)),
        ],
        compiler_params=params(4),
        name="begin",
    )(
        hbm(tokens),
        hbm(write_proj.T),
        hbm(read_proj.T),
        hbm(write_history.transpose(1, 2, 0)),
        hbm(read_history.transpose(1, 2, 0)),
    )
    mine = lax.all_to_all(sent, "kv", 0, 0, tiled=True)
    pack_kv = swapped(pack, "kv")
    pack_tp = swapped(pack, "tp")
    pack_both = swapped(pack_kv, "tp")
    gate_other = swapped(gate_proj, "tp")
    inner_other = swapped(inner_proj, "tp")
    out_other = swapped(out_proj, "tp")

    keep, give, held, step, acc, vec, derived = pl.pallas_call(
        prep_kernel,
        in_specs=[anywhere] * 12,
        out_specs=[anywhere] * 4 + [whole()] * 3,
        out_shape=[
            pltpu.HBM((32, 128, 128), bf16),
            pltpu.HBM((32, 128, 128), bf16),
            pltpu.HBM((8, 64, 128), f32),
            pltpu.HBM((256, 2048), bf16),
            shape(64, 128),
            shape(24, 128),
            shape(8, 32, 128),
        ],
        scratch_shapes=[
            pltpu.VMEM((8, 64, 128), f32),
            pltpu.VMEM((64, 128, 128), bf16),
            pltpu.VMEM((256, 2048), bf16),
            pltpu.VMEM((64, 128, 128), f32),
            pltpu.VMEM((7, 64, 128), bf16),
            pltpu.VMEM((4, 128), bf16),
            pltpu.VMEM((4, 128), bf16),
            pltpu.VMEM((4, 128), bf16),
            pltpu.VMEM((4, 128), bf16),
            pltpu.VMEM((1, 128), f32),
            pltpu.VMEM((1, 128), f32),
            pltpu.VMEM((4, 2, 64), f32),
            pltpu.VMEM((1, 64), jnp.int32),
            pltpu.VMEM((3, 64), f32),
            pltpu.VMEM((64, 2048), bf16),
            dma((45,)),
            dma((10,)),
        ],
        compiler_params=params(12),
        name="prep",
    )(
        *[
            hbm(v)
            for v in (
                saved,
                inner_history.transpose(1, 0, 2),
                conv_inner,
                conv_write,
                conv_read,
                out_gain[None, :],
                last_steps.transpose(1, 2, 0),
                accepted[None, :],
                decay_log[None, :],
                skip_gain[None, :],
                step_bias[None, :],
                step_proj.T,
            )
        ]
    )
    wall, mix = pl.pallas_call(
        group_kernel,
        in_specs=[whole()] * 6,
        out_specs=[anywhere] * 2,
        out_shape=[pltpu.HBM((256, 2048), bf16), pltpu.HBM((10, 64, 128), f32)],
        scratch_shapes=[
            pltpu.VMEM((256, 2048), bf16),
            pltpu.VMEM((10, 64, 128), f32),
            pltpu.VMEM((7, 128, 128), f32),
            dma((2,)),
        ],
        compiler_params=params(6),
        name="group",
    )(pack, pack_tp, pack_kv, pack_both, acc, vec)

    low_twin = swapped(give, "tp")
    derived_twin = swapped(derived, "tp")
    partial = pl.pallas_call(
        main_kernel,
        in_specs=[whole()] + [anywhere] * 10 + [whole()] * 5,
        out_specs=anywhere,
        out_shape=pltpu.HBM((128, 2176), bf16),
        scratch_shapes=[
            pltpu.VMEM((1, 2048), f32),
            pltpu.VMEM((256, 2048), bf16),
            pltpu.VMEM((256, 2048), bf16),
            pltpu.VMEM((2048, 128), bf16),
            pltpu.VMEM((2048, 128), bf16),
            pltpu.VMEM((10, 64, 128), f32),
            pltpu.VMEM((8, 64, 128), f32),
            pltpu.VMEM((2, 32, 128, 128), bf16),
            pltpu.VMEM((128, 2048), bf16),
            pltpu.VMEM((128, 2048), bf16),
            pltpu.VMEM((8, 128, 128), f32),
            pltpu.VMEM((2, 128, 128), f32),
            pltpu.VMEM((2, 128, 128), f32),
            pltpu.VMEM((128, 2176), bf16),
            dma((10,)),
            dma((4,)),
        ],
        compiler_params=params(12),
        name="main",
    )(
        mine,
        *[
            hbm(v)
            for v in (
                norm_gain[None, :],
                wall,
                step,
                inner_proj,
                gate_proj,
                held,
                mix,
                keep,
                low_twin,
                out_proj,
            )
        ],
        out_other,
        inner_other,
        gate_other,
        derived_twin,
        vec,
    )
    arrived = lax.all_to_all(partial.reshape(16, 8, 2176), "kv", 0, 0, tiled=True)
    base = pl.pallas_call(
        state_kernel,
        in_specs=[anywhere] * 4,
        out_specs=anywhere,
        out_shape=shape(64, 128, 128),
        scratch_shapes=[
            pltpu.VMEM((64, 128, 128), f32),
            pltpu.VMEM((64, 128, 128), f32),
            pltpu.VMEM((8, 64, 128), f32),
            pltpu.VMEM((4, 64, 128), f32),
            dma((10,)),
            dma((8,)),
        ],
        compiler_params=params(12),
        name="state",
    )(hbm(saved), hbm(held), hbm(mix), hbm(partial))
    mixed = pl.pallas_call(
        sum_kernel,
        in_specs=[whole()],
        out_specs=whole(),
        out_shape=shape(8, 2048, kind=bf16),
        compiler_params=params(4),
        name="total",
    )(arrived)
    return mixed, base.reshape(64, 2, 64, 128)


def solution(mesh):
    both = ("kv", "tp")
    placed = (
        P(("dp", "kv", "tp"), None),
        P(),
        P(None, both),
        P(None, both),
        P(None, both),
        P(None, both),
        P(),
        P(),
        P(),
        P(),
        P(),
        P(),
        P(),
        P(),
        P(both, None),
        P("dp", both, None, None),
        P("dp", None, both),
        P("dp", None, both),
        P("dp", None, both),
        P("dp", None, both),
        P("dp"),
    )
    return jax.shard_map(
        body,
        mesh=mesh,
        in_specs=placed,
        out_specs=(P(("dp", "kv", "tp"), None), P("dp", both, None, None)),
        check_vma=False,
    )
```

time: 57.2 us -> 58.9 us (1.030)
  starting transfers between devices: 17.7 us -> 14.9 us
  Pallas kernels: 17 us -> 19.3 us
  waiting for transfers between devices: 21.5 us -> 23.6 us
    ppermute x6 -> x8, waiting for transfers between devices: 2.43 us -> 9.11 us  [swapped(): lax.ppermute(value, axis, [(k, k ^ 1) for k in range(lax.axis_size(axis))])]
    all_to_all x1, starting transfers between devices: 6.46 us -> 3.59 us  [body(): lax.all_to_all(partial.reshape(16, 8, 2176), 'kv', 0, 0, tiled=True)]
    all_to_all x1, waiting for transfers between devices: 8.06 us -> 5.7 us  [body(): lax.all_to_all(partial.reshape(16, 8, 2176), 'kv', 0, 0, tiled=True)]
    all_to_all x1, waiting for transfers between devices: 11 us -> 8.81 us  [body(): mine = lax.all_to_all(sent, 'kv', 0, 0, tiled=True)]
    pallas_call x4 -> x3, Pallas kernels: 11.4 us -> 13.4 us  [the longest x1 5.98 us: body(): pl.pallas_call(main_kernel, in_specs=[whole()] + [anywhere] * 10 + [whole...]
    ppermute x6 -> x8, starting transfers between devices: 3.03 us -> 3.11 us  [swapped(): lax.ppermute(value, axis, [(k, k ^ 1) for k in range(lax.axis_size(axis))])]
  transfers between devices with their start and end apart: 8 -> 10, of which waited for: 4 -> 4; matrix products, arithmetic and copies ran while one was open for 0% -> 0% of each run, Pallas kernels for 23% -> 15%
where the time goes in v2:
time: 58.9 us; the launch traced here: 58.6 us
  waiting for transfers between devices  23.6 us (40%)
  Pallas kernels  19.3 us (33%)
  starting transfers between devices  14.9 us (25%)
  between operations  0.73 us (1%)
    ppermute x8, waiting for transfers between devices, swapped(): lax.ppermute(value, axis, [(k, k ^ 1) for k in range(lax.axis_size(axis))])  9.11 us
    all_to_all x1, waiting for transfers between devices, body(): mine = lax.all_to_all(sent, 'kv', 0, 0, tiled=True)  8.81 us
    all_to_all x1, starting transfers between devices, body(): mine = lax.all_to_all(sent, 'kv', 0, 0, tiled=True)  8.16 us
    pallas_call x1, Pallas kernels, body(): pl.pallas_call(main_kernel, in_specs=[whole()] + [anywhere] * 10 + [whole...  5.98 us
    all_to_all x1, waiting for transfers between devices, body(): lax.all_to_all(partial.reshape(16, 8, 2176), 'kv', 0, 0, tiled=True)  5.7 us
    pallas_call x1, Pallas kernels, body(): pl.pallas_call(state_kernel, in_specs=[anywhere] * 4, out_specs=anywhere,...  5.67 us
    pallas_call x1, Pallas kernels, body(): pl.pallas_call(prep_kernel, in_specs=[anywhere] * 12, out_specs=[anywhere...  3.8 us
    all_to_all x1, starting transfers between devices, body(): lax.all_to_all(partial.reshape(16, 8, 2176), 'kv', 0, 0, tiled=True)  3.59 us
  transfers between devices with their start and end apart: 10, of which 4 were waited for; matrix products, arithmetic and copies ran while one was open for 0% of the time, Pallas kernels for 15%

profile of v2, /device:TPU:0, one launch (start us, length us, event | category | flops | bytes accessed | tf_op | source)
XLA Modules:
  0.0 58.6 jit_solution(13022419585169497898)
XLA Ops:
  0.6 3.8 %prep.1 = (bf16[32,128,128]{2,1,0:T(8,128)(2,1)}, bf16[32,128,128]{2,1,0:T(8,128)(2,1)}, f32[8,64,128]{2,1,0:T(8,128)}, bf16[256,2048]{1,0:T(8,128)(2,1)}, f32[6...) custom-call(f32[64,128,128]{2,1,0:T(8,128)} %bitcast.16, bf16[7,64,128]{2,1,0:T(8,128)(2,1)} %bitcast.23, ...), custom_call_target="tpu_custom_call" | custom-call | tf_op jit(solution)/shard_map/prep/pallas_call | solution.py:556
  4.4 0.1 collective-permute-start.3
  4.5 1.8 %begin.1 = (bf16[16,8,2048]{2,1,0:T(8,128)(2,1)}, bf16[80,2048]{1,0:T(8,128)(2,1)S(1)}) custom-call(bf16[8,2048]{1,0:T(8,128)(2,1)} %tok_hbm.1, bf16[32,2048]{1,0:T(8,128)(2,1)} %bitcast.21, bf16[32,2048]{1,0:T(8,128)(2,1)} %bitcast.22, bf16[7,32,64]{2,1,0:T(8,128)(2,1)} %bitcast.24, bf16[7,32,64]{2,1,0:T(8,128)(2,1)} %bitcast.25), custom_call_target="tpu_custom_call" | custom-call | tf_op jit(solution)/shard_map/begin/pallas_call | solution.py:527
  6.3 1.8 %collective-permute-start.1 = (bf16[80,2048]{1,0:T(8,128)(2,1)S(1)}, bf16[80,2048]{1,0:T(8,128)(2,1)S(1)}, u32[]{:S(2)}, u32[]{:S(2)}) collective-permute-start(bf16[80,2048]{1,0:T(8,128)(2,1)S(1)} %get-tuple-element.14.p0_ref), channel_id=1, source_target_pairs={{0,2},{2,0},{4,6},{6,4},{8,10},{10,8},{12,14},{14,12},{16,18},{18,... | collective-permute-start | bytes 983048 | tf_op jit(solution)/shard_map/ppermute | solution.py:487
  8.1 0.2 collective-permute-start
  8.3 0.3 collective-permute-start.4
  8.6 0.2 collective-permute-start.5
  8.8 7.7 %collective-permute-done.1.p2_ref = bf16[80,2048]{1,0:T(8,128)(2,1)S(1)} collective-permute-done((bf16[80,2048]{1,0:T(8,128)(2,1)S(1)}, bf16[80,2048]{1,0:T(8,128)(2,1)S(1)}, u32[]{:S(2)}, u32[]{:S(2)}) %collective-permute-start.1) | collective-permute-done | bytes 327712 | tf_op jit(solution)/shard_map/ppermute | solution.py:487
  16.5 0.0 collective-permute-start.6
  16.5 8.2 %all-to-all-start = ((bf16[16,8,2048]{2,1,0:T(8,128)(2,1)}), bf16[16,8,2048]{2,1,0:T(8,128)(2,1)S(1)}, u32[]{:S(2)}, u32[]{:S(2)}) async-start(bf16[16,8,2048]{2,1,0:T(8,128)(2,1)} %get-tuple-element.13), calls=%async_computation | async-start | bytes 1048576 | tf_op jit(solution)/shard_map/all_to_all | solution.py:548
  24.6 0.0 collective-permute-done.p1_ref
  24.7 0.3 collective-permute-start.2
  25.0 1.4 %collective-permute-done.2.p3_ref = bf16[80,2048]{1,0:T(8,128)(2,1)S(1)} collective-permute-done((bf16[80,2048]{1,0:T(8,128)(2,1)S(1)}, bf16[80,2048]{1,0:T(8,128)(2,1)S(1)}, u32[]{:S(2)}, u32[]{:S(2)}) %collective-permute-start.2) | collective-permute-done | bytes 327712 | tf_op jit(solution)/shard_map/ppermute | solution.py:487
  26.4 0.2 collective-permute-start.7
  26.6 1.4 %group.1 = (bf16[256,2048]{1,0:T(8,128)(2,1)}, f32[10,64,128]{2,1,0:T(8,128)}) custom-call(bf16[80,2048]{1,0:T(8,128)(2,1)S(1)} %get-tuple-element.14.p0_ref, bf16[80,2048]{1,0:T(8,128)(2,1)S(1)} %collective-permute-done.p1_ref, bf16[80,2048]{1,0:T(8,128)(2,1)S(1)} %collective-permute-done.1.p2_ref, bf16[80,2048]{1,0:T(8,128)(2,1)S(1)} %collective-permute-done.2.p3_ref, ...), custom_call_target="tpu_custom_call" | custom-call | tf_op jit(solution)/shard_map/group/pallas_call | solution.py:609
  28.0 0.0 collective-permute-done.7.got_ref
  28.0 8.8 %all-to-all-done.mine_ref = bf16[16,8,2048]{2,1,0:T(8,128)(2,1)S(1)} async-done(((bf16[16,8,2048]{2,1,0:T(8,128)(2,1)}), bf16[16,8,2048]{2,1,0:T(8,128)(2,1)S(1)}, u32[]{:S(2)}, u32[]{:S(2)}) %all-to-all-start) | async-done | bytes 524320 | tf_op jit(solution)/shard_map/all_to_all | solution.py:548
  36.9 0.0 collective-permute-done.4.twin_own_ref
  36.9 0.0 collective-permute-done.5.twin_inner_ref
  36.9 0.0 collective-permute-done.6.twin_gate_ref
  36.9 0.0 collective-permute-done.3.twin_low_hbm
  36.9 6.0 %main.1.after_hbm = bf16[128,2176]{1,0:T(8,128)(2,1)} custom-call(bf16[16,8,2048]{2,1,0:T(8,128)(2,1)S(1)} %all-to-all-done.mine_ref, f32[1,2048]{1,0:T(1,128)} %bitcast.27, bf16[256,2048]{1,0:T(8,128)(2,1)} %get-tuple-element.17.wall_hbm, bf16[256,2048]{1,0:T(8,128)(2,1)} %get-tuple-element.18.step_hbm, bf16[2048,128]{1,0:T(8,128)(2,1)} %inner_hbm.1, ...), custom_call_target="tpu_custom_call" | custom-call | tf_op jit(solution)/shard_map/main/pallas_call | solution.py:626
  42.9 3.6 %all-to-all-start.1 = ((bf16[16,8,2176]{2,1,0:T(8,128)(2,1)}), bf16[16,8,2176]{2,1,0:T(8,128)(2,1)S(1)}, u32[]{:S(2)}, u32[]{:S(2)}) async-start(bf16[16,8,2176]{2,1,0:T(8,128)(2,1)} %bitcast.18), calls=%async_computation.1 | async-start | bytes 1114112 | tf_op jit(solution)/shard_map/all_to_all | solution.py:674
  46.5 5.7 %state.1 = f32[64,128,128]{2,1,0:T(8,128)} custom-call(f32[64,128,128]{2,1,0:T(8,128)} %bitcast.17, f32[8,64,128]{2,1,0:T(8,128)} %get-tuple-element.19.held_hbm, f32[10,64,128]{2,1,0:T(8,128)} %get-tuple-element.20.mix_hbm, bf16[128,2176]{1,0:T(8,128)(2,1)} %main.1.after_hbm), custom_call_target="tpu_custom_call" | custom-call | tf_op jit(solution)/shard_map/state/pallas_call | solution.py:675
  52.1 5.7 %all-to-all-done.1.in_ref = bf16[16,8,2176]{2,1,0:T(8,128)(2,1)S(1)} async-done(((bf16[16,8,2176]{2,1,0:T(8,128)(2,1)}), bf16[16,8,2176]{2,1,0:T(8,128)(2,1)S(1)}, u32[]{:S(2)}, u32[]{:S(2)}) %all-to-all-start.1) | async-done | bytes 557088 | tf_op jit(solution)/shard_map/all_to_all | solution.py:674
  57.8 0.7 %total.1 = bf16[8,2048]{1,0:T(8,128)(2,1)} custom-call(bf16[16,8,2176]{2,1,0:T(8,128)(2,1)S(1)} %all-to-all-done.1.in_ref), custom_call_target="tpu_custom_call" | custom-call | tf_op jit(solution)/shard_map/total/pallas_call | solution.py:691
Async XLA Ops:
  4.4 32.4 %collective-permute-start.3 = (bf16[32,128,128]{2,1,0:T(8,128)(2,1)}, bf16[32,128,128]{2,1,0:T(8,128)(2,1)}, u32[]{:S(2)}, u32[]{:S(2)}) collective-permute-start(bf16[32,128,128]{2,1,0:T(8,128)(2,1)} %get-tuple-element.22), channel_id=1, source_target_pairs={{0,1},{1,0},{2,3},{3,2},{4,5},{5,4},{6,7},{7,6},{8,9},{9,8},{10,11... | collective-permute-start | bytes 3145736 | tf_op jit(solution)/shard_map/ppermute | solution.py:487
  6.3 10.2 %collective-permute-start.1 = (bf16[80,2048]{1,0:T(8,128)(2,1)S(1)}, bf16[80,2048]{1,0:T(8,128)(2,1)S(1)}, u32[]{:S(2)}, u32[]{:S(2)}) collective-permute-start(bf16[80,2048]{1,0:T(8,128)(2,1)S(1)} %get-tuple-element.14.p0_ref), channel_id=1, source_target_pairs={{0,2},{2,0},{4,6},{6,4},{8,10},{10,8},{12,14},{14,12},{16,18},{18,... | collective-permute-start | bytes 983048 | tf_op jit(solution)/shard_map/ppermute | solution.py:487
  8.1 16.6 %collective-permute-start = (bf16[80,2048]{1,0:T(8,128)(2,1)S(1)}, bf16[80,2048]{1,0:T(8,128)(2,1)S(1)}, u32[]{:S(2)}, u32[]{:S(2)}) collective-permute-start(bf16[80,2048]{1,0:T(8,128)(2,1)S(1)} %get-tuple-element.14.p0_ref), channel_id=1, source_target_pairs={{0,1},{1,0},{2,3},{3,2},{4,5},{5,4},{6,7},{7,6},{8,9},{9,8},{10,11... | collective-permute-start | bytes 983048 | tf_op jit(solution)/shard_map/ppermute | solution.py:487
  8.3 28.6 %collective-permute-start.4 = (bf16[128,2048]{1,0:T(8,128)(2,1)}, bf16[128,2048]{1,0:T(8,128)(2,1)S(1)}, u32[]{:S(2)}, u32[]{:S(2)}) collective-permute-start(bf16[128,2048]{1,0:T(8,128)(2,1)} %own_hbm.1), channel_id=1, source_target_pairs={{0,1},{1,0},{2,3},{3,2},{4,5},{5,4},{6,7},{7,6},{8,9},{9,8},{10,11... | collective-permute-start | bytes 1572872 | tf_op jit(solution)/shard_map/ppermute | solution.py:487
  8.6 28.3 %collective-permute-start.5 = (bf16[2048,128]{1,0:T(8,128)(2,1)}, bf16[2048,128]{1,0:T(8,128)(2,1)S(1)}, u32[]{:S(2)}, u32[]{:S(2)}) collective-permute-start(bf16[2048,128]{1,0:T(8,128)(2,1)} %inner_hbm.1), channel_id=1, source_target_pairs={{0,1},{1,0},{2,3},{3,2},{4,5},{5,4},{6,7},{7,6},{8,9},{9,8},{10,11... | collective-permute-start | bytes 1572872 | tf_op jit(solution)/shard_map/ppermute | solution.py:487
  16.5 20.4 %collective-permute-start.6 = (bf16[2048,128]{1,0:T(8,128)(2,1)}, bf16[2048,128]{1,0:T(8,128)(2,1)S(1)}, u32[]{:S(2)}, u32[]{:S(2)}) collective-permute-start(bf16[2048,128]{1,0:T(8,128)(2,1)} %gate_hbm.1), channel_id=1, source_target_pairs={{0,1},{1,0},{2,3},{3,2},{4,5},{5,4},{6,7},{7,6},{8,9},{9,8},{10,11... | collective-permute-start | bytes 1572872 | tf_op jit(solution)/shard_map/ppermute | solution.py:487
  16.5 20.4 %all-to-all-start = ((bf16[16,8,2048]{2,1,0:T(8,128)(2,1)}), bf16[16,8,2048]{2,1,0:T(8,128)(2,1)S(1)}, u32[]{:S(2)}, u32[]{:S(2)}) async-start(bf16[16,8,2048]{2,1,0:T(8,128)(2,1)} %get-tuple-element.13), calls=%async_computation | async-start | bytes 1048576 | tf_op jit(solution)/shard_map/all_to_all | solution.py:548
  24.7 1.7 %collective-permute-start.2 = (bf16[80,2048]{1,0:T(8,128)(2,1)S(1)}, bf16[80,2048]{1,0:T(8,128)(2,1)S(1)}, u32[]{:S(2)}, u32[]{:S(2)}) collective-permute-start(bf16[80,2048]{1,0:T(8,128)(2,1)S(1)} %collective-permute-done.1.p2_ref), channel_id=1, source_target_pairs={{0,1},{1,0},{2,3},{3,2},{4,5},{5,4},{6,7},{7,6},{8,9},{9,8},{10,11... | collective-permute-start | bytes 983048 | tf_op jit(solution)/shard_map/ppermute | solution.py:487
  26.4 1.7 %collective-permute-start.7 = (f32[8,32,128]{2,1,0:T(8,128)S(1)}, f32[8,32,128]{2,1,0:T(8,128)S(1)}, u32[]{:S(2)}, u32[]{:S(2)}) collective-permute-start(f32[8,32,128]{2,1,0:T(8,128)S(1)} %get-tuple-element.23), channel_id=1, source_target_pairs={{0,1},{1,0},{2,3},{3,2},{4,5},{5,4},{6,7},{7,6},{8,9},{9,8},{10,11... | collective-permute-start | bytes 393224 | tf_op jit(solution)/shard_map/ppermute | solution.py:487
  42.9 15.0 %all-to-all-start.1 = ((bf16[16,8,2176]{2,1,0:T(8,128)(2,1)}), bf16[16,8,2176]{2,1,0:T(8,128)(2,1)S(1)}, u32[]{:S(2)}, u32[]{:S(2)}) async-start(bf16[16,8,2176]{2,1,0:T(8,128)(2,1)} %bitcast.18), calls=%async_computation.1 | async-start | bytes 1114112 | tf_op jit(solution)/shard_map/all_to_all | solution.py:674

commit v3 on v2

--- a/solution.py
+++ b/solution.py
@@ -89,17 +89,12 @@
     decay_hbm,
     skip_hbm,
     bias_hbm,
-    step_hbm,
-    keep_hbm,
     give_hbm,
-    held_hbm,
-    wide_hbm,
+    held_s,
     acc_ref,
     vec_ref,
     sent_ref,
-    held_s,
     low_s,
-    wide_s,
     saved_s,
     ihist_s,
     tin_s,
@@ -111,7 +106,6 @@
     ls_s,
     acc_s,
     heads_s,
-    step_s,
     sems,
     sent,
 ):
@@ -134,15 +128,21 @@
         (gain_hbm.at[:, pl.ds(col, 128)], gain_s),
         (gain_hbm.at[:, pl.ds(twin_col, 128)], twin_gain_s),
         (ihist_hbm, ihist_s),
-        (step_hbm, step_s),
     )
     big = tuple(
-        (saved_hbm.at[pl.ds(kv * 4 + c * 2, 2)], saved_s.at[p * 32 + kv * 2 : p * 32 + kv * 2 + 2])
-        for p, c in enumerate((1 - core, core))
+        (saved_hbm.at[pl.ds(kv * 4 + (1 - core) * 2, 2)], saved_s.at[kv * 2 : kv * 2 + 2])
         for kv in range(16)
     )
-    copies = fetch(small + big, sems)
-    for copy in copies[: len(small)]:
+    copies = fetch(big + small, sems)
+    out = []
+    for k in range(4):
+        block = slice(k * 8, (k + 1) * 8)
+        for copy in copies[k * 4 : k * 4 + 4]:
+            copy.wait()
+        low_s[block] = saved_s[block].astype(bf16)
+        out.append(pltpu.make_async_copy(low_s.at[block], give_hbm.at[block], sent.at[k]))
+        out[-1].start()
+    for copy in copies[len(big) :]:
         copy.wait()
 
     tin = tin_s[...].astype(f32)
@@ -202,24 +202,6 @@
         block = slice(q * 16, (q + 1) * 16)
         for t in range(8):
             sent_ref[t, block] = held_s[t, pl.ds(start, 16, stride=4), :]
-    held = pltpu.make_async_copy(held_s, held_hbm, sent.at[9])
-    held.start()
-
-    row = lax.broadcasted_iota(jnp.int32, (256, 64), 0)
-    base = jnp.where(row < 128, head, twin_head)
-    pick = lax.broadcasted_iota(jnp.int32, (256, 64), 1) == base + ((row >> 6) & 1)
-    wide_s[...] = dot(pick.astype(f32).astype(bf16), step_s[...]).astype(bf16)
-    out = [pltpu.make_async_copy(wide_s, wide_hbm, sent.at[8])]
-    out[0].start()
-    out.append(held)
-    for k in range(8):
-        block = slice(k * 8, (k + 1) * 8)
-        for copy in copies[len(small) + k * 4 : len(small) + k * 4 + 4]:
-            copy.wait()
-        low_s[block] = saved_s[block].astype(bf16)
-        dest = (give_hbm if k < 4 else keep_hbm).at[slice((k % 4) * 8, (k % 4 + 1) * 8)]
-        out.append(pltpu.make_async_copy(low_s.at[block], dest, sent.at[k]))
-        out[-1].start()
     for copy in out:
         copy.wait()
 
@@ -261,16 +243,15 @@
 
 
 def state_kernel(
-    saved_hbm, held_hbm, mix_hbm, after_hbm, base_hbm, saved_s, base_s, held_s, mix_s, sems, sent
+    saved_hbm, mix_hbm, after_hbm, held_s, base_hbm, saved_s, base_s, mix_s, sems, sent
 ):
     blocks = [slice(k * 8, (k + 1) * 8) for k in range(8)]
     copies = fetch(
         [(saved_hbm.at[k], saved_s.at[k]) for k in blocks]
-        + [(held_hbm, held_s), (mix_hbm.at[6:10], mix_s)],
+        + [(mix_hbm.at[6:10], mix_s)],
         sems,
     )
     copies[8].wait()
-    copies[9].wait()
     tot = jnp.concatenate([held_s[7], held_s[7]], axis=0).T
     at = jnp.concatenate(
         [jnp.concatenate([held_s[2 * p], held_s[2 * p + 1]], axis=0).T for p in range(2)], axis=1
@@ -301,15 +282,15 @@
     step_hbm,
     inner_hbm,
     gate_hbm,
-    held_hbm,
     mix_hbm,
-    low_hbm,
-    twin_low_hbm,
+    saved_hbm,
     own_hbm,
-    twin_own_ref,
+    twin_own_hbm,
+    got_hbm,
+    held_s,
+    twin_low_ref,
     twin_inner_ref,
     twin_gate_ref,
-    got_ref,
     vec_ref,
     out_hbm,
     norm_s,
@@ -318,17 +299,18 @@
     inner_s,
     gate_s,
     mix_s,
-    held_s,
+    got_ref,
     low_s,
     proj_s,
     nrm_s,
     rows_s,
     read_s,
-    car_s,
+    part_s,
     out_s,
     sems,
     sent,
 ):
+    core = lax.axis_index("tp")
     copies = fetch(
         (
             (norm_hbm, norm_s),
@@ -337,14 +319,16 @@
             (inner_hbm, inner_s),
             (gate_hbm, gate_s),
             (mix_hbm, mix_s),
-            (held_hbm, held_s),
-            (low_hbm, low_s.at[0]),
-            (twin_low_hbm, low_s.at[1]),
-            (own_hbm, proj_s),
+            (got_hbm, got_ref),
+            (own_hbm, proj_s.at[0]),
+            (twin_own_hbm, proj_s.at[1]),
+        )
+        + tuple(
+            (saved_hbm.at[pl.ds(kv * 4 + core * 2, 2)], low_s.at[kv * 2 : kv * 2 + 2])
+            for kv in range(16)
         ),
         sems,
     )
-    core = lax.axis_index("tp")
     copies[0].wait()
     gain = norm_s[...]
     for k in range(8):
@@ -352,20 +336,29 @@
         scale = lax.rsqrt(jnp.mean(x * x, axis=-1, keepdims=True) + EPSILON)
         nrm_s[k * 16 : (k + 1) * 16, :] = (x * scale * gain).astype(bf16)
     normed = nrm_s[...]
-    copies[1].wait()
+    for copy in copies[1:5]:
+        copy.wait()
     both = rounded(dot(normed, wall_s[...], NT))
     rows_s[2] = both[:, 0:128]
     rows_s[3] = both[:, 128:256]
-    copies[2].wait()
+    weights = [inner_s[...], twin_inner_ref[...], gate_s[...], twin_gate_ref[...]]
+    both = rounded(dot(normed, jnp.concatenate(weights, axis=1)))
+    for k in range(4):
+        rows_s[4 + k] = both[:, k * 128 : (k + 1) * 128]
     both = dot(normed, step_s[...], NT)
+    lane = lax.broadcasted_iota(jnp.int32, (64, 256), 1)
+    head = (device_rank() ^ (lane >> 7)) * 2 + ((lane >> 6) & 1)
+    pick = lax.broadcasted_iota(jnp.int32, (64, 256), 0) == head
+    pick = pick.astype(f32).astype(bf16)
+    high = both.astype(bf16)
+    rest = both - high.astype(f32)
+    mid = rest.astype(bf16)
+    low = (rest - mid.astype(f32)).astype(bf16)
+    both = dot(high, pick) + (dot(mid, pick) + dot(low, pick))
     rows_s[0] = both[:, 0:128]
     rows_s[1] = both[:, 128:256]
-    rows_s[5] = rounded(dot(normed, twin_inner_ref[...]))
-    rows_s[7] = rounded(dot(normed, twin_gate_ref[...]))
-    copies[3].wait()
-    rows_s[4] = rounded(dot(normed, inner_s[...]))
-    copies[4].wait()
-    rows_s[6] = rounded(dot(normed, gate_s[...]))
+    for copy in copies[5:]:
+        copy.wait()
 
     def at_time(ref, t, k):
         return jnp.concatenate([ref[k, pl.ds(q * 4 + t, 16, stride=8), :] for q in range(2)], axis=0)
@@ -395,29 +388,16 @@
         new = [at_time(rows_s, t, k) for t in range(4)]
         return [rounded(v) for v in conv_new(new, [chosen(mix_s, base + i) for i in range(3)], taps)]
 
-    copies[5].wait()
     write = mixing(2, 0, taps_of(4))
     read = mixing(3, 3, taps_of(8))
     for t in range(4):
         put(read_s, t, 0, read[t])
-    quarter = lax.broadcasted_iota(jnp.int32, (16, 128), 0) >> 2
-    copies[7].wait()
-    copies[8].wait()
-    for g in range(8):
-        r = read_s[0, g * 16 : (g + 1) * 16, :].astype(bf16)
-        for p in range(2):
-            full = dot(r, low_s[p, g * 4 : (g + 1) * 4].reshape(512, 128), NT)
-            v = full[:, 0:128]
-            for q in range(1, 4):
-                v = jnp.where(quarter == q, full[:, q * 128 : (q + 1) * 128], v)
-            car_s[p, g * 16 : (g + 1) * 16, :] = v
 
     def score(x, y):
         return jnp.sum(x * y, axis=-1, keepdims=True)
 
     scores = [[score(read[i], write[j]) for j in range(i + 1)] for i in range(4)]
     past = [chosen(mix_s, 6 + t) for t in range(4)]
-    copies[6].wait()
     olds = [[score(read[i], past[t]) for t in range(4)] for i in range(4)]
     for p in range(2):
         if p == 0:
@@ -442,27 +422,40 @@
             sums.append(sums[-1] + rate * steps[t])
         moved = [steps[t] * inner[t] for t in range(4)]
         for i in range(4):
-            state = tot * at_time(car_s, i, p)
-            for t in range(4):
+            decay = jnp.exp(sums[i])
+            state = held[0] * olds[i][0]
+            for t in range(1, 4):
                 state = state + held[t] * olds[i][t]
-            y = jnp.exp(sums[i]) * state + skip * inner[i] + scores[i][i] * moved[i]
+            y = decay * state + skip * inner[i] + scores[i][i] * moved[i]
             for j in range(i):
                 y = y + scores[i][j] * jnp.exp(sums[i] - sums[j]) * moved[j]
-            put(read_s, i, p, y * silu(at_time(rows_s, i, 6 + p)))
+            gate = silu(at_time(rows_s, i, 6 + p))
+            put(part_s, i, p, y * gate)
+            put(part_s, i, 2 + p, decay * tot * gate)
+
+    quarter = lax.broadcasted_iota(jnp.int32, (16, 128), 0) >> 2
+    for g in range(8):
+        rows = slice(g * 16, (g + 1) * 16)
+        r = read_s[0, rows, :].astype(bf16)
+        for p, low in enumerate((low_s, twin_low_ref)):
+            full = dot(r, low[g * 4 : (g + 1) * 4].reshape(512, 128).astype(bf16), NT)
+            v = full[:, 0:128]
+            for q in range(1, 4):
+                v = jnp.where(quarter == q, full[:, q * 128 : (q + 1) * 128], v)
+            part_s[p, rows, :] = part_s[p, rows, :] + part_s[2 + p, rows, :] * v
 
     lane = lax.broadcasted_iota(jnp.int32, (128, 128), 1)
-    gated = [read_s[p] for p in range(2)]
+    gated = [part_s[p] for p in range(2)]
     sq = jnp.sum(gated[0] * gated[0] + gated[1] * gated[1], axis=-1, keepdims=True)
     hi = rounded(sq)
     out_s[:, 2048:2176] = jnp.where(lane == 0, hi, jnp.where(lane == 1, sq - hi, 0.0)).astype(bf16)
     unscaled = [
         (gated[p] * vec_ref[15 + 8 * p : 16 + 8 * p, :]).astype(bf16) for p in range(2)
     ]
-    copies[9].wait()
     out = []
     for k in range(4):
         cols = slice(k * 512, (k + 1) * 512)
-        value = dot(unscaled[0], proj_s[:, cols]) + dot(unscaled[1], twin_own_ref[:, cols])
+        value = dot(unscaled[0], proj_s[0, :, cols]) + dot(unscaled[1], proj_s[1, :, cols])
         out_s[:, cols] = value.astype(bf16)
         cols = slice(k * 512, 2176 if k == 3 else (k + 1) * 512)
         out.append(pltpu.make_async_copy(out_s.at[:, cols], out_hbm.at[:, cols], sent.at[k]))
@@ -553,24 +546,20 @@
     inner_other = swapped(inner_proj, "tp")
     out_other = swapped(out_proj, "tp")
 
-    keep, give, held, step, acc, vec, derived = pl.pallas_call(
+    give, held, acc, vec, derived = pl.pallas_call(
         prep_kernel,
-        in_specs=[anywhere] * 12,
-        out_specs=[anywhere] * 4 + [whole()] * 3,
+        in_specs=[anywhere] * 11,
+        out_specs=[anywhere] + [whole()] * 4,
         out_shape=[
             pltpu.HBM((32, 128, 128), bf16),
-            pltpu.HBM((32, 128, 128), bf16),
-            pltpu.HBM((8, 64, 128), f32),
-            pltpu.HBM((256, 2048), bf16),
+            shape(8, 64, 128),
             shape(64, 128),
             shape(24, 128),
             shape(8, 32, 128),
         ],
         scratch_shapes=[
-            pltpu.VMEM((8, 64, 128), f32),
-            pltpu.VMEM((64, 128, 128), bf16),
-            pltpu.VMEM((256, 2048), bf16),
-            pltpu.VMEM((64, 128, 128), f32),
+            pltpu.VMEM((32, 128, 128), bf16),
+            pltpu.VMEM((32, 128, 128), f32),
             pltpu.VMEM((7, 64, 128), bf16),
             pltpu.VMEM((4, 128), bf16),
             pltpu.VMEM((4, 128), bf16),
@@ -581,9 +570,8 @@
             pltpu.VMEM((4, 2, 64), f32),
             pltpu.VMEM((1, 64), jnp.int32),
             pltpu.VMEM((3, 64), f32),
-            pltpu.VMEM((64, 2048), bf16),
-            dma((45,)),
-            dma((10,)),
+            dma((28,)),
+            dma((4,)),
         ],
         compiler_params=params(12),
         name="prep",
@@ -602,7 +590,6 @@
                 decay_log[None, :],
                 skip_gain[None, :],
                 step_bias[None, :],
-                step_proj.T,
             )
         ]
     )
@@ -621,8 +608,8 @@
         name="group",
     )(pack, pack_tp, pack_kv, pack_both, acc, vec)
 
+    derived_twin = swapped(derived, "tp")
     low_twin = swapped(give, "tp")
-    derived_twin = swapped(derived, "tp")
     partial = pl.pallas_call(
         main_kernel,
         in_specs=[whole()] + [anywhere] * 10 + [whole()] * 5,
@@ -631,19 +618,19 @@
         scratch_shapes=[
             pltpu.VMEM((1, 2048), f32),
             pltpu.VMEM((256, 2048), bf16),
-            pltpu.VMEM((256, 2048), bf16),
+            pltpu.VMEM((64, 2048), bf16),
             pltpu.VMEM((2048, 128), bf16),
             pltpu.VMEM((2048, 128), bf16),
             pltpu.VMEM((10, 64, 128), f32),
-            pltpu.VMEM((8, 64, 128), f32),
-            pltpu.VMEM((2, 32, 128, 128), bf16),
-            pltpu.VMEM((128, 2048), bf16),
+            pltpu.VMEM((8, 32, 128), f32),
+            pltpu.VMEM((32, 128, 128), f32),
+            pltpu.VMEM((2, 128, 2048), bf16),
             pltpu.VMEM((128, 2048), bf16),
             pltpu.VMEM((8, 128, 128), f32),
-            pltpu.VMEM((2, 128, 128), f32),
-            pltpu.VMEM((2, 128, 128), f32),
+            pltpu.VMEM((1, 128, 128), f32),
+            pltpu.VMEM((4, 128, 128), f32),
             pltpu.VMEM((128, 2176), bf16),
-            dma((10,)),
+            dma((25,)),
             dma((4,)),
         ],
         compiler_params=params(12),
@@ -655,39 +642,38 @@
             for v in (
                 norm_gain[None, :],
                 wall,
-                step,
+                step_proj.T,
                 inner_proj,
                 gate_proj,
-                held,
                 mix,
-                keep,
-                low_twin,
+                saved,
                 out_proj,
+                out_other,
+                derived_twin,
             )
         ],
-        out_other,
+        held,
+        low_twin,
         inner_other,
         gate_other,
-        derived_twin,
         vec,
     )
     arrived = lax.all_to_all(partial.reshape(16, 8, 2176), "kv", 0, 0, tiled=True)
     base = pl.pallas_call(
         state_kernel,
-        in_specs=[anywhere] * 4,
+        in_specs=[anywhere] * 3 + [whole()],
         out_specs=anywhere,
         out_shape=shape(64, 128, 128),
         scratch_shapes=[
             pltpu.VMEM((64, 128, 128), f32),
             pltpu.VMEM((64, 128, 128), f32),
-            pltpu.VMEM((8, 64, 128), f32),
             pltpu.VMEM((4, 64, 128), f32),
-            dma((10,)),
+            dma((9,)),
             dma((8,)),
         ],
         compiler_params=params(12),
         name="state",
-    )(hbm(saved), hbm(held), hbm(mix), hbm(partial))
+    )(hbm(saved), hbm(mix), hbm(partial), held)
     mixed = pl.pallas_call(
         sum_kernel,
         in_specs=[whole()],

time: 58.9 us -> 56.9 us (0.966)
  waiting for transfers between devices: 23.6 us -> 22 us
  Pallas kernels: 19.3 us -> 18.1 us
  local copies, waits for them, and re-layouts: 0 us -> 0.77 us
    all_to_all x1, waiting for transfers between devices: 8.81 us -> 7.11 us  [body(): mine = lax.all_to_all(sent, 'kv', 0, 0, tiled=True)]
    pallas_call x2, Pallas kernels: 9.46 us -> 8.2 us  [the longest x1 5.57 us: body(): pl.pallas_call(state_kernel, in_specs=[anywhere] * 3 + [whole()], out_spe...]
    pallas_call x1, Pallas kernels: 5.98 us -> 5 us  [body(): pl.pallas_call(main_kernel, in_specs=[whole()] + [anywhere] * 10 + [whole...]
    pallas_call x1, Pallas kernels: 1.43 us -> 2.37 us  [body(): pl.pallas_call(group_kernel, in_specs=[whole()] * 6, out_specs=[anywhere]...]
    unnamed x0 -> x6, local copies, waits for them, and re-layouts: none -> 0.77 us
  transfers between devices with their start and end apart: 10 -> 10, of which waited for: 4 -> 4; matrix products, arithmetic and copies ran while one was open for 0% -> 0% of each run, Pallas kernels for 15% -> 17%
where the time goes in v3:
time: 56.9 us; the launch traced here: 56.4 us
  waiting for transfers between devices  22 us (39%)
  Pallas kernels  18.1 us (32%)
  starting transfers between devices  14.8 us (26%)
  local copies, waits for them, and re-layouts  0.77 us (1%)
  between operations  0.75 us (1%)
    ppermute x8, waiting for transfers between devices, swapped(): lax.ppermute(value, axis, [(k, k ^ 1) for k in range(lax.axis_size(axis))])  9.13 us
    all_to_all x1, starting transfers between devices, body(): mine = lax.all_to_all(sent, 'kv', 0, 0, tiled=True)  8.17 us
    all_to_all x1, waiting for transfers between devices, body(): mine = lax.all_to_all(sent, 'kv', 0, 0, tiled=True)  7.11 us
    all_to_all x1, waiting for transfers between devices, body(): lax.all_to_all(partial.reshape(16, 8, 2176), 'kv', 0, 0, tiled=True)  5.78 us
    pallas_call x1, Pallas kernels, body(): pl.pallas_call(state_kernel, in_specs=[anywhere] * 3 + [whole()], out_spe...  5.57 us
    pallas_call x1, Pallas kernels, body(): pl.pallas_call(main_kernel, in_specs=[whole()] + [anywhere] * 10 + [whole...  5 us
    all_to_all x1, starting transfers between devices, body(): lax.all_to_all(partial.reshape(16, 8, 2176), 'kv', 0, 0, tiled=True)  3.59 us
    ppermute x8, starting transfers between devices, swapped(): lax.ppermute(value, axis, [(k, k ^ 1) for k in range(lax.axis_size(axis))])  3.08 us
  transfers between devices with their start and end apart: 10, of which 4 were waited for; matrix products, arithmetic and copies ran while one was open for 0% of the time, Pallas kernels for 17%

profile of v3, /device:TPU:0, one launch (start us, length us, event | category | flops | bytes accessed | tf_op | source)
XLA Modules:
  0.0 56.4 jit_solution(4309133869008369967)
XLA Ops:
  0.6 2.6 %prep.1 = (bf16[32,128,128]{2,1,0:T(8,128)(2,1)}, f32[8,64,128]{2,1,0:T(8,128)S(1)}, f32[64,128]{1,0:T(8,128)S(1)}, f32[24,128]{1,0:T(8,128)S(1)}, f32[8,32,128]{2,1,0:T(8,128)S(1)}) custom-call(f32[64,128,128]{2,1,0:T(8,128)} %bitcast.16, bf16[7,64,128]{2,1,0:T(8,128)(2,1)} %bitcast.24, bf16[4,4096]{1,0:T(4,128)(2,1)} %tin_hbm.1, bf16[4,1024]{1,0:T(4,128)(2,1)} %tw_hbm.1, ...), custom_call_target="tpu_custom_call" | custom-call | tf_op jit(solution)/shard_map/prep/pallas_call | solution.py:549
  3.3 0.0 copy-start
  3.3 0.0 copy-start.2
  3.3 0.1 collective-permute-start.5
  3.4 1.8 %begin.1 = (bf16[16,8,2048]{2,1,0:T(8,128)(2,1)}, bf16[80,2048]{1,0:T(8,128)(2,1)S(1)}) custom-call(bf16[8,2048]{1,0:T(8,128)(2,1)} %tok_hbm.1, bf16[32,2048]{1,0:T(8,128)(2,1)} %bitcast.22, bf16[32,2048]{1,0:T(8,128)(2,1)} %bitcast.23, bf16[7,32,64]{2,1,0:T(8,128)(2,1)} %bitcast.25, bf16[7,32,64]{2,1,0:T(8,128)(2,1)} %bitcast.26), custom_call_target="tpu_custom_call" | custom-call | tf_op jit(solution)/shard_map/begin/pallas_call | solution.py:520
  5.2 1.8 %collective-permute-start.1 = (bf16[80,2048]{1,0:T(8,128)(2,1)S(1)}, bf16[80,2048]{1,0:T(8,128)(2,1)S(1)}, u32[]{:S(2)}, u32[]{:S(2)}) collective-permute-start(bf16[80,2048]{1,0:T(8,128)(2,1)S(1)} %get-tuple-element.12.p0_ref), channel_id=1, source_target_pairs={{0,2},{2,0},{4,6},{6,4},{8,10},{10,8},{12,14},{14,12},{16,18},{18,... | collective-permute-start | bytes 983048 | tf_op jit(solution)/shard_map/ppermute | solution.py:480
  6.9 0.2 collective-permute-start
  7.1 0.3 collective-permute-start.3
  7.4 0.2 collective-permute-start.6
  7.6 7.7 %collective-permute-done.1.p2_ref = bf16[80,2048]{1,0:T(8,128)(2,1)S(1)} collective-permute-done((bf16[80,2048]{1,0:T(8,128)(2,1)S(1)}, bf16[80,2048]{1,0:T(8,128)(2,1)S(1)}, u32[]{:S(2)}, u32[]{:S(2)}) %collective-permute-start.1) | collective-permute-done | bytes 327712 | tf_op jit(solution)/shard_map/ppermute | solution.py:480
  15.3 0.0 copy-done
  15.3 0.0 collective-permute-start.7
  15.3 0.0 copy-done.2
  15.4 8.2 %all-to-all-start = ((bf16[16,8,2048]{2,1,0:T(8,128)(2,1)}), bf16[16,8,2048]{2,1,0:T(8,128)(2,1)S(1)}, u32[]{:S(2)}, u32[]{:S(2)}) async-start(bf16[16,8,2048]{2,1,0:T(8,128)(2,1)} %get-tuple-element.11), calls=%async_computation | async-start | bytes 1048576 | tf_op jit(solution)/shard_map/all_to_all | solution.py:541
  23.5 0.0 collective-permute-done.p1_ref
  23.5 0.3 collective-permute-start.2
  23.8 1.4 %collective-permute-done.2.p3_ref = bf16[80,2048]{1,0:T(8,128)(2,1)S(1)} collective-permute-done((bf16[80,2048]{1,0:T(8,128)(2,1)S(1)}, bf16[80,2048]{1,0:T(8,128)(2,1)S(1)}, u32[]{:S(2)}, u32[]{:S(2)}) %collective-permute-start.2) | collective-permute-done | bytes 327712 | tf_op jit(solution)/shard_map/ppermute | solution.py:480
  25.3 0.2 collective-permute-start.4
  25.5 0.0 copy-start.1
  25.5 0.8 %copy-done.1 = f32[64,128]{1,0:T(8,128)S(1)} copy-done((f32[64,128]{1,0:T(8,128)S(1)}, f32[64,128]{1,0:T(8,128)}, u32[]{:S(2)}) %copy-start.1) | copy-done | bytes 32792
  26.2 2.4 %group.1 = (bf16[256,2048]{1,0:T(8,128)(2,1)}, f32[10,64,128]{2,1,0:T(8,128)}) custom-call(bf16[80,2048]{1,0:T(8,128)(2,1)S(1)} %get-tuple-element.12.p0_ref, bf16[80,2048]{1,0:T(8,128)(2,1)} %collective-permute-done.p1_ref, bf16[80,2048]{1,0:T(8,128)(2,1)S(1)} %collective-permute-done.1.p2_ref, bf16[80,2048]{1,0:T(8,128)(2,1)S(1)} %collective-permute-done.2.p3_ref, ...), custom_call_target="tpu_custom_call" | custom-call | tf_op jit(solution)/shard_map/group/pallas_call | solution.py:596
  28.6 0.0 collective-permute-done.4.got_hbm
  28.6 7.1 %all-to-all-done.mine_ref = bf16[16,8,2048]{2,1,0:T(8,128)(2,1)S(1)} async-done(((bf16[16,8,2048]{2,1,0:T(8,128)(2,1)}), bf16[16,8,2048]{2,1,0:T(8,128)(2,1)S(1)}, u32[]{:S(2)}, u32[]{:S(2)}) %all-to-all-start) | async-done | bytes 524320 | tf_op jit(solution)/shard_map/all_to_all | solution.py:541
  35.7 0.0 collective-permute-done.3.twin_own_hbm
  35.7 0.0 collective-permute-done.6.twin_inner_ref
  35.7 0.0 collective-permute-done.7.twin_gate_ref
  35.7 0.0 collective-permute-done.5.twin_low_ref
  35.7 5.0 %main.1.after_hbm = bf16[128,2176]{1,0:T(8,128)(2,1)} custom-call(bf16[16,8,2048]{2,1,0:T(8,128)(2,1)S(1)} %all-to-all-done.mine_ref, f32[1,2048]{1,0:T(1,128)} %bitcast.28, bf16[256,2048]{1,0:T(8,128)(2,1)} %get-tuple-element.15.wall_hbm, bf16[64,2048]{1,0:T(8,128)(2,1)} %bitcast.21, bf16[2048,128]{1,0:T(8,128)(2,1)} %inner_hbm.1, ...), custom_call_target="tpu_custom_call" | custom-call | tf_op jit(solution)/shard_map/main/pallas_call | solution.py:613
  40.8 3.6 %all-to-all-start.1 = ((bf16[16,8,2176]{2,1,0:T(8,128)(2,1)}), bf16[16,8,2176]{2,1,0:T(8,128)(2,1)S(1)}, u32[]{:S(2)}, u32[]{:S(2)}) async-start(bf16[16,8,2176]{2,1,0:T(8,128)(2,1)} %bitcast.19), calls=%async_computation.1 | async-start | bytes 1114112 | tf_op jit(solution)/shard_map/all_to_all | solution.py:661
  44.4 5.6 %state.1 = f32[64,128,128]{2,1,0:T(8,128)} custom-call(f32[64,128,128]{2,1,0:T(8,128)} %bitcast.18, f32[10,64,128]{2,1,0:T(8,128)} %get-tuple-element.16.mix_hbm, bf16[128,2176]{1,0:T(8,128)(2,1)} %main.1.after_hbm, f32[8,64,128]{2,1,0:T(8,128)S(1)} %get-tuple-element.18.held_s), custom_call_target="tpu_custom_call" | custom-call | tf_op jit(solution)/shard_map/state/pallas_call | solution.py:662
  49.9 5.8 %all-to-all-done.1.in_ref = bf16[16,8,2176]{2,1,0:T(8,128)(2,1)S(1)} async-done(((bf16[16,8,2176]{2,1,0:T(8,128)(2,1)}), bf16[16,8,2176]{2,1,0:T(8,128)(2,1)S(1)}, u32[]{:S(2)}, u32[]{:S(2)}) %all-to-all-start.1) | async-done | bytes 557088 | tf_op jit(solution)/shard_map/all_to_all | solution.py:661
  55.7 0.7 %total.1 = bf16[8,2048]{1,0:T(8,128)(2,1)} custom-call(bf16[16,8,2176]{2,1,0:T(8,128)(2,1)S(1)} %all-to-all-done.1.in_ref), custom_call_target="tpu_custom_call" | custom-call | tf_op jit(solution)/shard_map/total/pallas_call | solution.py:677
Async XLA Ops:
  3.3 12.1 %copy-start = (f32[64,128]{1,0:T(8,128)}, f32[64,128]{1,0:T(8,128)S(1)}, u32[]{:S(2)}) copy-start(f32[64,128]{1,0:T(8,128)S(1)} %get-tuple-element.13.acc_ref) | copy-start | bytes 98308
  3.3 12.1 %copy-start.2 = (f32[8,32,128]{2,1,0:T(8,128)}, f32[8,32,128]{2,1,0:T(8,128)S(1)}, u32[]{:S(2)}) copy-start(f32[8,32,128]{2,1,0:T(8,128)S(1)} %get-tuple-element.17) | copy-start | bytes 393220
  3.3 32.5 %collective-permute-start.5 = (bf16[32,128,128]{2,1,0:T(8,128)(2,1)}, bf16[32,128,128]{2,1,0:T(8,128)(2,1)S(1)}, u32[]{:S(2)}, u32[]{:S(2)}) collective-permute-start(bf16[32,128,128]{2,1,0:T(8,128)(2,1)} %get-tuple-element.19), channel_id=1, source_target_pairs={{0,1},{1,0},{2,3},{3,2},{4,5},{5,4},{6,7},{7,6},{8,9},{9,8},{10,11... | collective-permute-start | bytes 3145736 | tf_op jit(solution)/shard_map/ppermute | solution.py:480
  5.2 10.2 %collective-permute-start.1 = (bf16[80,2048]{1,0:T(8,128)(2,1)S(1)}, bf16[80,2048]{1,0:T(8,128)(2,1)S(1)}, u32[]{:S(2)}, u32[]{:S(2)}) collective-permute-start(bf16[80,2048]{1,0:T(8,128)(2,1)S(1)} %get-tuple-element.12.p0_ref), channel_id=1, source_target_pairs={{0,2},{2,0},{4,6},{6,4},{8,10},{10,8},{12,14},{14,12},{16,18},{18,... | collective-permute-start | bytes 983048 | tf_op jit(solution)/shard_map/ppermute | solution.py:480
  6.9 16.6 %collective-permute-start = (bf16[80,2048]{1,0:T(8,128)(2,1)S(1)}, bf16[80,2048]{1,0:T(8,128)(2,1)}, u32[]{:S(2)}, u32[]{:S(2)}) collective-permute-start(bf16[80,2048]{1,0:T(8,128)(2,1)S(1)} %get-tuple-element.12.p0_ref), channel_id=1, source_target_pairs={{0,1},{1,0},{2,3},{3,2},{4,5},{5,4},{6,7},{7,6},{8,9},{9,8},{10,11... | collective-permute-start | bytes 983048 | tf_op jit(solution)/shard_map/ppermute | solution.py:480
  7.1 28.6 %collective-permute-start.3 = (bf16[128,2048]{1,0:T(8,128)(2,1)}, bf16[128,2048]{1,0:T(8,128)(2,1)}, u32[]{:S(2)}, u32[]{:S(2)}) collective-permute-start(bf16[128,2048]{1,0:T(8,128)(2,1)} %own_hbm.1), channel_id=1, source_target_pairs={{0,1},{1,0},{2,3},{3,2},{4,5},{5,4},{6,7},{7,6},{8,9},{9,8},{10,11... | collective-permute-start | bytes 1572872 | tf_op jit(solution)/shard_map/ppermute | solution.py:480
  7.4 28.3 %collective-permute-start.6 = (bf16[2048,128]{1,0:T(8,128)(2,1)}, bf16[2048,128]{1,0:T(8,128)(2,1)S(1)}, u32[]{:S(2)}, u32[]{:S(2)}) collective-permute-start(bf16[2048,128]{1,0:T(8,128)(2,1)} %inner_hbm.1), channel_id=1, source_target_pairs={{0,1},{1,0},{2,3},{3,2},{4,5},{5,4},{6,7},{7,6},{8,9},{9,8},{10,11... | collective-permute-start | bytes 1572872 | tf_op jit(solution)/shard_map/ppermute | solution.py:480
  15.3 20.4 %collective-permute-start.7 = (bf16[2048,128]{1,0:T(8,128)(2,1)}, bf16[2048,128]{1,0:T(8,128)(2,1)S(1)}, u32[]{:S(2)}, u32[]{:S(2)}) collective-permute-start(bf16[2048,128]{1,0:T(8,128)(2,1)} %gate_hbm.1), channel_id=1, source_target_pairs={{0,1},{1,0},{2,3},{3,2},{4,5},{5,4},{6,7},{7,6},{8,9},{9,8},{10,11... | collective-permute-start | bytes 1572872 | tf_op jit(solution)/shard_map/ppermute | solution.py:480
  15.4 20.4 %all-to-all-start = ((bf16[16,8,2048]{2,1,0:T(8,128)(2,1)}), bf16[16,8,2048]{2,1,0:T(8,128)(2,1)S(1)}, u32[]{:S(2)}, u32[]{:S(2)}) async-start(bf16[16,8,2048]{2,1,0:T(8,128)(2,1)} %get-tuple-element.11), calls=%async_computation | async-start | bytes 1048576 | tf_op jit(solution)/shard_map/all_to_all | solution.py:541
  23.5 1.7 %collective-permute-start.2 = (bf16[80,2048]{1,0:T(8,128)(2,1)S(1)}, bf16[80,2048]{1,0:T(8,128)(2,1)S(1)}, u32[]{:S(2)}, u32[]{:S(2)}) collective-permute-start(bf16[80,2048]{1,0:T(8,128)(2,1)S(1)} %collective-permute-done.1.p2_ref), channel_id=1, source_target_pairs={{0,1},{1,0},{2,3},{3,2},{4,5},{5,4},{6,7},{7,6},{8,9},{9,8},{10,11... | collective-permute-start | bytes 983048 | tf_op jit(solution)/shard_map/ppermute | solution.py:480
  25.3 3.4 %collective-permute-start.4 = (f32[8,32,128]{2,1,0:T(8,128)}, f32[8,32,128]{2,1,0:T(8,128)}, u32[]{:S(2)}, u32[]{:S(2)}) collective-permute-start(f32[8,32,128]{2,1,0:T(8,128)} %copy-done.2), channel_id=1, source_target_pairs={{0,1},{1,0},{2,3},{3,2},{4,5},{5,4},{6,7},{7,6},{8,9},{9,8},{10,11... | collective-permute-start | bytes 393224 | tf_op jit(solution)/shard_map/ppermute | solution.py:480
  25.5 0.8 %copy-start.1 = (f32[64,128]{1,0:T(8,128)S(1)}, f32[64,128]{1,0:T(8,128)}, u32[]{:S(2)}) copy-start(f32[64,128]{1,0:T(8,128)} %copy-done) | copy-start | bytes 98308
  40.8 15.0 %all-to-all-start.1 = ((bf16[16,8,2176]{2,1,0:T(8,128)(2,1)}), bf16[16,8,2176]{2,1,0:T(8,128)(2,1)S(1)}, u32[]{:S(2)}, u32[]{:S(2)}) async-start(bf16[16,8,2176]{2,1,0:T(8,128)(2,1)} %bitcast.19), calls=%async_computation.1 | async-start | bytes 1114112 | tf_op jit(solution)/shard_map/all_to_all | solution.py:661

commit v4 on v3

--- a/solution.py
+++ b/solution.py
@@ -34,7 +34,7 @@
 
 
 def begin_kernel(
-    tok_hbm, w_hbm, r_hbm, wh_hbm, rh_hbm, all_hbm, out_ref, tok_s, wh_s, rh_s, sems, sent
+    tok_hbm, w_hbm, r_hbm, wh_hbm, rh_hbm, all_hbm, out_ref, hist_ref, tok_s, wh_s, rh_s, sems, sent
 ):
     copies = fetch(
         (
@@ -55,6 +55,7 @@
         out_ref[64:80, t * 128 : (t + 1) * 128] = both[0:16]
         out_ref[64:80, (7 + t) * 128 : (8 + t) * 128] = both[16:32]
     out_ref[64:80, 1792:2048] = jnp.zeros((16, 256), bf16)
+    hist_ref[...] = out_ref[64:80, :]
     for copy in copies[3:] + out:
         copy.wait()
 
@@ -206,17 +207,14 @@
         copy.wait()
 
 
-def group_kernel(p0_ref, p1_ref, p2_ref, p3_ref, acc_ref, vec_ref, wall_hbm, mix_hbm, wall_s, mix_s, hist_s, sems):
+def group_kernel(own_ref, twin_ref, near_ref, far_ref, acc_ref, vec_ref, mix_s, hist_s):
     member = device_rank() & 3
-    for x, p in enumerate((p0_ref, p1_ref, p2_ref, p3_ref)):
+    pieces = (own_ref.at[64:80], twin_ref.at[64:80], near_ref, far_ref)
+    for x, p in enumerate(pieces):
         at = pl.multiple_of((member ^ x) * 32, 32)
-        wall_s[pl.ds(at, 32), :] = p[0:32, :]
-        wall_s[pl.ds(128 + at, 32), :] = p[32:64, :]
         for t in range(7):
-            hist_s[t, pl.ds(at, 16), :] = p[64:80, t * 128 : (t + 1) * 128].astype(f32)
-            hist_s[t, pl.ds(at + 16, 16), :] = p[64:80, (7 + t) * 128 : (8 + t) * 128].astype(f32)
-    copy = pltpu.make_async_copy(wall_s, wall_hbm, sems.at[0])
-    copy.start()
+            hist_s[t, pl.ds(at, 16), :] = p[:, t * 128 : (t + 1) * 128].astype(f32)
+            hist_s[t, pl.ds(at + 16, 16), :] = p[:, (7 + t) * 128 : (8 + t) * 128].astype(f32)
     both = [hist_s[t].T for t in range(7)]
     acc = acc_ref[...]
     acc2 = jnp.concatenate([acc, acc], axis=0)
@@ -236,34 +234,28 @@
     for t in range(4):
         w_old = silu(sum(vec_ref[4 + k : 5 + k, :] * both[t + k][0:64] for k in range(4)))
         mix_s[6 + t] = w_old.astype(bf16).astype(f32)
-    last = pltpu.make_async_copy(mix_s, mix_hbm, sems.at[1])
-    last.start()
-    copy.wait()
-    last.wait()
 
 
 def state_kernel(
-    saved_hbm, mix_hbm, after_hbm, held_s, base_hbm, saved_s, base_s, mix_s, sems, sent
+    saved_hbm, after_hbm, held_s, mix_s, base_hbm, saved_s, base_s, sems, sent
 ):
     blocks = [slice(k * 8, (k + 1) * 8) for k in range(8)]
-    copies = fetch(
-        [(saved_hbm.at[k], saved_s.at[k]) for k in blocks]
-        + [(mix_hbm.at[6:10], mix_s)],
-        sems,
-    )
-    copies[8].wait()
+    copies = fetch([(saved_hbm.at[k], saved_s.at[k]) for k in blocks], sems)
     tot = jnp.concatenate([held_s[7], held_s[7]], axis=0).T
     at = jnp.concatenate(
         [jnp.concatenate([held_s[2 * p], held_s[2 * p + 1]], axis=0).T for p in range(2)], axis=1
     ).astype(bf16)
-    b = mix_s[...].reshape(256, 128).astype(bf16)
+    b = mix_s[6:10].reshape(256, 128).astype(bf16)
     lane = lax.broadcasted_iota(jnp.int32, (1, 256), 1) & 63
     out = []
     for k in range(8):
         copies[k].wait()
-        for s in range(k * 8, (k + 1) * 8):
-            mask = (lane == s).astype(f32).astype(bf16)
-            base_s[s] = saved_s[s] * tot[:, s : s + 1] + dot(at * mask, b)
+        for first in range(k * 8, (k + 1) * 8, 4):
+            parts = [at * (lane == first + q).astype(f32).astype(bf16) for q in range(4)]
+            new = dot(jnp.concatenate(parts, axis=0), b)
+            for q in range(4):
+                s = first + q
+                base_s[s] = saved_s[s] * tot[:, s : s + 1] + new[q * 128 : (q + 1) * 128]
         copy = pltpu.make_async_copy(base_s.at[blocks[k]], base_hbm.at[blocks[k]], sent.at[k])
         copy.start()
         out.append(copy)
@@ -275,53 +267,51 @@
     return v.astype(bf16).astype(f32)
 
 
-def main_kernel(
-    mine_ref,
-    norm_hbm,
-    wall_hbm,
+def norm_kernel(mine_ref, norm_ref, own_ref, twin_ref, nrm_ref, rows_ref, wall_s):
+    core = lax.axis_index("tp")
+    for c, p in ((core, own_ref), (1 - core, twin_ref)):
+        at = pl.multiple_of(c * 32, 32)
+        wall_s[pl.ds(at, 32), :] = p[0:32, :]
+        wall_s[pl.ds(64 + at, 32), :] = p[32:64, :]
+    gain = norm_ref[...]
+    for k in range(8):
+        x = mine_ref[2 * k : 2 * k + 2].astype(f32).reshape(16, 2048)
+        scale = lax.rsqrt(jnp.mean(x * x, axis=-1, keepdims=True) + EPSILON)
+        nrm_ref[k * 16 : (k + 1) * 16, :] = (x * scale * gain).astype(bf16)
+    rows_ref[...] = dot(nrm_ref[...], wall_s[...], NT).astype(bf16)
+
+
+def rows_kernel(
+    nrm_ref,
     step_hbm,
     inner_hbm,
     gate_hbm,
-    mix_hbm,
-    saved_hbm,
+    twin_inner_hbm,
+    twin_gate_hbm,
     own_hbm,
     twin_own_hbm,
-    got_hbm,
-    held_s,
-    twin_low_ref,
-    twin_inner_ref,
-    twin_gate_ref,
-    vec_ref,
-    out_hbm,
-    norm_s,
-    wall_s,
+    saved_hbm,
+    rows_ref,
+    proj_ref,
+    low_ref,
     step_s,
     inner_s,
     gate_s,
-    mix_s,
-    got_ref,
+    twin_inner_s,
+    twin_gate_s,
     low_s,
-    proj_s,
-    nrm_s,
-    rows_s,
-    read_s,
-    part_s,
-    out_s,
     sems,
-    sent,
 ):
     core = lax.axis_index("tp")
     copies = fetch(
         (
-            (norm_hbm, norm_s),
-            (wall_hbm, wall_s),
             (step_hbm, step_s),
             (inner_hbm, inner_s),
             (gate_hbm, gate_s),
-            (mix_hbm, mix_s),
-            (got_hbm, got_ref),
-            (own_hbm, proj_s.at[0]),
-            (twin_own_hbm, proj_s.at[1]),
+            (twin_inner_hbm, twin_inner_s),
+            (twin_gate_hbm, twin_gate_s),
+            (own_hbm, proj_ref.at[0]),
+            (twin_own_hbm, proj_ref.at[1]),
         )
         + tuple(
             (saved_hbm.at[pl.ds(kv * 4 + core * 2, 2)], low_s.at[kv * 2 : kv * 2 + 2])
@@ -329,22 +319,13 @@
         ),
         sems,
     )
-    copies[0].wait()
-    gain = norm_s[...]
-    for k in range(8):
-        x = mine_ref[2 * k : 2 * k + 2].astype(f32).reshape(16, 2048)
-        scale = lax.rsqrt(jnp.mean(x * x, axis=-1, keepdims=True) + EPSILON)
-        nrm_s[k * 16 : (k + 1) * 16, :] = (x * scale * gain).astype(bf16)
-    normed = nrm_s[...]
-    for copy in copies[1:5]:
+    normed = nrm_ref[...]
+    for copy in copies[0:5]:
         copy.wait()
-    both = rounded(dot(normed, wall_s[...], NT))
-    rows_s[2] = both[:, 0:128]
-    rows_s[3] = both[:, 128:256]
-    weights = [inner_s[...], twin_inner_ref[...], gate_s[...], twin_gate_ref[...]]
+    weights = [inner_s[...], twin_inner_s[...], gate_s[...], twin_gate_s[...]]
     both = rounded(dot(normed, jnp.concatenate(weights, axis=1)))
     for k in range(4):
-        rows_s[4 + k] = both[:, k * 128 : (k + 1) * 128]
+        rows_ref[2 + k] = both[:, k * 128 : (k + 1) * 128]
     both = dot(normed, step_s[...], NT)
     lane = lax.broadcasted_iota(jnp.int32, (64, 256), 1)
     head = (device_rank() ^ (lane >> 7)) * 2 + ((lane >> 6) & 1)
@@ -355,10 +336,40 @@
     mid = rest.astype(bf16)
     low = (rest - mid.astype(f32)).astype(bf16)
     both = dot(high, pick) + (dot(mid, pick) + dot(low, pick))
-    rows_s[0] = both[:, 0:128]
-    rows_s[1] = both[:, 128:256]
+    rows_ref[0] = both[:, 0:128]
+    rows_ref[1] = both[:, 128:256]
     for copy in copies[5:]:
         copy.wait()
+    low_ref[...] = low_s[...].astype(bf16)
+
+
+def main_kernel(
+    own_rows_ref,
+    near_rows_ref,
+    rows_s,
+    mix_s,
+    got_ref,
+    proj_s,
+    low_s,
+    held_s,
+    twin_low_ref,
+    vec_ref,
+    out_hbm,
+    pair_s,
+    read_s,
+    part_s,
+    out_s,
+    sent,
+):
+    core = lax.axis_index("tp")
+    lower = (lax.axis_index("kv") & 1) == 0
+    half = lax.broadcasted_iota(jnp.int32, (128, 128), 1) < 64
+    own = own_rows_ref[...].astype(f32)
+    near = near_rows_ref[...].astype(f32)
+    left = jnp.where(lower, own, near)
+    right = jnp.where(lower, near, own)
+    pair_s[0] = jnp.where(half, left, pltpu.roll(right, 64, 1))
+    pair_s[1] = jnp.where(half, pltpu.roll(left, 64, 1), right)
 
     def at_time(ref, t, k):
         return jnp.concatenate([ref[k, pl.ds(q * 4 + t, 16, stride=8), :] for q in range(2)], axis=0)
@@ -385,11 +396,11 @@
         return [vec_ref[first + k : first + k + 1, :] for k in range(4)]
 
     def mixing(k, base, taps):
-        new = [at_time(rows_s, t, k) for t in range(4)]
+        new = [at_time(pair_s, t, k) for t in range(4)]
         return [rounded(v) for v in conv_new(new, [chosen(mix_s, base + i) for i in range(3)], taps)]
 
-    write = mixing(2, 0, taps_of(4))
-    read = mixing(3, 3, taps_of(8))
+    write = mixing(0, 0, taps_of(4))
+    read = mixing(1, 3, taps_of(8))
     for t in range(4):
         put(read_s, t, 0, read[t])
 
@@ -409,7 +420,7 @@
             parts = [got_ref[4 + t] for t in range(3)]
             tot = got_ref[7]
         inner = conv_new(
-            [at_time(rows_s, t, 4 + p) for t in range(4)], parts, taps_of(16 if p else 0)
+            [at_time(rows_s, t, 2 + p) for t in range(4)], parts, taps_of(16 if p else 0)
         )
         first = 20 if p else 12
         rate, skip, bias = (vec_ref[first + k : first + k + 1, :] for k in range(3))
@@ -429,7 +440,7 @@
             y = decay * state + skip * inner[i] + scores[i][i] * moved[i]
             for j in range(i):
                 y = y + scores[i][j] * jnp.exp(sums[i] - sums[j]) * moved[j]
-            gate = silu(at_time(rows_s, i, 6 + p))
+            gate = silu(at_time(rows_s, i, 4 + p))
             put(part_s, i, p, y * gate)
             put(part_s, i, 2 + p, decay * tot * gate)
 
@@ -438,7 +449,7 @@
         rows = slice(g * 16, (g + 1) * 16)
         r = read_s[0, rows, :].astype(bf16)
         for p, low in enumerate((low_s, twin_low_ref)):
-            full = dot(r, low[g * 4 : (g + 1) * 4].reshape(512, 128).astype(bf16), NT)
+            full = dot(r, low[g * 4 : (g + 1) * 4].reshape(512, 128), NT)
             v = full[:, 0:128]
             for q in range(1, 4):
                 v = jnp.where(quarter == q, full[:, q * 128 : (q + 1) * 128], v)
@@ -517,11 +528,15 @@
         return jax.ShapeDtypeStruct(dims, kind)
 
     saved = saved_state.reshape(64, 128, 128)
-    sent, pack = pl.pallas_call(
+    sent, pack, hist = pl.pallas_call(
         begin_kernel,
-        out_shape=[pltpu.HBM((16, 8, 2048), bf16), shape(80, 2048, kind=bf16)],
+        out_shape=[
+            pltpu.HBM((16, 8, 2048), bf16),
+            shape(80, 2048, kind=bf16),
+            shape(16, 2048, kind=bf16),
+        ],
         in_specs=[anywhere] * 5,
-        out_specs=[anywhere, whole()],
+        out_specs=[anywhere, whole(), whole()],
         scratch_shapes=[
             pltpu.VMEM((8, 2048), bf16),
             pltpu.VMEM((7, 32, 64), bf16),
@@ -539,9 +554,9 @@
         hbm(read_history.transpose(1, 2, 0)),
     )
     mine = lax.all_to_all(sent, "kv", 0, 0, tiled=True)
-    pack_kv = swapped(pack, "kv")
+    hist_kv = swapped(hist, "kv")
     pack_tp = swapped(pack, "tp")
-    pack_both = swapped(pack_kv, "tp")
+    hist_both = swapped(hist_kv, "tp")
     gate_other = swapped(gate_proj, "tp")
     inner_other = swapped(inner_proj, "tp")
     out_other = swapped(out_proj, "tp")
@@ -593,87 +608,94 @@
             )
         ]
     )
-    wall, mix = pl.pallas_call(
+    mix = pl.pallas_call(
         group_kernel,
         in_specs=[whole()] * 6,
-        out_specs=[anywhere] * 2,
-        out_shape=[pltpu.HBM((256, 2048), bf16), pltpu.HBM((10, 64, 128), f32)],
-        scratch_shapes=[
-            pltpu.VMEM((256, 2048), bf16),
-            pltpu.VMEM((10, 64, 128), f32),
-            pltpu.VMEM((7, 128, 128), f32),
-            dma((2,)),
-        ],
+        out_specs=whole(),
+        out_shape=shape(10, 64, 128),
+        scratch_shapes=[pltpu.VMEM((7, 128, 128), f32)],
         compiler_params=params(6),
         name="group",
-    )(pack, pack_tp, pack_kv, pack_both, acc, vec)
+    )(pack, pack_tp, hist_kv, hist_both, acc, vec)
 
     derived_twin = swapped(derived, "tp")
     low_twin = swapped(give, "tp")
+    normed, own_rows = pl.pallas_call(
+        norm_kernel,
+        in_specs=[whole()] * 4,
+        out_specs=[whole()] * 2,
+        out_shape=[shape(128, 2048, kind=bf16), shape(128, 128, kind=bf16)],
+        scratch_shapes=[pltpu.VMEM((128, 2048), bf16)],
+        compiler_params=params(6),
+        name="norm",
+    )(mine, norm_gain[None, :], pack, pack_tp)
+    near_rows = swapped(own_rows, "kv")
+    rows, proj_v, low_v = pl.pallas_call(
+        rows_kernel,
+        in_specs=[whole()] + [anywhere] * 8,
+        out_specs=[whole()] * 3,
+        out_shape=[
+            shape(6, 128, 128),
+            shape(2, 128, 2048, kind=bf16),
+            shape(32, 128, 128, kind=bf16),
+        ],
+        scratch_shapes=[
+            pltpu.VMEM((64, 2048), bf16),
+            pltpu.VMEM((2048, 128), bf16),
+            pltpu.VMEM((2048, 128), bf16),
+            pltpu.VMEM((2048, 128), bf16),
+            pltpu.VMEM((2048, 128), bf16),
+            pltpu.VMEM((32, 128, 128), f32),
+            dma((23,)),
+        ],
+        compiler_params=params(10),
+        name="rows",
+    )(
+        normed,
+        *[
+            hbm(v)
+            for v in (
+                step_proj.T,
+                inner_proj,
+                gate_proj,
+                inner_other,
+                gate_other,
+                out_proj,
+                out_other,
+                saved,
+            )
+        ],
+    )
     partial = pl.pallas_call(
         main_kernel,
-        in_specs=[whole()] + [anywhere] * 10 + [whole()] * 5,
+        in_specs=[whole()] * 10,
         out_specs=anywhere,
         out_shape=pltpu.HBM((128, 2176), bf16),
         scratch_shapes=[
-            pltpu.VMEM((1, 2048), f32),
-            pltpu.VMEM((256, 2048), bf16),
-            pltpu.VMEM((64, 2048), bf16),
-            pltpu.VMEM((2048, 128), bf16),
-            pltpu.VMEM((2048, 128), bf16),
-            pltpu.VMEM((10, 64, 128), f32),
-            pltpu.VMEM((8, 32, 128), f32),
-            pltpu.VMEM((32, 128, 128), f32),
-            pltpu.VMEM((2, 128, 2048), bf16),
-            pltpu.VMEM((128, 2048), bf16),
-            pltpu.VMEM((8, 128, 128), f32),
+            pltpu.VMEM((2, 128, 128), f32),
             pltpu.VMEM((1, 128, 128), f32),
             pltpu.VMEM((4, 128, 128), f32),
             pltpu.VMEM((128, 2176), bf16),
-            dma((25,)),
             dma((4,)),
         ],
-        compiler_params=params(12),
+        compiler_params=params(6),
         name="main",
-    )(
-        mine,
-        *[
-            hbm(v)
-            for v in (
-                norm_gain[None, :],
-                wall,
-                step_proj.T,
-                inner_proj,
-                gate_proj,
-                mix,
-                saved,
-                out_proj,
-                out_other,
-                derived_twin,
-            )
-        ],
-        held,
-        low_twin,
-        inner_other,
-        gate_other,
-        vec,
-    )
+    )(own_rows, near_rows, rows, mix, derived_twin, proj_v, low_v, held, low_twin, vec)
     arrived = lax.all_to_all(partial.reshape(16, 8, 2176), "kv", 0, 0, tiled=True)
     base = pl.pallas_call(
         state_kernel,
-        in_specs=[anywhere] * 3 + [whole()],
+        in_specs=[anywhere] * 2 + [whole()] * 2,
         out_specs=anywhere,
         out_shape=shape(64, 128, 128),
         scratch_shapes=[
             pltpu.VMEM((64, 128, 128), f32),
             pltpu.VMEM((64, 128, 128), f32),
-            pltpu.VMEM((4, 64, 128), f32),
-            dma((9,)),
+            dma((8,)),
             dma((8,)),
         ],
         compiler_params=params(12),
         name="state",
-    )(hbm(saved), hbm(mix), hbm(partial), held)
+    )(hbm(saved), hbm(partial), held, mix)
     mixed = pl.pallas_call(
         sum_kernel,
         in_specs=[whole()],

time: 56.9 us -> 49 us (0.86)
  waiting for transfers between devices: 22 us -> 17.7 us
  Pallas kernels: 18.1 us -> 15.2 us
  local copies, waits for them, and re-layouts: 0.77 us -> 0.01 us
    ppermute x8 -> x9, waiting for transfers between devices: 9.13 us -> 4.12 us  [swapped(): lax.ppermute(value, axis, [(k, k ^ 1) for k in range(lax.axis_size(axis))])]
    pallas_call x3 -> x5, Pallas kernels: 13 us -> 10.1 us  [the longest x1 4.47 us: body(): pl.pallas_call(state_kernel, in_specs=[anywhere] * 2 + [whole()] * 2, out...]
    unnamed x6 -> x2, local copies, waits for them, and re-layouts: 0.77 us -> 0.01 us
    all_to_all x1, waiting for transfers between devices: 5.78 us -> 6.44 us  [body(): lax.all_to_all(partial.reshape(16, 8, 2176), 'kv', 0, 0, tiled=True)]
    ppermute x8 -> x9, starting transfers between devices: 3.08 us -> 3.66 us  [swapped(): lax.ppermute(value, axis, [(k, k ^ 1) for k in range(lax.axis_size(axis))])]
  transfers between devices with their start and end apart: 10 -> 11, of which waited for: 4 -> 5; matrix products, arithmetic and copies ran while one was open for 0% -> 0% of each run, Pallas kernels for 17% -> 20%
where the time goes in v4:
time: 49 us; the launch traced here: 48.7 us
  waiting for transfers between devices  17.7 us (36%)
  Pallas kernels  15.2 us (31%)
  starting transfers between devices  15 us (31%)
  between operations  0.76 us (2%)
    all_to_all x1, starting transfers between devices, body(): mine = lax.all_to_all(sent, 'kv', 0, 0, tiled=True)  7.75 us
    all_to_all x1, waiting for transfers between devices, body(): mine = lax.all_to_all(sent, 'kv', 0, 0, tiled=True)  7.15 us
    all_to_all x1, waiting for transfers between devices, body(): lax.all_to_all(partial.reshape(16, 8, 2176), 'kv', 0, 0, tiled=True)  6.44 us
    pallas_call x1, Pallas kernels, body(): pl.pallas_call(state_kernel, in_specs=[anywhere] * 2 + [whole()] * 2, out...  4.47 us
    ppermute x9, waiting for transfers between devices, swapped(): lax.ppermute(value, axis, [(k, k ^ 1) for k in range(lax.axis_size(axis))])  4.12 us
    ppermute x9, starting transfers between devices, swapped(): lax.ppermute(value, axis, [(k, k ^ 1) for k in range(lax.axis_size(axis))])  3.66 us
    all_to_all x1, starting transfers between devices, body(): lax.all_to_all(partial.reshape(16, 8, 2176), 'kv', 0, 0, tiled=True)  3.59 us
    pallas_call x1, Pallas kernels, body(): pl.pallas_call(rows_kernel, in_specs=[whole()] + [anywhere] * 8, out_spec...  2.83 us
  transfers between devices with their start and end apart: 11, of which 5 were waited for; matrix products, arithmetic and copies ran while one was open for 0% of the time, Pallas kernels for 20%

profile of v4, /device:TPU:0, one launch (start us, length us, event | category | flops | bytes accessed | tf_op | source)
XLA Modules:
  0.0 48.7 jit_solution(15315681554726668162)
XLA Ops:
  0.6 0.0 copy-start
  0.6 2.6 %prep.1 = (bf16[32,128,128]{2,1,0:T(8,128)(2,1)}, f32[8,64,128]{2,1,0:T(8,128)S(1)}, f32[64,128]{1,0:T(8,128)S(1)}, f32[24,128]{1,0:T(8,128)S(1)}, f32[8,32,128]{2,1,0:T(8,128)S(1)}) custom-call(f32[64,128,128]{2,1,0:T(8,128)} %bitcast.17, bf16[7,64,128]{2,1,0:T(8,128)(2,1)} %bitcast.25, bf16[4,4096]{1,0:T(4,128)(2,1)} %tin_hbm.1, bf16[4,1024]{1,0:T(4,128)(2,1)} %tw_hbm.1, ...), custom_call_target="tpu_custom_call" | custom-call | tf_op jit(solution)/shard_map/prep/pallas_call | solution.py:564
  3.3 0.1 collective-permute-start.8
  3.4 1.7 %begin.1 = (bf16[16,8,2048]{2,1,0:T(8,128)(2,1)}, bf16[80,2048]{1,0:T(8,128)(2,1)S(1)}, bf16[16,2048]{1,0:T(8,128)(2,1)S(1)}) custom-call(bf16[8,2048]{1,0:T(8,128)(2,1)} %tok_hbm.1, bf16[32,2048]{1,0:T(8,128)(2,1)} %bitcast.23, bf16[32,2048]{1,0:T(8,128)(2,1)} %bitcast.24, bf16[7,32,64]{2,1,0:T(8,128)(2,1)} %bitcast.26, bf16[7,32,64]{2,1,0:T(8,128)(2,1)} %bitcast.27), custom_call_target="tpu_custom_call" | custom-call | tf_op jit(solution)/shard_map/begin/pallas_call | solution.py:531
  5.1 1.8 %collective-permute-start.5 = (bf16[16,2048]{1,0:T(8,128)(2,1)S(1)}, bf16[16,2048]{1,0:T(8,128)(2,1)S(1)}, u32[]{:S(2)}, u32[]{:S(2)}) collective-permute-start(bf16[16,2048]{1,0:T(8,128)(2,1)S(1)} %get-tuple-element.20), channel_id=1, source_target_pairs={{0,2},{2,0},{4,6},{6,4},{8,10},{10,8},{12,14},{14,12},{16,18},{18,... | collective-permute-start | bytes 196616 | tf_op jit(solution)/shard_map/ppermute | solution.py:491
  6.9 0.2 collective-permute-start.2
  7.1 7.8 %all-to-all-start = ((bf16[16,8,2048]{2,1,0:T(8,128)(2,1)}), bf16[16,8,2048]{2,1,0:T(8,128)(2,1)S(1)}, u32[]{:S(2)}, u32[]{:S(2)}) async-start(bf16[16,8,2048]{2,1,0:T(8,128)(2,1)} %get-tuple-element.15), calls=%async_computation | async-start | bytes 1048576 | tf_op jit(solution)/shard_map/all_to_all | solution.py:556
  14.9 0.1 collective-permute-start.3
  15.0 0.5 %collective-permute-start.4 = (bf16[128,2048]{1,0:T(8,128)(2,1)}, bf16[128,2048]{1,0:T(8,128)(2,1)}, u32[]{:S(2)}, u32[]{:S(2)}) collective-permute-start(bf16[128,2048]{1,0:T(8,128)(2,1)} %own_hbm.1), channel_id=1, source_target_pairs={{0,1},{1,0},{2,3},{3,2},{4,5},{5,4},{6,7},{7,6},{8,9},{9,8},{10,11... | collective-permute-start | bytes 1572872 | tf_op jit(solution)/shard_map/ppermute | solution.py:491
  15.4 0.0 collective-permute-done.5.near_ref
  15.4 0.1 collective-permute-start.6
  15.5 2.4 %collective-permute-done.6.far_ref = bf16[16,2048]{1,0:T(8,128)(2,1)S(1)} collective-permute-done((bf16[16,2048]{1,0:T(8,128)(2,1)S(1)}, bf16[16,2048]{1,0:T(8,128)(2,1)S(1)}, u32[]{:S(2)}, u32[]{:S(2)}) %collective-permute-start.6) | collective-permute-done | bytes 65568 | tf_op jit(solution)/shard_map/ppermute | solution.py:491
  17.9 0.1 collective-permute-start
  18.1 1.5 %collective-permute-done.twin_ref = bf16[80,2048]{1,0:T(8,128)(2,1)S(1)} collective-permute-done((bf16[80,2048]{1,0:T(8,128)(2,1)S(1)}, bf16[80,2048]{1,0:T(8,128)(2,1)S(1)}, u32[]{:S(2)}, u32[]{:S(2)}) %collective-permute-start) | collective-permute-done | bytes 327712 | tf_op jit(solution)/shard_map/ppermute | solution.py:491
  19.6 0.1 collective-permute-start.7
  19.7 7.1 %all-to-all-done.mine_ref = bf16[16,8,2048]{2,1,0:T(8,128)(2,1)S(1)} async-done(((bf16[16,8,2048]{2,1,0:T(8,128)(2,1)}), bf16[16,8,2048]{2,1,0:T(8,128)(2,1)S(1)}, u32[]{:S(2)}, u32[]{:S(2)}) %all-to-all-start) | async-done | bytes 524320 | tf_op jit(solution)/shard_map/all_to_all | solution.py:556
  26.9 0.0 copy-done
  26.9 0.5 %norm.1 = (bf16[128,2048]{1,0:T(8,128)(2,1)S(1)}, bf16[128,128]{1,0:T(8,128)(2,1)S(1)}) custom-call(bf16[16,8,2048]{2,1,0:T(8,128)(2,1)S(1)} %all-to-all-done.mine_ref, f32[1,2048]{1,0:T(1,128)S(1)} %bitcast.16, bf16[80,2048]{1,0:T(8,128)(2,1)S(1)} %get-tuple-element.16.own_ref, bf16[80,2048]{1,0:T(8,128)(2,1)S(1)} %collective-permute-done.twin_ref), custom_call_target="tpu_custom_call" | custom-call | tf_op jit(solution)/shard_map/norm/pallas_call | solution.py:623
  27.4 0.0 collective-permute-done.2.twin_inner_hbm
  27.4 0.6 %collective-permute-start.1 = (bf16[128,128]{1,0:T(8,128)(2,1)S(1)}, bf16[128,128]{1,0:T(8,128)(2,1)S(1)}, u32[]{:S(2)}, u32[]{:S(2)}) collective-permute-start(bf16[128,128]{1,0:T(8,128)(2,1)S(1)} %get-tuple-element.17.own_rows_ref), channel_id=1, source_target_pairs={{0,2},{2,0},{4,6},{6,4},{8,10},{10,8},{12,14},{14,12},{16,18},{18,... | collective-permute-start | bytes 98312 | tf_op jit(solution)/shard_map/ppermute | solution.py:491
  28.0 0.3 group.1.mix_s
  28.3 0.0 collective-permute-done.3.twin_gate_hbm
  28.3 0.0 collective-permute-done.4.twin_own_hbm
  28.3 2.8 %rows.1 = (f32[6,128,128]{2,1,0:T(8,128)S(1)}, bf16[2,128,2048]{2,1,0:T(8,128)(2,1)S(1)}, bf16[32,128,128]{2,1,0:T(8,128)(2,1)S(1)}) custom-call(bf16[128,2048]{1,0:T(8,128)(2,1)S(1)} %get-tuple-element.18.nrm_ref, bf16[64,2048]{1,0:T(8,128)(2,1)} %bitcast.22, bf16[2048,128]{1,0:T(8,128)(2,1)} %inner_hbm.1, bf16[2048,128]{1,0:T(8,128)(2,1)} %gate_hbm.1, ...), custom_call_target="tpu_custom_call" | custom-call | tf_op jit(solution)/shard_map/rows/pallas_call | solution.py:633
  31.2 0.0 collective-permute-done.7.got_ref
  31.2 0.2 collective-permute-done.1.near_rows_ref
  31.4 0.0 collective-permute-done.8.twin_low_ref
  31.4 2.0 %main.1.after_hbm = bf16[128,2176]{1,0:T(8,128)(2,1)} custom-call(bf16[128,128]{1,0:T(8,128)(2,1)S(1)} %get-tuple-element.17.own_rows_ref, bf16[128,128]{1,0:T(8,128)(2,1)S(1)} %collective-permute-done.1.near_rows_ref, f32[6,128,128]{2,1,0:T(8,128)S(1)} %get-tuple-element.19.rows_s, f32[10,64,128]{2,1,0:T(8,128)S(1)} %group.1.mix_s, ...), custom_call_target="tpu_custom_call" | custom-call | tf_op jit(solution)/shard_map/main/pallas_call | solution.py:669
  33.4 3.6 %all-to-all-start.1 = ((bf16[16,8,2176]{2,1,0:T(8,128)(2,1)}), bf16[16,8,2176]{2,1,0:T(8,128)(2,1)S(1)}, u32[]{:S(2)}, u32[]{:S(2)}) async-start(bf16[16,8,2176]{2,1,0:T(8,128)(2,1)} %bitcast.20), calls=%async_computation.1 | async-start | bytes 1114112 | tf_op jit(solution)/shard_map/all_to_all | solution.py:684
  37.0 4.5 %state.1 = f32[64,128,128]{2,1,0:T(8,128)} custom-call(f32[64,128,128]{2,1,0:T(8,128)} %bitcast.19, bf16[128,2176]{1,0:T(8,128)(2,1)} %main.1.after_hbm, f32[8,64,128]{2,1,0:T(8,128)S(1)} %get-tuple-element.26.held_s, f32[10,64,128]{2,1,0:T(8,128)S(1)} %group.1.mix_s), custom_call_target="tpu_custom_call" | custom-call | tf_op jit(solution)/shard_map/state/pallas_call | solution.py:685
  41.5 6.4 %all-to-all-done.1.in_ref = bf16[16,8,2176]{2,1,0:T(8,128)(2,1)S(1)} async-done(((bf16[16,8,2176]{2,1,0:T(8,128)(2,1)}), bf16[16,8,2176]{2,1,0:T(8,128)(2,1)S(1)}, u32[]{:S(2)}, u32[]{:S(2)}) %all-to-all-start.1) | async-done | bytes 557088 | tf_op jit(solution)/shard_map/all_to_all | solution.py:684
  47.9 0.7 %total.1 = bf16[8,2048]{1,0:T(8,128)(2,1)} custom-call(bf16[16,8,2176]{2,1,0:T(8,128)(2,1)S(1)} %all-to-all-done.1.in_ref), custom_call_target="tpu_custom_call" | custom-call | tf_op jit(solution)/shard_map/total/pallas_call | solution.py:699
Async XLA Ops:
  0.6 26.2 %copy-start = (f32[2048]{0:T(1024)S(1)}, f32[2048]{0:T(1024)}, u32[]{:S(2)}) copy-start(f32[2048]{0:T(1024)} %param.22) | copy-start | bytes 24580
  3.3 28.1 %collective-permute-start.8 = (bf16[32,128,128]{2,1,0:T(8,128)(2,1)}, bf16[32,128,128]{2,1,0:T(8,128)(2,1)S(1)}, u32[]{:S(2)}, u32[]{:S(2)}) collective-permute-start(bf16[32,128,128]{2,1,0:T(8,128)(2,1)} %get-tuple-element.27), channel_id=1, source_target_pairs={{0,1},{1,0},{2,3},{3,2},{4,5},{5,4},{6,7},{7,6},{8,9},{9,8},{10,11... | collective-permute-start | bytes 3145736 | tf_op jit(solution)/shard_map/ppermute | solution.py:491
  5.1 10.3 %collective-permute-start.5 = (bf16[16,2048]{1,0:T(8,128)(2,1)S(1)}, bf16[16,2048]{1,0:T(8,128)(2,1)S(1)}, u32[]{:S(2)}, u32[]{:S(2)}) collective-permute-start(bf16[16,2048]{1,0:T(8,128)(2,1)S(1)} %get-tuple-element.20), channel_id=1, source_target_pairs={{0,2},{2,0},{4,6},{6,4},{8,10},{10,8},{12,14},{14,12},{16,18},{18,... | collective-permute-start | bytes 196616 | tf_op jit(solution)/shard_map/ppermute | solution.py:491
  6.9 20.5 %collective-permute-start.2 = (bf16[2048,128]{1,0:T(8,128)(2,1)}, bf16[2048,128]{1,0:T(8,128)(2,1)}, u32[]{:S(2)}, u32[]{:S(2)}) collective-permute-start(bf16[2048,128]{1,0:T(8,128)(2,1)} %inner_hbm.1), channel_id=1, source_target_pairs={{0,1},{1,0},{2,3},{3,2},{4,5},{5,4},{6,7},{7,6},{8,9},{9,8},{10,11... | collective-permute-start | bytes 1572872 | tf_op jit(solution)/shard_map/ppermute | solution.py:491
  7.1 19.8 %all-to-all-start = ((bf16[16,8,2048]{2,1,0:T(8,128)(2,1)}), bf16[16,8,2048]{2,1,0:T(8,128)(2,1)S(1)}, u32[]{:S(2)}, u32[]{:S(2)}) async-start(bf16[16,8,2048]{2,1,0:T(8,128)(2,1)} %get-tuple-element.15), calls=%async_computation | async-start | bytes 1048576 | tf_op jit(solution)/shard_map/all_to_all | solution.py:556
  14.9 13.4 %collective-permute-start.3 = (bf16[2048,128]{1,0:T(8,128)(2,1)}, bf16[2048,128]{1,0:T(8,128)(2,1)}, u32[]{:S(2)}, u32[]{:S(2)}) collective-permute-start(bf16[2048,128]{1,0:T(8,128)(2,1)} %gate_hbm.1), channel_id=1, source_target_pairs={{0,1},{1,0},{2,3},{3,2},{4,5},{5,4},{6,7},{7,6},{8,9},{9,8},{10,11... | collective-permute-start | bytes 1572872 | tf_op jit(solution)/shard_map/ppermute | solution.py:491
  15.0 13.4 %collective-permute-start.4 = (bf16[128,2048]{1,0:T(8,128)(2,1)}, bf16[128,2048]{1,0:T(8,128)(2,1)}, u32[]{:S(2)}, u32[]{:S(2)}) collective-permute-start(bf16[128,2048]{1,0:T(8,128)(2,1)} %own_hbm.1), channel_id=1, source_target_pairs={{0,1},{1,0},{2,3},{3,2},{4,5},{5,4},{6,7},{7,6},{8,9},{9,8},{10,11... | collective-permute-start | bytes 1572872 | tf_op jit(solution)/shard_map/ppermute | solution.py:491
  15.4 2.5 %collective-permute-start.6 = (bf16[16,2048]{1,0:T(8,128)(2,1)S(1)}, bf16[16,2048]{1,0:T(8,128)(2,1)S(1)}, u32[]{:S(2)}, u32[]{:S(2)}) collective-permute-start(bf16[16,2048]{1,0:T(8,128)(2,1)S(1)} %collective-permute-done.5.near_ref), channel_id=1, source_target_pairs={{0,1},{1,0},{2,3},{3,2},{4,5},{5,4},{6,7},{7,6},{8,9},{9,8},{10,11... | collective-permute-start | bytes 196616 | tf_op jit(solution)/shard_map/ppermute | solution.py:491
  17.9 1.6 %collective-permute-start = (bf16[80,2048]{1,0:T(8,128)(2,1)S(1)}, bf16[80,2048]{1,0:T(8,128)(2,1)S(1)}, u32[]{:S(2)}, u32[]{:S(2)}) collective-permute-start(bf16[80,2048]{1,0:T(8,128)(2,1)S(1)} %get-tuple-element.16.own_ref), channel_id=1, source_target_pairs={{0,1},{1,0},{2,3},{3,2},{4,5},{5,4},{6,7},{7,6},{8,9},{9,8},{10,11... | collective-permute-start | bytes 983048 | tf_op jit(solution)/shard_map/ppermute | solution.py:491
  19.6 11.6 %collective-permute-start.7 = (f32[8,32,128]{2,1,0:T(8,128)S(1)}, f32[8,32,128]{2,1,0:T(8,128)S(1)}, u32[]{:S(2)}, u32[]{:S(2)}) collective-permute-start(f32[8,32,128]{2,1,0:T(8,128)S(1)} %get-tuple-element.23), channel_id=1, source_target_pairs={{0,1},{1,0},{2,3},{3,2},{4,5},{5,4},{6,7},{7,6},{8,9},{9,8},{10,11... | collective-permute-start | bytes 393224 | tf_op jit(solution)/shard_map/ppermute | solution.py:491
  27.4 4.0 %collective-permute-start.1 = (bf16[128,128]{1,0:T(8,128)(2,1)S(1)}, bf16[128,128]{1,0:T(8,128)(2,1)S(1)}, u32[]{:S(2)}, u32[]{:S(2)}) collective-permute-start(bf16[128,128]{1,0:T(8,128)(2,1)S(1)} %get-tuple-element.17.own_rows_ref), channel_id=1, source_target_pairs={{0,2},{2,0},{4,6},{6,4},{8,10},{10,8},{12,14},{14,12},{16,18},{18,... | collective-permute-start | bytes 98312 | tf_op jit(solution)/shard_map/ppermute | solution.py:491
  33.4 14.5 %all-to-all-start.1 = ((bf16[16,8,2176]{2,1,0:T(8,128)(2,1)}), bf16[16,8,2176]{2,1,0:T(8,128)(2,1)S(1)}, u32[]{:S(2)}, u32[]{:S(2)}) async-start(bf16[16,8,2176]{2,1,0:T(8,128)(2,1)} %bitcast.20), calls=%async_computation.1 | async-start | bytes 1114112 | tf_op jit(solution)/shard_map/all_to_all | solution.py:684

commit v5 on v4

--- a/solution.py
+++ b/solution.py
@@ -310,13 +310,12 @@
             (gate_hbm, gate_s),
             (twin_inner_hbm, twin_inner_s),
             (twin_gate_hbm, twin_gate_s),
-            (own_hbm, proj_ref.at[0]),
-            (twin_own_hbm, proj_ref.at[1]),
         )
         + tuple(
             (saved_hbm.at[pl.ds(kv * 4 + core * 2, 2)], low_s.at[kv * 2 : kv * 2 + 2])
             for kv in range(16)
-        ),
+        )
+        + ((own_hbm, proj_ref.at[0]), (twin_own_hbm, proj_ref.at[1])),
         sems,
     )
     normed = nrm_ref[...]
@@ -338,9 +337,11 @@
     both = dot(high, pick) + (dot(mid, pick) + dot(low, pick))
     rows_ref[0] = both[:, 0:128]
     rows_ref[1] = both[:, 128:256]
-    for copy in copies[5:]:
+    for copy in copies[5:21]:
         copy.wait()
     low_ref[...] = low_s[...].astype(bf16)
+    for copy in copies[21:]:
+        copy.wait()
 
 
 def main_kernel(

time: 49 us -> 48.9 us (level)
  no operation moved by 1% of the time
where the time goes in v5:
time: 48.9 us; the launch traced here: 48.6 us
  waiting for transfers between devices  17.7 us (36%)
  Pallas kernels  15.1 us (31%)
  starting transfers between devices  15 us (31%)
  between operations  0.76 us (2%)
    all_to_all x1, starting transfers between devices, body(): mine = lax.all_to_all(sent, 'kv', 0, 0, tiled=True)  7.75 us
    all_to_all x1, waiting for transfers between devices, body(): mine = lax.all_to_all(sent, 'kv', 0, 0, tiled=True)  7.15 us
    all_to_all x1, waiting for transfers between devices, body(): lax.all_to_all(partial.reshape(16, 8, 2176), 'kv', 0, 0, tiled=True)  6.33 us
    pallas_call x1, Pallas kernels, body(): pl.pallas_call(state_kernel, in_specs=[anywhere] * 2 + [whole()] * 2, out...  4.47 us
    ppermute x9, waiting for transfers between devices, swapped(): lax.ppermute(value, axis, [(k, k ^ 1) for k in range(lax.axis_size(axis))])  4.19 us
    ppermute x9, starting transfers between devices, swapped(): lax.ppermute(value, axis, [(k, k ^ 1) for k in range(lax.axis_size(axis))])  3.66 us
    all_to_all x1, starting transfers between devices, body(): lax.all_to_all(partial.reshape(16, 8, 2176), 'kv', 0, 0, tiled=True)  3.59 us
    pallas_call x1, Pallas kernels, body(): pl.pallas_call(rows_kernel, in_specs=[whole()] + [anywhere] * 8, out_spec...  2.76 us
  transfers between devices with their start and end apart: 11, of which 5 were waited for; matrix products, arithmetic and copies ran while one was open for 0% of the time, Pallas kernels for 20%

profile of v5, /device:TPU:0, one launch (start us, length us, event | category | flops | bytes accessed | tf_op | source)
XLA Modules:
  0.0 48.6 jit_solution(16816935475690422858)
XLA Ops:
  0.6 0.0 copy-start
  0.6 2.6 %prep.1 = (bf16[32,128,128]{2,1,0:T(8,128)(2,1)}, f32[8,64,128]{2,1,0:T(8,128)S(1)}, f32[64,128]{1,0:T(8,128)S(1)}, f32[24,128]{1,0:T(8,128)S(1)}, f32[8,32,128]{2,1,0:T(8,128)S(1)}) custom-call(f32[64,128,128]{2,1,0:T(8,128)} %bitcast.17, bf16[7,64,128]{2,1,0:T(8,128)(2,1)} %bitcast.25, bf16[4,4096]{1,0:T(4,128)(2,1)} %tin_hbm.1, bf16[4,1024]{1,0:T(4,128)(2,1)} %tw_hbm.1, ...), custom_call_target="tpu_custom_call" | custom-call | tf_op jit(solution)/shard_map/prep/pallas_call | solution.py:565
  3.3 0.1 collective-permute-start.8
  3.4 1.7 %begin.1 = (bf16[16,8,2048]{2,1,0:T(8,128)(2,1)}, bf16[80,2048]{1,0:T(8,128)(2,1)S(1)}, bf16[16,2048]{1,0:T(8,128)(2,1)S(1)}) custom-call(bf16[8,2048]{1,0:T(8,128)(2,1)} %tok_hbm.1, bf16[32,2048]{1,0:T(8,128)(2,1)} %bitcast.23, bf16[32,2048]{1,0:T(8,128)(2,1)} %bitcast.24, bf16[7,32,64]{2,1,0:T(8,128)(2,1)} %bitcast.26, bf16[7,32,64]{2,1,0:T(8,128)(2,1)} %bitcast.27), custom_call_target="tpu_custom_call" | custom-call | tf_op jit(solution)/shard_map/begin/pallas_call | solution.py:532
  5.1 1.8 %collective-permute-start.5 = (bf16[16,2048]{1,0:T(8,128)(2,1)S(1)}, bf16[16,2048]{1,0:T(8,128)(2,1)S(1)}, u32[]{:S(2)}, u32[]{:S(2)}) collective-permute-start(bf16[16,2048]{1,0:T(8,128)(2,1)S(1)} %get-tuple-element.20), channel_id=1, source_target_pairs={{0,2},{2,0},{4,6},{6,4},{8,10},{10,8},{12,14},{14,12},{16,18},{18,... | collective-permute-start | bytes 196616 | tf_op jit(solution)/shard_map/ppermute | solution.py:492
  6.9 0.2 collective-permute-start.2
  7.1 7.8 %all-to-all-start = ((bf16[16,8,2048]{2,1,0:T(8,128)(2,1)}), bf16[16,8,2048]{2,1,0:T(8,128)(2,1)S(1)}, u32[]{:S(2)}, u32[]{:S(2)}) async-start(bf16[16,8,2048]{2,1,0:T(8,128)(2,1)} %get-tuple-element.15), calls=%async_computation | async-start | bytes 1048576 | tf_op jit(solution)/shard_map/all_to_all | solution.py:557
  14.9 0.1 collective-permute-start.3
  15.0 0.5 %collective-permute-start.4 = (bf16[128,2048]{1,0:T(8,128)(2,1)}, bf16[128,2048]{1,0:T(8,128)(2,1)}, u32[]{:S(2)}, u32[]{:S(2)}) collective-permute-start(bf16[128,2048]{1,0:T(8,128)(2,1)} %own_hbm.1), channel_id=1, source_target_pairs={{0,1},{1,0},{2,3},{3,2},{4,5},{5,4},{6,7},{7,6},{8,9},{9,8},{10,11... | collective-permute-start | bytes 1572872 | tf_op jit(solution)/shard_map/ppermute | solution.py:492
  15.4 0.0 collective-permute-done.5.near_ref
  15.4 0.1 collective-permute-start.6
  15.5 2.4 %collective-permute-done.6.far_ref = bf16[16,2048]{1,0:T(8,128)(2,1)S(1)} collective-permute-done((bf16[16,2048]{1,0:T(8,128)(2,1)S(1)}, bf16[16,2048]{1,0:T(8,128)(2,1)S(1)}, u32[]{:S(2)}, u32[]{:S(2)}) %collective-permute-start.6) | collective-permute-done | bytes 65568 | tf_op jit(solution)/shard_map/ppermute | solution.py:492
  17.9 0.1 collective-permute-start
  18.1 1.5 %collective-permute-done.twin_ref = bf16[80,2048]{1,0:T(8,128)(2,1)S(1)} collective-permute-done((bf16[80,2048]{1,0:T(8,128)(2,1)S(1)}, bf16[80,2048]{1,0:T(8,128)(2,1)S(1)}, u32[]{:S(2)}, u32[]{:S(2)}) %collective-permute-start) | collective-permute-done | bytes 327712 | tf_op jit(solution)/shard_map/ppermute | solution.py:492
  19.6 0.1 collective-permute-start.7
  19.7 7.1 %all-to-all-done.mine_ref = bf16[16,8,2048]{2,1,0:T(8,128)(2,1)S(1)} async-done(((bf16[16,8,2048]{2,1,0:T(8,128)(2,1)}), bf16[16,8,2048]{2,1,0:T(8,128)(2,1)S(1)}, u32[]{:S(2)}, u32[]{:S(2)}) %all-to-all-start) | async-done | bytes 524320 | tf_op jit(solution)/shard_map/all_to_all | solution.py:557
  26.9 0.0 copy-done
  26.9 0.5 %norm.1 = (bf16[128,2048]{1,0:T(8,128)(2,1)S(1)}, bf16[128,128]{1,0:T(8,128)(2,1)S(1)}) custom-call(bf16[16,8,2048]{2,1,0:T(8,128)(2,1)S(1)} %all-to-all-done.mine_ref, f32[1,2048]{1,0:T(1,128)S(1)} %bitcast.16, bf16[80,2048]{1,0:T(8,128)(2,1)S(1)} %get-tuple-element.16.own_ref, bf16[80,2048]{1,0:T(8,128)(2,1)S(1)} %collective-permute-done.twin_ref), custom_call_target="tpu_custom_call" | custom-call | tf_op jit(solution)/shard_map/norm/pallas_call | solution.py:624
  27.4 0.0 collective-permute-done.2.twin_inner_hbm
  27.4 0.6 %collective-permute-start.1 = (bf16[128,128]{1,0:T(8,128)(2,1)S(1)}, bf16[128,128]{1,0:T(8,128)(2,1)S(1)}, u32[]{:S(2)}, u32[]{:S(2)}) collective-permute-start(bf16[128,128]{1,0:T(8,128)(2,1)S(1)} %get-tuple-element.17.own_rows_ref), channel_id=1, source_target_pairs={{0,2},{2,0},{4,6},{6,4},{8,10},{10,8},{12,14},{14,12},{16,18},{18,... | collective-permute-start | bytes 98312 | tf_op jit(solution)/shard_map/ppermute | solution.py:492
  28.0 0.3 group.1.mix_s
  28.3 0.0 collective-permute-done.3.twin_gate_hbm
  28.3 0.0 collective-permute-done.4.twin_own_hbm
  28.3 2.8 %rows.1 = (f32[6,128,128]{2,1,0:T(8,128)S(1)}, bf16[2,128,2048]{2,1,0:T(8,128)(2,1)S(1)}, bf16[32,128,128]{2,1,0:T(8,128)(2,1)S(1)}) custom-call(bf16[128,2048]{1,0:T(8,128)(2,1)S(1)} %get-tuple-element.18.nrm_ref, bf16[64,2048]{1,0:T(8,128)(2,1)} %bitcast.22, bf16[2048,128]{1,0:T(8,128)(2,1)} %inner_hbm.1, bf16[2048,128]{1,0:T(8,128)(2,1)} %gate_hbm.1, ...), custom_call_target="tpu_custom_call" | custom-call | tf_op jit(solution)/shard_map/rows/pallas_call | solution.py:634
  31.1 0.0 collective-permute-done.7.got_ref
  31.1 0.3 collective-permute-done.1.near_rows_ref
  31.4 0.0 collective-permute-done.8.twin_low_ref
  31.4 2.0 %main.1.after_hbm = bf16[128,2176]{1,0:T(8,128)(2,1)} custom-call(bf16[128,128]{1,0:T(8,128)(2,1)S(1)} %get-tuple-element.17.own_rows_ref, bf16[128,128]{1,0:T(8,128)(2,1)S(1)} %collective-permute-done.1.near_rows_ref, f32[6,128,128]{2,1,0:T(8,128)S(1)} %get-tuple-element.19.rows_s, f32[10,64,128]{2,1,0:T(8,128)S(1)} %group.1.mix_s, ...), custom_call_target="tpu_custom_call" | custom-call | tf_op jit(solution)/shard_map/main/pallas_call | solution.py:670
  33.4 3.6 %all-to-all-start.1 = ((bf16[16,8,2176]{2,1,0:T(8,128)(2,1)}), bf16[16,8,2176]{2,1,0:T(8,128)(2,1)S(1)}, u32[]{:S(2)}, u32[]{:S(2)}) async-start(bf16[16,8,2176]{2,1,0:T(8,128)(2,1)} %bitcast.20), calls=%async_computation.1 | async-start | bytes 1114112 | tf_op jit(solution)/shard_map/all_to_all | solution.py:685
  37.0 4.5 %state.1 = f32[64,128,128]{2,1,0:T(8,128)} custom-call(f32[64,128,128]{2,1,0:T(8,128)} %bitcast.19, bf16[128,2176]{1,0:T(8,128)(2,1)} %main.1.after_hbm, f32[8,64,128]{2,1,0:T(8,128)S(1)} %get-tuple-element.26.held_s, f32[10,64,128]{2,1,0:T(8,128)S(1)} %group.1.mix_s), custom_call_target="tpu_custom_call" | custom-call | tf_op jit(solution)/shard_map/state/pallas_call | solution.py:686
  41.5 6.3 %all-to-all-done.1.in_ref = bf16[16,8,2176]{2,1,0:T(8,128)(2,1)S(1)} async-done(((bf16[16,8,2176]{2,1,0:T(8,128)(2,1)}), bf16[16,8,2176]{2,1,0:T(8,128)(2,1)S(1)}, u32[]{:S(2)}, u32[]{:S(2)}) %all-to-all-start.1) | async-done | bytes 557088 | tf_op jit(solution)/shard_map/all_to_all | solution.py:685
  47.8 0.7 %total.1 = bf16[8,2048]{1,0:T(8,128)(2,1)} custom-call(bf16[16,8,2176]{2,1,0:T(8,128)(2,1)S(1)} %all-to-all-done.1.in_ref), custom_call_target="tpu_custom_call" | custom-call | tf_op jit(solution)/shard_map/total/pallas_call | solution.py:700
Async XLA Ops:
  0.6 26.2 %copy-start = (f32[2048]{0:T(1024)S(1)}, f32[2048]{0:T(1024)}, u32[]{:S(2)}) copy-start(f32[2048]{0:T(1024)} %param.22) | copy-start | bytes 24580
  3.3 28.1 %collective-permute-start.8 = (bf16[32,128,128]{2,1,0:T(8,128)(2,1)}, bf16[32,128,128]{2,1,0:T(8,128)(2,1)S(1)}, u32[]{:S(2)}, u32[]{:S(2)}) collective-permute-start(bf16[32,128,128]{2,1,0:T(8,128)(2,1)} %get-tuple-element.27), channel_id=1, source_target_pairs={{0,1},{1,0},{2,3},{3,2},{4,5},{5,4},{6,7},{7,6},{8,9},{9,8},{10,11... | collective-permute-start | bytes 3145736 | tf_op jit(solution)/shard_map/ppermute | solution.py:492
  5.1 10.3 %collective-permute-start.5 = (bf16[16,2048]{1,0:T(8,128)(2,1)S(1)}, bf16[16,2048]{1,0:T(8,128)(2,1)S(1)}, u32[]{:S(2)}, u32[]{:S(2)}) collective-permute-start(bf16[16,2048]{1,0:T(8,128)(2,1)S(1)} %get-tuple-element.20), channel_id=1, source_target_pairs={{0,2},{2,0},{4,6},{6,4},{8,10},{10,8},{12,14},{14,12},{16,18},{18,... | collective-permute-start | bytes 196616 | tf_op jit(solution)/shard_map/ppermute | solution.py:492
  6.9 20.5 %collective-permute-start.2 = (bf16[2048,128]{1,0:T(8,128)(2,1)}, bf16[2048,128]{1,0:T(8,128)(2,1)}, u32[]{:S(2)}, u32[]{:S(2)}) collective-permute-start(bf16[2048,128]{1,0:T(8,128)(2,1)} %inner_hbm.1), channel_id=1, source_target_pairs={{0,1},{1,0},{2,3},{3,2},{4,5},{5,4},{6,7},{7,6},{8,9},{9,8},{10,11... | collective-permute-start | bytes 1572872 | tf_op jit(solution)/shard_map/ppermute | solution.py:492
  7.1 19.8 %all-to-all-start = ((bf16[16,8,2048]{2,1,0:T(8,128)(2,1)}), bf16[16,8,2048]{2,1,0:T(8,128)(2,1)S(1)}, u32[]{:S(2)}, u32[]{:S(2)}) async-start(bf16[16,8,2048]{2,1,0:T(8,128)(2,1)} %get-tuple-element.15), calls=%async_computation | async-start | bytes 1048576 | tf_op jit(solution)/shard_map/all_to_all | solution.py:557
  14.9 13.4 %collective-permute-start.3 = (bf16[2048,128]{1,0:T(8,128)(2,1)}, bf16[2048,128]{1,0:T(8,128)(2,1)}, u32[]{:S(2)}, u32[]{:S(2)}) collective-permute-start(bf16[2048,128]{1,0:T(8,128)(2,1)} %gate_hbm.1), channel_id=1, source_target_pairs={{0,1},{1,0},{2,3},{3,2},{4,5},{5,4},{6,7},{7,6},{8,9},{9,8},{10,11... | collective-permute-start | bytes 1572872 | tf_op jit(solution)/shard_map/ppermute | solution.py:492
  15.0 13.4 %collective-permute-start.4 = (bf16[128,2048]{1,0:T(8,128)(2,1)}, bf16[128,2048]{1,0:T(8,128)(2,1)}, u32[]{:S(2)}, u32[]{:S(2)}) collective-permute-start(bf16[128,2048]{1,0:T(8,128)(2,1)} %own_hbm.1), channel_id=1, source_target_pairs={{0,1},{1,0},{2,3},{3,2},{4,5},{5,4},{6,7},{7,6},{8,9},{9,8},{10,11... | collective-permute-start | bytes 1572872 | tf_op jit(solution)/shard_map/ppermute | solution.py:492
  15.4 2.5 %collective-permute-start.6 = (bf16[16,2048]{1,0:T(8,128)(2,1)S(1)}, bf16[16,2048]{1,0:T(8,128)(2,1)S(1)}, u32[]{:S(2)}, u32[]{:S(2)}) collective-permute-start(bf16[16,2048]{1,0:T(8,128)(2,1)S(1)} %collective-permute-done.5.near_ref), channel_id=1, source_target_pairs={{0,1},{1,0},{2,3},{3,2},{4,5},{5,4},{6,7},{7,6},{8,9},{9,8},{10,11... | collective-permute-start | bytes 196616 | tf_op jit(solution)/shard_map/ppermute | solution.py:492
  17.9 1.6 %collective-permute-start = (bf16[80,2048]{1,0:T(8,128)(2,1)S(1)}, bf16[80,2048]{1,0:T(8,128)(2,1)S(1)}, u32[]{:S(2)}, u32[]{:S(2)}) collective-permute-start(bf16[80,2048]{1,0:T(8,128)(2,1)S(1)} %get-tuple-element.16.own_ref), channel_id=1, source_target_pairs={{0,1},{1,0},{2,3},{3,2},{4,5},{5,4},{6,7},{7,6},{8,9},{9,8},{10,11... | collective-permute-start | bytes 983048 | tf_op jit(solution)/shard_map/ppermute | solution.py:492
  19.6 11.5 %collective-permute-start.7 = (f32[8,32,128]{2,1,0:T(8,128)S(1)}, f32[8,32,128]{2,1,0:T(8,128)S(1)}, u32[]{:S(2)}, u32[]{:S(2)}) collective-permute-start(f32[8,32,128]{2,1,0:T(8,128)S(1)} %get-tuple-element.23), channel_id=1, source_target_pairs={{0,1},{1,0},{2,3},{3,2},{4,5},{5,4},{6,7},{7,6},{8,9},{9,8},{10,11... | collective-permute-start | bytes 393224 | tf_op jit(solution)/shard_map/ppermute | solution.py:492
  27.4 4.0 %collective-permute-start.1 = (bf16[128,128]{1,0:T(8,128)(2,1)S(1)}, bf16[128,128]{1,0:T(8,128)(2,1)S(1)}, u32[]{:S(2)}, u32[]{:S(2)}) collective-permute-start(bf16[128,128]{1,0:T(8,128)(2,1)S(1)} %get-tuple-element.17.own_rows_ref), channel_id=1, source_target_pairs={{0,2},{2,0},{4,6},{6,4},{8,10},{10,8},{12,14},{14,12},{16,18},{18,... | collective-permute-start | bytes 98312 | tf_op jit(solution)/shard_map/ppermute | solution.py:492
  33.4 14.4 %all-to-all-start.1 = ((bf16[16,8,2176]{2,1,0:T(8,128)(2,1)}), bf16[16,8,2176]{2,1,0:T(8,128)(2,1)S(1)}, u32[]{:S(2)}, u32[]{:S(2)}) async-start(bf16[16,8,2176]{2,1,0:T(8,128)(2,1)} %bitcast.20), calls=%async_computation.1 | async-start | bytes 1114112 | tf_op jit(solution)/shard_map/all_to_all | solution.py:685
